TPU v7x, 512 devices: a whole 4x4x16 slice. The times are simulated.
512 devices in a mesh: sp: 64 (over z, y), tp: 8 (over x, core).
Axes of the slice: x: 4, y: 4, z: 16, core: 2. Of those that a mesh axis runs over, the one named last changes fastest.
Arguments:
- queries: bfloat16 [32768, 1024], P('sp', 'tp'), may hold values from -8 to 8
- key_rows: bfloat16 [32768, 512], P('sp', 'tp'), may hold values from -8 to 8
- values: bfloat16 [32768, 512], P('sp', 'tp'), may hold values from -16 to 16
- doc_ids: int32 [32768], P('sp'), may hold values from 0 to 31, never falling along the last dimension, each value on 1 to 2048 neighbouring positions
- sink_logits: float32 [16], P('tp'), may hold values from 2.5 to 6
- residual: bfloat16 [32768, 2048], P('sp'), may hold values from -6 to 6
- out_weight: bfloat16 [1024, 2048], P('tp'), may hold values from -0.1875 to 0.1875
- norm_gain: float32 [2048], replicated, may hold values from 0.1 to 1.9
- w_gate: bfloat16 [2048, 5632], P('sp', 'tp'), may hold values from -0.125 to 0.125
- w_up: bfloat16 [2048, 5632], P('sp', 'tp'), may hold values from -0.125 to 0.125
- w_down: bfloat16 [5632, 2048], P('tp', 'sp'), may hold values from -0.078125 to 0.078125
Outputs:
- layer_out: bfloat16 [32768, 2048], P('sp')
Inputs may be any that keep to these rules, and one draw needn't show every extreme that they name: `doc_ids`: document numbers never fall along the positions; each document has 1 to 2048 positions.
All inputs are finite; a program needn't handle non-finite values.
Results may differ from a plain program's by a relative error of at most 0.014.
Values may be sent and summed in bfloat16 or wider, within the bound.
No kernel may reach another device: no remote copies, remote signals or barrier semaphores. Data moves between devices by JAX's collectives and lax.ppermute only.
A program may use at most 64 MiB of HBM per device.

v0:
```python
import jax
import jax.numpy as jnp
from jax import lax
from jax.sharding import PartitionSpec as P

HD = 64
WINDOW = 128


def from_behind(shard, axis, by):
    size = lax.axis_size(axis)
    pairs = [(i, i + by) for i in range(size) if 0 <= i + by < size]
    return lax.ppermute(shard, axis, pairs)


def gather_turned(arrays, axis, dims):
    turned = [jnp.moveaxis(a, dim, 0) for a, dim in zip(arrays, dims)]
    both = jnp.concatenate([t.reshape(len(t), -1) for t in turned], axis=1)
    result, at, finished = (lax.all_gather(both, axis, axis=0, tiled=True), 0, [])
    for t, dim in zip(turned, dims):
        slab = result[:, at : at + t[0].size].reshape(-1, *t.shape[1:])
        finished.append(jnp.moveaxis(slab, 0, dim))
        at += t[0].size
    return tuple(finished)


def cut_along(shard, dim, size):
    before, after = (shard.shape[:dim], shard.shape[dim + 1 :])
    return jnp.moveaxis(shard.reshape(*before, size, -1, *after), dim, 0)


def sum_at_owner(shard, axis, dim):
    pieces = cut_along(shard, dim, lax.axis_size(axis))
    arrived = lax.all_to_all(pieces, axis, split_axis=0, concat_axis=0, tiled=True)
    return arrived.astype(jnp.float32).sum(axis=0)


def laid_out(pieces, dim):
    dims = list(pieces.shape[1:])
    dims[dim] *= pieces.shape[0]
    return jnp.moveaxis(pieces, 0, dim).reshape(dims)


def sent_to_all(shard, axis):
    size = lax.axis_size(axis)
    return lax.all_to_all(
        jnp.broadcast_to(shard[None], (size, *shard.shape)), axis, 0, 0, tiled=True
    )


def gathered_copies(shard, axis, dim):
    return laid_out(sent_to_all(shard, axis), dim)


def rms_norm(stream, norm_gain):
    floats = stream.astype(jnp.float32)
    scale = lax.rsqrt(jnp.mean(floats * floats, axis=-1, keepdims=True) + 1e-06)
    return floats * scale * norm_gain


def band_rows(tensor, blocks):
    tensor = tensor.reshape((blocks + 1, WINDOW) + tensor.shape[1:])
    return jnp.concatenate([tensor[:-1], tensor[1:]], axis=1)


def attend(queries, key_rows, values, doc_ids, sink_logits):
    local_rows = queries.shape[0]
    blocks = local_rows // WINDOW
    kv_local = key_rows.shape[1] // HD
    per_kv = queries.shape[1] // key_rows.shape[1]
    tail_docs = doc_ids[local_rows - WINDOW :] + 1
    prev_keys, prev_values, prev_docs = from_behind(
        (key_rows[local_rows - WINDOW :], values[local_rows - WINDOW :], tail_docs), "sp", 1
    )
    key_band = band_rows(jnp.concatenate([prev_keys, key_rows], axis=0), blocks).reshape(
        blocks, 2 * WINDOW, kv_local, HD
    )
    value_band = band_rows(jnp.concatenate([prev_values, values], axis=0), blocks).reshape(
        blocks, 2 * WINDOW, kv_local, HD
    )
    doc_band = band_rows(jnp.concatenate([prev_docs - 1, doc_ids]), blocks)
    query_band = queries.reshape(blocks, WINDOW, kv_local, per_kv, HD)
    scores = jnp.einsum(
        "nqhgd,nkhd->nhgqk", query_band, key_band, preferred_element_type=jnp.float32
    ) * HD ** (-0.5)
    offsets = jnp.arange(WINDOW)[:, None] + WINDOW - jnp.arange(2 * WINDOW)[None, :]
    inside = (offsets >= 0) & (offsets < WINDOW)
    query_docs = doc_ids.reshape(blocks, WINDOW)
    allowed = inside[None] & (query_docs[:, :, None] == doc_band[:, None, :])
    scores = jnp.where(allowed[:, None, None], scores, -1e30)
    sink_logit = sink_logits.reshape(kv_local, per_kv)[None, :, :, None, None]
    peak = jnp.maximum(jnp.max(scores, axis=-1, keepdims=True), sink_logit)
    raised = jnp.exp(scores - peak)
    denom = jnp.sum(raised, axis=-1, keepdims=True) + jnp.exp(sink_logit - peak)
    weights = (raised / denom).astype(jnp.bfloat16)
    attended = jnp.einsum(
        "nhgqk,nkhd->nqhgd", weights, value_band, preferred_element_type=jnp.float32
    )
    return attended.astype(jnp.bfloat16).reshape(local_rows, queries.shape[1])


def on_device(
    queries,
    key_rows,
    values,
    doc_ids,
    sink_logits,
    residual,
    out_weight,
    norm_gain,
    w_gate,
    w_up,
    w_down,
):
    gate_whole, up_whole, down_whole = gather_turned((w_gate, w_up, w_down), "sp", (0, 0, 1))
    attended = attend(queries, key_rows, values, doc_ids, sink_logits)
    row_share = residual.shape[0] // lax.axis_size("tp")
    picked = attended
    mixed_sum = sum_at_owner(
        jnp.dot(picked, out_weight, preferred_element_type=jnp.float32).astype(jnp.bfloat16),
        "tp",
        0,
    )
    base_rows = lax.dynamic_slice_in_dim(residual, lax.axis_index("tp") * row_share, row_share, 0)
    stream = (base_rows.astype(jnp.float32) + mixed_sum).astype(jnp.bfloat16)
    normed = rms_norm(stream, norm_gain).astype(jnp.bfloat16)
    normed = gathered_copies(normed, "tp", 0)
    gate_act = jnp.dot(normed, gate_whole, preferred_element_type=jnp.float32)
    up_act = jnp.dot(normed, up_whole, preferred_element_type=jnp.float32)
    hidden = (jax.nn.silu(gate_act) * up_act).astype(jnp.bfloat16)
    picked = hidden
    mlp_total = sum_at_owner(
        jnp.dot(picked, down_whole, preferred_element_type=jnp.float32).astype(jnp.bfloat16),
        "tp",
        0,
    )
    finished = (stream.astype(jnp.float32) + mlp_total).astype(jnp.bfloat16)
    return gathered_copies(finished, "tp", 0)


def solution(mesh):
    in_specs = (
        P("sp", "tp"),
        P("sp", "tp"),
        P("sp", "tp"),
        P("sp"),
        P("tp"),
        P("sp", None),
        P("tp", None),
        P(),
        P("sp", "tp"),
        P("sp", "tp"),
        P("tp", "sp"),
    )
    out_specs = P("sp", None)
    return jax.shard_map(
        on_device, mesh=mesh, in_specs=in_specs, out_specs=out_specs, check_vma=False
    )
```

profile of v0, /device:TPU:1, one launch (start us, length us, event | category | flops | bytes accessed | tf_op | source)
XLA Modules:
  0.0 256.9 jit_solution(4028181509367564481)
XLA Ops:
  6.5 0.0 copy-start
  6.5 0.0 copy-start.2
  6.5 0.0 all-gather.2.cloned.1.call-start
  6.5 1.7 concatenate.27
  8.2 0.0 all-gather.2.cloned.1.call-update
  8.2 0.7 slice_add_fusion
  8.9 4.0 %collective-permute-start.1 = (s32[128]{0:T(128)S(1)}, s32[128]{0:T(128)S(1)}, u32[]{:S(2)}, u32[]{:S(2)}) collective-permute-start(s32[128]{0:T(128)S(1)} %slice_add_fusion), channel_id=1, source_target_pairs={{0,8},{8,16},{16,24},{24,32},{32,40},{40,48},{48,56},{56,64},{64,7... | collective-permute-start | bytes 1544 | tf_op jit(solution)/shard_map/ppermute | solution.py:13
  12.9 0.7 slice.56
  13.7 3.2 %collective-permute-start = (bf16[128,64]{0,1:T(8,128)(2,1)S(1)}, bf16[128,64]{0,1:T(8,128)(2,1)S(1)}, u32[]{:S(2)}, u32[]{:S(2)}) collective-permute-start(bf16[128,64]{0,1:T(8,128)(2,1)S(1)} %slice.56), channel_id=1, source_target_pairs={{0,8},{8,16},{16,24},{24,32},{32,40},{40,48},{48,56},{56,64},{64,7... | collective-permute-start | bytes 49160 | tf_op jit(solution)/shard_map/ppermute | solution.py:13
  16.9 0.7 slice.63
  17.6 2.9 %collective-permute-start.2 = (bf16[128,64]{0,1:T(8,128)(2,1)S(1)}, bf16[128,64]{0,1:T(8,128)(2,1)S(1)}, u32[]{:S(2)}, u32[]{:S(2)}) collective-permute-start(bf16[128,64]{0,1:T(8,128)(2,1)S(1)} %slice.63), channel_id=1, source_target_pairs={{0,8},{8,16},{16,24},{24,32},{32,40},{40,48},{48,56},{56,64},{64,7... | collective-permute-start | bytes 49160 | tf_op jit(solution)/shard_map/ppermute | solution.py:13
  20.5 0.9 copy_bitcast_fusion
  21.4 0.9 copy_bitcast_fusion.2
  22.3 1.0 reshape.134
  23.3 0.0 collective-permute-done.1
  23.3 0.7 pad_add_fusion
  24.0 0.7 pad_add_fusion.1
  24.7 0.9 compare_and_fusion
  25.6 0.0 collective-permute-done.2
  25.6 0.8 copy_bitcast_fusion.1
  26.4 0.0 collective-permute-done
  26.4 0.8 copy_bitcast_fusion.3
  27.3 0.4 fusion.42
  27.6 0.0 copy-done.2
  27.6 0.1 broadcast_maximum_fusion
  27.7 0.2 fusion.20
  27.9 0.1 exponential_add_fusion
  27.9 0.3 fusion.19
  28.3 0.1 copy.21
  28.4 0.0 copy-done
  28.4 2.1 convolution_convert_fusion
  30.4 5.8 %all-to-all-start = ((bf16[8,64,2048]{2,1,0:T(8,128)(2,1)}), bf16[8,64,2048]{2,1,0:T(8,128)(2,1)S(1)}, u32[]{:S(2)}, u32[]{:S(2)}) async-start(bf16[8,64,2048]{2,1,0:T(8,128)(2,1)} %bitcast.63), calls=%async_computation | async-start | bytes 4194304 | tf_op jit(solution)/shard_map/all_to_all | solution.py:34
  36.2 0.0 copy-start.1
  36.2 26.2 %all-to-all-done = bf16[8,64,2048]{2,1,0:T(8,128)(2,1)S(1)} async-done(((bf16[8,64,2048]{2,1,0:T(8,128)(2,1)}), bf16[8,64,2048]{2,1,0:T(8,128)(2,1)S(1)}, u32[]{:S(2)}, u32[]{:S(2)}) %all-to-all-start) | async-done | bytes 2097184 | tf_op jit(solution)/shard_map/all_to_all | solution.py:34
  62.4 0.4 convert_reduce_fusion.1
  62.8 1.1 fusion.22
  64.0 0.0 copy-done.1
  64.0 0.1 fusion.24
  64.1 0.2 broadcast_in_dim.18
  64.4 29.6 %all_to_all.20 = bf16[8,64,2048]{2,1,0:T(8,128)(2,1)S(1)} all-to-all(bf16[8,64,2048]{2,1,0:T(8,128)(2,1)S(1)} %broadcast_in_dim.18), channel_id=1, replica_groups=mesh['sp'=64,'tp'=8] {'tp'}, dimensions={0} | all-to-all | bytes 4194304 | tf_op jit(solution)/shard_map/all_to_all | solution.py:46
  94.0 71.6 %all-gather.2.cloned.1.call-done = bf16[2048,2112]{1,0:T(8,128)(2,1)} async-done(((bf16[32,2112]{1,0:T(8,128)(2,1)}), bf16[2048,2112]{1,0:T(8,128)(2,1)}) %all-gather.2.cloned.1.call-update) | async-done | bytes 8650768 | tf_op jit(solution)/shard_map/all_gather | solution.py:19
  165.5 4.7 %fusion.4 = f32[512,704]{0,1:T(8,128)} fusion(bf16[512,2048]{1,0:T(8,128)(2,1)S(1)} %bitcast.65, bf16[2048,2112]{1,0:T(8,128)(2,1)} %all-gather.2.cloned.1.call-done), kind=kOutput, calls=%fused_computation.6 | convolution fusion | flops 1476395008 | bytes 6684672 | tf_op jit(solution)/shard_map/dot_general | solution.py:128
  170.3 9.4 %fusion.6 = bf16[512,2048]{1,0:T(8,128)(2,1)} fusion(bf16[2048,2112]{1,0:T(8,128)(2,1)} %all-gather.2.cloned.1.call-done, bf16[512,2048]{1,0:T(8,128)(2,1)S(1)} %bitcast.66, f32[512,704]{0,1:T(8,128)} %fusion.4), kind=kOutput, calls=%fused_computation.9 | convolution fusion | flops 2956001280 | bytes 11927552 | tf_op jit(solution)/shard_map/dot_general | solution.py:133
  179.7 38.7 %all_to_all.21 = bf16[8,64,2048]{2,1,0:T(8,128)(2,1)S(1)} all-to-all(bf16[8,64,2048]{2,1,0:T(8,128)(2,1)} %bitcast.67), channel_id=1, replica_groups=mesh['sp'=64,'tp'=8] {'tp'}, dimensions={0} | all-to-all | bytes 4194304 | tf_op jit(solution)/shard_map/all_to_all | solution.py:34
  218.4 0.4 convert_reduce_fusion
  218.8 0.1 fusion.25
  218.8 0.2 broadcast_in_dim.19
  219.1 29.7 %all_to_all.22 = bf16[8,64,2048]{2,1,0:T(8,128)(2,1)S(1)} all-to-all(bf16[8,64,2048]{2,1,0:T(8,128)(2,1)S(1)} %broadcast_in_dim.19), channel_id=1, replica_groups=mesh['sp'=64,'tp'=8] {'tp'}, dimensions={0} | all-to-all | bytes 4194304 | tf_op jit(solution)/shard_map/all_to_all | solution.py:46
  248.7 1.3 copy.45
  (5 shorter events, 0.1 us)
Async XLA Ops:
  6.5 21.8 %copy-start = (bf16[128,2048]{1,0:T(8,128)(2,1)S(1)}, bf16[128,2048]{1,0:T(8,128)(2,1)}, u32[]{:S(2)}) copy-start(bf16[128,2048]{1,0:T(8,128)(2,1)} %param.17) | copy-start | bytes 1572868
  6.5 21.1 %copy-start.2 = (f32[2]{0:T(128)S(1)}, f32[2]{0:T(128)}, u32[]{:S(2)}) copy-start(f32[2]{0:T(128)} %param.15) | copy-start | bytes 28
  6.5 159.0 %all-gather.2.cloned.1.call-start = ((), (), s32[]{:S(2)}) async-start(), calls=%async_computation.4 | async-start | bytes 9052160 | tf_op jit(solution)/shard_map/all_gather | solution.py:19
  8.9 14.4 %collective-permute-start.1 = (s32[128]{0:T(128)S(1)}, s32[128]{0:T(128)S(1)}, u32[]{:S(2)}, u32[]{:S(2)}) collective-permute-start(s32[128]{0:T(128)S(1)} %slice_add_fusion), channel_id=1, source_target_pairs={{0,8},{8,16},{16,24},{24,32},{32,40},{40,48},{48,56},{56,64},{64,7... | collective-permute-start | bytes 1544 | tf_op jit(solution)/shard_map/ppermute | solution.py:13
  13.7 12.8 %collective-permute-start = (bf16[128,64]{0,1:T(8,128)(2,1)S(1)}, bf16[128,64]{0,1:T(8,128)(2,1)S(1)}, u32[]{:S(2)}, u32[]{:S(2)}) collective-permute-start(bf16[128,64]{0,1:T(8,128)(2,1)S(1)} %slice.56), channel_id=1, source_target_pairs={{0,8},{8,16},{16,24},{24,32},{32,40},{40,48},{48,56},{56,64},{64,7... | collective-permute-start | bytes 49160 | tf_op jit(solution)/shard_map/ppermute | solution.py:13
  17.6 8.0 %collective-permute-start.2 = (bf16[128,64]{0,1:T(8,128)(2,1)S(1)}, bf16[128,64]{0,1:T(8,128)(2,1)S(1)}, u32[]{:S(2)}, u32[]{:S(2)}) collective-permute-start(bf16[128,64]{0,1:T(8,128)(2,1)S(1)} %slice.63), channel_id=1, source_target_pairs={{0,8},{8,16},{16,24},{24,32},{32,40},{40,48},{48,56},{56,64},{64,7... | collective-permute-start | bytes 49160 | tf_op jit(solution)/shard_map/ppermute | solution.py:13
  30.4 32.0 %all-to-all-start = ((bf16[8,64,2048]{2,1,0:T(8,128)(2,1)}), bf16[8,64,2048]{2,1,0:T(8,128)(2,1)S(1)}, u32[]{:S(2)}, u32[]{:S(2)}) async-start(bf16[8,64,2048]{2,1,0:T(8,128)(2,1)} %bitcast.63), calls=%async_computation | async-start | bytes 4194304 | tf_op jit(solution)/shard_map/all_to_all | solution.py:34
  36.2 27.7 %copy-start.1 = (f32[2048]{0:T(1024)S(1)}, f32[2048]{0:T(1024)}, u32[]{:S(2)}) copy-start(f32[2048]{0:T(1024)} %param.18) | copy-start | bytes 24580
Sparse Core Ops, SparseCore 0:
  10.3 155.2 all-gather.1
where the time goes:
time: 258 us; the launch traced here: 257 us
  blocking collectives  97.9 us (38%)
  waiting for transfers between devices  97.8 us (38%)
  matrix products  16.9 us (7%)
  starting transfers between devices  15.9 us (6%)
  between operations  13.6 us (5%)
  local copies, waits for them, and re-layouts  7.79 us (3%)
  other arithmetic  6.98 us (3%)
    all_gather x1, waiting for transfers between devices, gather_turned(): lax.all_gather(both, axis, axis=0, tiled=True)  71.6 us
    all_to_all x2, blocking collectives, sent_to_all(): lax.all_to_all(jnp.broadcast_to(shard[None], (size, *shard.shape)), axis,...  59.2 us
    all_to_all x1, blocking collectives, sum_at_owner(): lax.all_to_all(pieces, axis, split_axis=0, concat_axis=0, tiled=True)  38.7 us
    all_to_all x1, waiting for transfers between devices, sum_at_owner(): lax.all_to_all(pieces, axis, split_axis=0, concat_axis=0, tiled=True)  26.2 us
    ppermute x3, starting transfers between devices, from_behind(): return lax.ppermute(shard, axis, pairs)  10.1 us
    dot_general x1, matrix products, on_device(): jnp.dot(picked, down_whole, preferred_element_type=jnp.float32)  9.43 us
    all_to_all x1, starting transfers between devices, sum_at_owner(): lax.all_to_all(pieces, axis, split_axis=0, concat_axis=0, tiled=True)  5.81 us
  transfers between devices with their start and end apart: 5, of which 2 were waited for; matrix products, arithmetic and copies ran while one was open for 5% of the time, Pallas kernels for 0%

commit v1 on v0

v1 whole, which is shorter than its diff:
```python
import jax
import jax.numpy as jnp
from jax import lax
from jax.sharding import PartitionSpec as P

HD = 64
WINDOW = 128
NZ, NY, NX = 16, 4, 4
FAR_Z = [[z * NY + y for z in range(NZ)] for y in range(NY)]
FAR_Y = [[z * NY + y for y in range(NY)] for z in range(NZ)]
FAR_X = [[2 * x + c for x in range(NX)] for c in range(2)]


def from_behind(shard, axis, by):
    size = lax.axis_size(axis)
    pairs = [(i, i + by) for i in range(size) if 0 <= i + by < size]
    return lax.ppermute(shard, axis, pairs)


def other_core(shard):
    return lax.ppermute(shard, "tp", [(i, i ^ 1) for i in range(2 * NX)])


def swapped(pieces, axis, groups):
    return lax.all_to_all(pieces, axis, 0, 0, tiled=True, axis_index_groups=groups)


def copies(shard, axis, groups):
    return swapped(jnp.broadcast_to(shard[None], (len(groups[0]), *shard.shape)), axis, groups)


def rms_norm(stream, norm_gain):
    floats = stream.astype(jnp.float32)
    scale = lax.rsqrt(jnp.mean(floats * floats, axis=-1, keepdims=True) + 1e-06)
    return floats * scale * norm_gain


def band_rows(tensor, blocks):
    tensor = tensor.reshape((blocks + 1, WINDOW) + tensor.shape[1:])
    return jnp.concatenate([tensor[:-1], tensor[1:]], axis=1)


def attend(queries, key_rows, values, doc_ids, sink_logits):
    local_rows = queries.shape[0]
    blocks = local_rows // WINDOW
    kv_local = key_rows.shape[1] // HD
    per_kv = queries.shape[1] // key_rows.shape[1]
    width = key_rows.shape[1]
    tail = local_rows - WINDOW
    tail_docs = (doc_ids[tail:] + 1).astype(jnp.bfloat16)
    tail_rows = jnp.concatenate([key_rows[tail:], values[tail:]], axis=1)
    docs_rows = jnp.broadcast_to(tail_docs.reshape(-1, 2 * width), (8 * WINDOW // (2 * width), 2 * width))
    before = from_behind(jnp.concatenate([tail_rows, docs_rows], axis=0), "sp", 1)
    prev_keys, prev_values = before[:WINDOW, :width], before[:WINDOW, width:]
    prev_docs = before[WINDOW].reshape(-1).astype(jnp.int32) - 1
    key_band = band_rows(jnp.concatenate([prev_keys, key_rows], axis=0), blocks).reshape(
        blocks, 2 * WINDOW, kv_local, HD
    )
    value_band = band_rows(jnp.concatenate([prev_values, values], axis=0), blocks).reshape(
        blocks, 2 * WINDOW, kv_local, HD
    )
    doc_band = band_rows(jnp.concatenate([prev_docs, doc_ids]), blocks)
    query_band = queries.reshape(blocks, WINDOW, kv_local, per_kv, HD)
    scores = jnp.einsum(
        "nqhgd,nkhd->nhgqk", query_band, key_band, preferred_element_type=jnp.float32
    ) * HD ** (-0.5)
    offsets = jnp.arange(WINDOW)[:, None] + WINDOW - jnp.arange(2 * WINDOW)[None, :]
    inside = (offsets >= 0) & (offsets < WINDOW)
    query_docs = doc_ids.reshape(blocks, WINDOW)
    allowed = inside[None] & (query_docs[:, :, None] == doc_band[:, None, :])
    scores = jnp.where(allowed[:, None, None], scores, -1e30)
    sink_logit = sink_logits.reshape(kv_local, per_kv)[None, :, :, None, None]
    peak = jnp.maximum(jnp.max(scores, axis=-1, keepdims=True), sink_logit)
    raised = jnp.exp(scores - peak)
    denom = jnp.sum(raised, axis=-1, keepdims=True) + jnp.exp(sink_logit - peak)
    weights = (raised / denom).astype(jnp.bfloat16)
    attended = jnp.einsum(
        "nhgqk,nkhd->nqhgd", weights, value_band, preferred_element_type=jnp.float32
    )
    return attended.astype(jnp.bfloat16).reshape(local_rows, queries.shape[1])


def sum_at_owner(theirs, mine):
    arrived = other_core(theirs)
    pair_sum = (mine + arrived.astype(jnp.float32)).astype(jnp.bfloat16)
    pieces = swapped(pair_sum.reshape(NX, -1, pair_sum.shape[1]), "tp", FAR_X)
    return pieces.astype(jnp.float32).sum(axis=0)


def on_device(
    queries,
    key_rows,
    values,
    doc_ids,
    sink_logits,
    residual,
    out_weight,
    norm_gain,
    w_gate,
    w_up,
    w_down,
):
    rows, width = residual.shape
    half, share = rows // 2, rows // (2 * NX)
    core = lax.rem(lax.axis_index("tp"), 2)
    chip = lax.div(lax.axis_index("tp"), 2)
    ff = w_gate.shape[1]

    near = copies(jnp.concatenate([w_gate, w_up], axis=1), "sp", FAR_Y)
    near = near.reshape(-1, 2 * ff)
    gate_up = lax.all_gather(near, "sp", axis=0, tiled=True, axis_index_groups=FAR_Z)
    column = lax.all_gather(w_down.T, "sp", axis=0, tiled=True, axis_index_groups=FAR_Z)
    down = copies(column, "sp", FAR_Y)
    down = jnp.swapaxes(down.reshape(NY, NZ, -1, ff), 0, 1).reshape(width, ff)

    attended = attend(queries, key_rows, values, doc_ids, sink_logits)
    at_mine = lax.dynamic_slice_in_dim(attended, core * half, half, 0)
    at_theirs = lax.dynamic_slice_in_dim(attended, (1 - core) * half, half, 0)
    mixed_sum = sum_at_owner(
        jnp.dot(at_theirs, out_weight, preferred_element_type=jnp.float32).astype(jnp.bfloat16),
        jnp.dot(at_mine, out_weight, preferred_element_type=jnp.float32),
    )
    base_rows = lax.dynamic_slice_in_dim(residual, core * half + chip * share, share, 0)
    stream = (base_rows.astype(jnp.float32) + mixed_sum).astype(jnp.bfloat16)
    normed = rms_norm(stream, norm_gain).astype(jnp.bfloat16)
    normed = copies(normed, "tp", FAR_X).reshape(half, width)
    normed = jnp.concatenate([normed, other_core(normed)], axis=0)

    acts = jnp.dot(normed, gate_up, preferred_element_type=jnp.float32)
    hidden = (jax.nn.silu(acts[:, :ff]) * acts[:, ff:]).astype(jnp.bfloat16)

    def through(part):
        return lax.dot_general(
            part, down, (((1,), (1,)), ((), ())), preferred_element_type=jnp.float32
        )

    mlp_total = sum_at_owner(through(hidden[half:]).astype(jnp.bfloat16), through(hidden[:half]))
    finished = (stream.astype(jnp.float32) + mlp_total).astype(jnp.bfloat16)
    mine = copies(finished, "tp", FAR_X).reshape(half, width)
    theirs = other_core(mine)
    return jnp.where(
        core == 0,
        jnp.concatenate([mine, theirs], axis=0),
        jnp.concatenate([theirs, mine], axis=0),
    )


def solution(mesh):
    in_specs = (
        P("sp", "tp"),
        P("sp", "tp"),
        P("sp", "tp"),
        P("sp"),
        P("tp"),
        P("sp", None),
        P("tp", None),
        P(),
        P("sp", "tp"),
        P("sp", "tp"),
        P("tp", "sp"),
    )
    out_specs = P("sp", None)
    return jax.shard_map(
        on_device, mesh=mesh, in_specs=in_specs, out_specs=out_specs, check_vma=False
    )
```

time: 258 us -> 223 us (0.86)
  waiting for transfers between devices: 97.8 us -> 43.7 us
  starting transfers between devices: 15.9 us -> 42.2 us
  blocking collectives: 97.9 us -> 90.3 us
  local copies, waits for them, and re-layouts: 7.79 us -> 15 us
  matrix products: 16.9 us -> 10.7 us
    all_gather x1, waiting for transfers between devices: 71.6 us -> 0.01 us  [on_device(): lax.all_gather(near, 'sp', axis=0, tiled=True, axis_index_groups=FAR_Z)]
    all_to_all x3, blocking collectives: 97.9 us -> 45.6 us  [swapped(): lax.all_to_all(pieces, axis, 0, 0, tiled=True, axis_index_groups=groups)]
    all_gather x0 -> x1, blocking collectives: none -> 44.7 us  [on_device(): lax.all_gather(w_down.T, 'sp', axis=0, tiled=True, axis_index_groups=FAR_Z)]
    ppermute x0 -> x4, starting transfers between devices: none -> 29.2 us  [other_core(): return lax.ppermute(shard, 'tp', [(i, i ^ 1) for i in range(2 * NX)])]
    all_to_all x1 -> x3, waiting for transfers between devices: 26.2 us -> 36.7 us  [swapped(): lax.all_to_all(pieces, axis, 0, 0, tiled=True, axis_index_groups=groups)]
    ppermute x3 -> x1, starting transfers between devices: 10.1 us -> 2.19 us  [from_behind(): return lax.ppermute(shard, axis, pairs)]
    ppermute x0 -> x4, waiting for transfers between devices: none -> 6.78 us  [other_core(): return lax.ppermute(shard, 'tp', [(i, i ^ 1) for i in range(2 * NX)])]
    dot_general x3 -> x5, matrix products: 16.2 us -> 10 us  [the longest x1 6.04 us: on_device(): acts = jnp.dot(normed, gate_up, preferred_element_type=jnp.float32)]
  transfers between devices with their start and end apart: 5 -> 9, of which waited for: 2 -> 6; matrix products, arithmetic and copies ran while one was open for 5% -> 8% of each run, Pallas kernels for 0% -> 0%
where the time goes in v1:
time: 223 us
  blocking collectives  90.3 us (40%)
  waiting for transfers between devices  43.7 us (20%)
  starting transfers between devices  42.2 us (19%)
  local copies, waits for them, and re-layouts  15 us (7%)
  between operations  13.8 us (6%)
  matrix products  10.7 us (5%)
  other arithmetic  6.82 us (3%)
    all_to_all x3, blocking collectives, swapped(): lax.all_to_all(pieces, axis, 0, 0, tiled=True, axis_index_groups=groups)  45.6 us
    all_gather x1, blocking collectives, on_device(): lax.all_gather(w_down.T, 'sp', axis=0, tiled=True, axis_index_groups=FAR_Z)  44.7 us
    all_to_all x3, waiting for transfers between devices, swapped(): lax.all_to_all(pieces, axis, 0, 0, tiled=True, axis_index_groups=groups)  36.7 us
    ppermute x4, starting transfers between devices, other_core(): return lax.ppermute(shard, 'tp', [(i, i ^ 1) for i in range(2 * NX)])  29.2 us
    all_to_all x3, starting transfers between devices, swapped(): lax.all_to_all(pieces, axis, 0, 0, tiled=True, axis_index_groups=groups)  10.8 us
    ppermute x4, waiting for transfers between devices, other_core(): return lax.ppermute(shard, 'tp', [(i, i ^ 1) for i in range(2 * NX)])  6.78 us
    dot_general x1, matrix products, on_device(): acts = jnp.dot(normed, gate_up, preferred_element_type=jnp.float32)  6.04 us
  transfers between devices with their start and end apart: 9, of which 6 were waited for; matrix products, arithmetic and copies ran while one was open for 8% of the time, Pallas kernels for 0%

profile of v1, /device:TPU:1, one launch (start us, length us, event | category | flops | bytes accessed | tf_op | source)
XLA Modules:
  0.0 222.6 jit_solution(6885718960344058722)
XLA Ops:
  6.5 0.0 copy-start
  6.5 0.0 all-gather.2.cloned.1.call-start
  6.6 1.0 pad_maximum_fusion
  7.6 11.0 %all_to_all.30 = bf16[4,32,1408]{2,1,0:T(8,128)(2,1)} all-to-all(bf16[4,32,1408]{2,1,0:T(8,128)(2,1)S(1)} %broadcast_in_dim.26), channel_id=1, replica_groups={{0,8,16,24},{32,40,48,56},{64,72,80,88},{96,104,112,120},{128,136,144,1..., dimensions={0} | all-to-all | bytes 720896 | tf_op jit(solution)/shard_map/all_to_all | solution.py:25
  18.6 0.0 all-gather.2.cloned.1.call-update
  18.6 0.7 slice.68
  19.3 0.7 slice.69
  20.0 0.7 add_convert_fusion.3
  20.7 0.1 broadcast_in_dim.18
  20.8 2.2 collective-permute-start
  23.0 0.9 copy_bitcast_fusion.1
  24.0 0.0 copy-done.8
  24.0 0.1 reshape.153
  24.1 0.2 collective-permute-done
  24.4 0.1 add_reduce_fusion
  24.5 0.0 copy-done.10
  24.6 0.2 compare_and_fusion
  24.8 0.4 fusion.40
  25.2 0.1 broadcast_maximum_fusion
  25.2 0.2 fusion.8
  25.4 0.1 exponential_add_fusion
  25.5 0.3 fusion.7
  25.8 0.1 copy.38
  25.9 0.5 convolution_convert_fusion
  26.4 8.9 %collective-permute-start.1 = (bf16[256,2048]{1,0:T(8,128)(2,1)S(1)}, bf16[256,2048]{1,0:T(8,128)(2,1)S(1)}, u32[]{:S(2)}, u32[]{:S(2)}) collective-permute-start(bf16[256,2048]{1,0:T(8,128)(2,1)S(1)} %convolution_convert_fusion), channel_id=1, source_target_pairs={{0,1},{1,0},{2,3},{3,2},{4,5},{5,4},{6,7},{7,6},{8,9},{9,8},{10,11... | collective-permute-start | bytes 3145736 | tf_op jit(solution)/shard_map/ppermute | solution.py:21
  35.3 2.3 %collective-permute-done.1 = bf16[256,2048]{1,0:T(8,128)(2,1)S(1)} collective-permute-done((bf16[256,2048]{1,0:T(8,128)(2,1)S(1)}, bf16[256,2048]{1,0:T(8,128)(2,1)S(1)}, u32[]{:S(2)}, u32[]{:S(2)}) %collective-permute-start.1) | collective-permute-done | bytes 1048608 | tf_op jit(solution)/shard_map/ppermute | solution.py:21
  37.6 1.4 add_convert_fusion.1
  39.0 3.6 %all-to-all-start = ((bf16[4,64,2048]{2,1,0:T(8,128)(2,1)}), bf16[4,64,2048]{2,1,0:T(8,128)(2,1)S(1)}, u32[]{:S(2)}, u32[]{:S(2)}) async-start(bf16[4,64,2048]{2,1,0:T(8,128)(2,1)} %bitcast.11), calls=%async_computation | async-start | bytes 2097152 | tf_op jit(solution)/shard_map/all_to_all | solution.py:25
  42.7 14.8 %all-to-all-done = bf16[4,64,2048]{2,1,0:T(8,128)(2,1)S(1)} async-done(((bf16[4,64,2048]{2,1,0:T(8,128)(2,1)}), bf16[4,64,2048]{2,1,0:T(8,128)(2,1)S(1)}, u32[]{:S(2)}, u32[]{:S(2)}) %all-to-all-start) | async-done | bytes 1048608 | tf_op jit(solution)/shard_map/all_to_all | solution.py:25
  57.5 0.2 convert_reduce_fusion.1
  57.7 1.1 fusion.9
  58.8 0.0 copy-start.2
  58.8 0.0 copy-start.9
  58.8 0.7 copy-done.2
  59.5 0.0 copy-done.11
  59.5 0.1 fusion.11
  59.6 1.1 broadcast_in_dim.25
  60.7 3.5 %all-to-all-start.1 = ((bf16[4,64,2048]{2,1,0:T(8,128)(2,1)}), bf16[4,64,2048]{2,1,0:T(8,128)(2,1)S(1)}, u32[]{:S(2)}, u32[]{:S(2)}) async-start(bf16[4,64,2048]{2,1,0:T(8,128)(2,1)} %broadcast_in_dim.25), calls=%async_computation.1 | async-start | bytes 2097152 | tf_op jit(solution)/shard_map/all_to_all | solution.py:25
  64.3 44.7 %all_gather.7 = bf16[512,704]{1,0:T(8,128)(2,1)S(1)} all-gather(bf16[32,704]{1,0:T(8,128)(2,1)S(1)} %bitcast.84), channel_id=1, replica_groups={{0,32,64,96,128,160,192,224,256,288,320,352,384,416,448,480},{8,40,72,1..., dimensions={0}, use_global_device_ids=true | all-gather | bytes 765952 | tf_op jit(solution)/shard_map/all_gather | solution.py:112
  108.9 0.3 copy.39
  109.2 0.0 all-to-all-done.1
  109.2 0.0 copy-start.4
  109.2 2.0 broadcast_in_dim.27
  111.2 0.0 copy-done.4
  111.2 3.7 %all-to-all-start.3 = ((bf16[4,512,704]{1,2,0:T(8,128)(2,1)}), bf16[4,512,704]{1,2,0:T(8,128)(2,1)S(1)}, u32[]{:S(2)}, u32[]{:S(2)}) async-start(bf16[4,512,704]{1,2,0:T(8,128)(2,1)} %broadcast_in_dim.27), calls=%async_computation.3 | async-start | bytes 5767168 | tf_op jit(solution)/shard_map/all_to_all | solution.py:25
  114.9 7.4 %collective-permute-start.2 = (bf16[256,2048]{1,0:T(8,128)(2,1)}, bf16[256,2048]{1,0:T(8,128)(2,1)}, u32[]{:S(2)}, u32[]{:S(2)}) collective-permute-start(bf16[256,2048]{1,0:T(8,128)(2,1)} %bitcast.76), channel_id=1, source_target_pairs={{0,1},{1,0},{2,3},{3,2},{4,5},{5,4},{6,7},{7,6},{8,9},{9,8},{10,11... | collective-permute-start | bytes 3145736 | tf_op jit(solution)/shard_map/ppermute | solution.py:21
  122.3 21.9 %all-to-all-done.3 = bf16[4,512,704]{1,2,0:T(8,128)(2,1)S(1)} async-done(((bf16[4,512,704]{1,2,0:T(8,128)(2,1)}), bf16[4,512,704]{1,2,0:T(8,128)(2,1)S(1)}, u32[]{:S(2)}, u32[]{:S(2)}) %all-to-all-start.3) | async-done | bytes 2883616 | tf_op jit(solution)/shard_map/all_to_all | solution.py:25
  144.2 2.8 %copy.40 = bf16[4,512,704]{2,1,0:T(8,128)(2,1)} copy(bf16[4,512,704]{1,2,0:T(8,128)(2,1)S(1)} %all-to-all-done.3) | data formatting | bytes 5767168 | tf_op jit(solution)/shard_map/all_to_all | solution.py:25
  147.0 4.0 %copy.41 = bf16[16,4,32,704]{3,2,1,0:T(8,128)(2,1)} copy(bf16[16,4,32,704]{3,2,0,1:T(8,128)(2,1)} %bitcast.70) | data formatting | bytes 5767168 | tf_op jit(solution)/shard_map/transpose | solution.py:114
  150.9 0.0 collective-permute-done.2
  151.0 6.0 %fusion = f32[512,1408]{1,0:T(8,128)S(1)} fusion(bf16[2048,1408]{1,0:T(8,128)(2,1)} %all-gather.2.cloned.1.call-done, bf16[256,2048]{1,0:T(8,128)(2,1)} %collective-permute-done.2, bf16[256,2048]{1,0:T(8,128)(2,1)S(1)} %bitcast.77), kind=kOutput, calls=%fused_computation.2 | convolution fusion | flops 2956984320 | bytes 10747904 | tf_op jit(solution)/shard_map/dot_general | solution.py:129
  157.0 0.5 fusion.4
  157.5 1.4 copy-done.1
  158.9 1.1 convolution_convert_fusion.1
  160.0 8.3 %collective-permute-start.3 = (bf16[256,2048]{1,0:T(8,128)(2,1)S(1)}, bf16[256,2048]{1,0:T(8,128)(2,1)S(1)}, u32[]{:S(2)}, u32[]{:S(2)}) collective-permute-start(bf16[256,2048]{1,0:T(8,128)(2,1)S(1)} %convolution_convert_fusion.1), channel_id=1, source_target_pairs={{0,1},{1,0},{2,3},{3,2},{4,5},{5,4},{6,7},{7,6},{8,9},{9,8},{10,11... | collective-permute-start | bytes 3145736 | tf_op jit(solution)/shard_map/ppermute | solution.py:21
  168.2 2.3 %collective-permute-done.3 = bf16[256,2048]{1,0:T(8,128)(2,1)S(1)} collective-permute-done((bf16[256,2048]{1,0:T(8,128)(2,1)S(1)}, bf16[256,2048]{1,0:T(8,128)(2,1)S(1)}, u32[]{:S(2)}, u32[]{:S(2)}) %collective-permute-start.3) | collective-permute-done | bytes 1048608 | tf_op jit(solution)/shard_map/ppermute | solution.py:21
  170.5 1.1 add_convert_fusion
  171.6 18.8 %all_to_all.31 = bf16[4,64,2048]{2,1,0:T(8,128)(2,1)S(1)} all-to-all(bf16[4,64,2048]{2,1,0:T(8,128)(2,1)S(1)} %bitcast.78), channel_id=1, replica_groups={{0,2,4,6},{1,3,5,7},{8,10,12,14},{9,11,13,15},{16,18,20,22},{17,19,21,2..., dimensions={0} | all-to-all | bytes 2097152 | tf_op jit(solution)/shard_map/all_to_all | solution.py:25
  190.4 0.2 convert_reduce_fusion
  190.6 0.1 broadcast_in_dim.28
  190.7 15.8 %all_to_all.32 = bf16[4,64,2048]{2,1,0:T(8,128)(2,1)S(1)} all-to-all(bf16[4,64,2048]{2,1,0:T(8,128)(2,1)S(1)} %broadcast_in_dim.28), channel_id=1, replica_groups={{0,2,4,6},{1,3,5,7},{8,10,12,14},{9,11,13,15},{16,18,20,22},{17,19,21,2..., dimensions={0} | all-to-all | bytes 2097152 | tf_op jit(solution)/shard_map/all_to_all | solution.py:25
  206.6 4.5 %collective-permute-start.4 = (bf16[256,2048]{1,0:T(8,128)(2,1)S(1)}, bf16[256,2048]{1,0:T(8,128)(2,1)S(1)}, u32[]{:S(2)}, u32[]{:S(2)}) collective-permute-start(bf16[256,2048]{1,0:T(8,128)(2,1)S(1)} %bitcast.71), channel_id=1, source_target_pairs={{0,1},{1,0},{2,3},{3,2},{4,5},{5,4},{6,7},{7,6},{8,9},{9,8},{10,11... | collective-permute-start | bytes 3145736 | tf_op jit(solution)/shard_map/ppermute | solution.py:21
  211.1 2.3 %collective-permute-done.4 = bf16[256,2048]{1,0:T(8,128)(2,1)S(1)} collective-permute-done((bf16[256,2048]{1,0:T(8,128)(2,1)S(1)}, bf16[256,2048]{1,0:T(8,128)(2,1)S(1)}, u32[]{:S(2)}, u32[]{:S(2)}) %collective-permute-start.4) | collective-permute-done | bytes 1048608 | tf_op jit(solution)/shard_map/ppermute | solution.py:21
  213.4 2.3 %maximum_select_fusion = bf16[512,2048]{1,0:T(8,128)(2,1)} fusion(bf16[256,2048]{1,0:T(8,128)(2,1)S(1)} %collective-permute-done.4, bf16[256,2048]{1,0:T(8,128)(2,1)S(1)} %bitcast.72, pred[]{:T(512)S(6)} %eq.22), kind=kLoop, calls=%fused_computation.6 | loop fusion | flops 9437184 | bytes 4194305 | tf_op jit(solution)/shard_map/jit(_where)/select_n | solution.py:141
  (32 shorter events, 0.3 us)
Async XLA Ops:
  6.5 19.4 %copy-start = (bf16[128,2048]{1,0:T(8,128)(2,1)S(1)}, bf16[128,2048]{1,0:T(8,128)(2,1)}, u32[]{:S(2)}) copy-start(bf16[128,2048]{1,0:T(8,128)(2,1)} %param.17) | copy-start | bytes 1572868
  6.5 17.8 %copy-start.6 = (bf16[512,64]{0,1:T(8,128)(2,1)S(1)}, bf16[512,64]{0,1:T(8,128)(2,1)}, u32[]{:S(2)}) copy-start(bf16[512,64]{0,1:T(8,128)(2,1)} %param.12) | copy-start | bytes 196612
  6.5 17.4 %copy-start.7 = (bf16[512,64]{0,1:T(8,128)(2,1)S(1)}, bf16[512,64]{0,1:T(8,128)(2,1)}, u32[]{:S(2)}) copy-start(bf16[512,64]{0,1:T(8,128)(2,1)} %param.13) | copy-start | bytes 196612
  6.5 18.0 %copy-start.10 = (s32[512]{0:T(512)S(1)}, s32[512]{0:T(512)}, u32[]{:S(2)}) copy-start(s32[512]{0:T(512)} %param.14) | copy-start | bytes 6148
  6.5 17.4 %copy-start.8 = (bf16[512,128]{1,0:T(8,128)(2,1)S(1)}, bf16[512,128]{1,0:T(8,128)(2,1)}, u32[]{:S(2)}) copy-start(bf16[512,128]{1,0:T(8,128)(2,1)} %param.11) | copy-start | bytes 393220
  6.5 144.4 %all-gather.2.cloned.1.call-start = ((), (), s32[]{:S(2)}) async-start(), calls=%async_computation.6 | async-start | bytes 6127616 | tf_op jit(solution)/shard_map/all_gather | solution.py:111
  18.6 6.6 %copy-start.12 = (f32[2]{0:T(128)S(1)}, f32[2]{0:T(128)}, u32[]{:S(2)}) copy-start(f32[2]{0:T(128)} %param.15) | copy-start | bytes 28
  20.8 3.5 %collective-permute-start = (bf16[136,128]{0,1:T(8,128)(2,1)S(1)}, bf16[136,128]{0,1:T(8,128)(2,1)S(1)}, u32[]{:S(2)}, u32[]{:S(2)}) collective-permute-start(bf16[136,128]{0,1:T(8,128)(2,1)S(1)} %pad_maximum_fusion.3), channel_id=1, source_target_pairs={{0,8},{8,16},{16,24},{24,32},{32,40},{40,48},{48,56},{56,64},{64,7... | collective-permute-start | bytes 104456 | tf_op jit(solution)/shard_map/ppermute | solution.py:17
  26.4 11.2 %collective-permute-start.1 = (bf16[256,2048]{1,0:T(8,128)(2,1)S(1)}, bf16[256,2048]{1,0:T(8,128)(2,1)S(1)}, u32[]{:S(2)}, u32[]{:S(2)}) collective-permute-start(bf16[256,2048]{1,0:T(8,128)(2,1)S(1)} %convolution_convert_fusion), channel_id=1, source_target_pairs={{0,1},{1,0},{2,3},{3,2},{4,5},{5,4},{6,7},{7,6},{8,9},{9,8},{10,11... | collective-permute-start | bytes 3145736 | tf_op jit(solution)/shard_map/ppermute | solution.py:21
  39.0 20.5 %copy-start.11 = (f32[2048]{0:T(1024)S(1)}, f32[2048]{0:T(1024)}, u32[]{:S(2)}) copy-start(f32[2048]{0:T(1024)} %param.18) | copy-start | bytes 24580
  39.0 18.4 %all-to-all-start = ((bf16[4,64,2048]{2,1,0:T(8,128)(2,1)}), bf16[4,64,2048]{2,1,0:T(8,128)(2,1)S(1)}, u32[]{:S(2)}, u32[]{:S(2)}) async-start(bf16[4,64,2048]{2,1,0:T(8,128)(2,1)} %bitcast.11), calls=%async_computation | async-start | bytes 2097152 | tf_op jit(solution)/shard_map/all_to_all | solution.py:25
  58.8 0.7 copy-start.2
  58.8 5.5 %copy-start.9 = (bf16[704,32]{0,1:T(8,128)(2,1)S(1)}, bf16[704,32]{0,1:T(8,128)(2,1)}, u32[]{:S(2)}) copy-start(bf16[704,32]{0,1:T(8,128)(2,1)} %param.21) | copy-start | bytes 135172
  60.7 48.5 %all-to-all-start.1 = ((bf16[4,64,2048]{2,1,0:T(8,128)(2,1)}), bf16[4,64,2048]{2,1,0:T(8,128)(2,1)S(1)}, u32[]{:S(2)}, u32[]{:S(2)}) async-start(bf16[4,64,2048]{2,1,0:T(8,128)(2,1)} %broadcast_in_dim.25), calls=%async_computation.1 | async-start | bytes 2097152 | tf_op jit(solution)/shard_map/all_to_all | solution.py:25
  109.2 2.0 copy-start.4
  111.2 33.0 %all-to-all-start.3 = ((bf16[4,512,704]{1,2,0:T(8,128)(2,1)}), bf16[4,512,704]{1,2,0:T(8,128)(2,1)S(1)}, u32[]{:S(2)}, u32[]{:S(2)}) async-start(bf16[4,512,704]{1,2,0:T(8,128)(2,1)} %broadcast_in_dim.27), calls=%async_computation.3 | async-start | bytes 5767168 | tf_op jit(solution)/shard_map/all_to_all | solution.py:25
  114.9 36.1 %collective-permute-start.2 = (bf16[256,2048]{1,0:T(8,128)(2,1)}, bf16[256,2048]{1,0:T(8,128)(2,1)}, u32[]{:S(2)}, u32[]{:S(2)}) collective-permute-start(bf16[256,2048]{1,0:T(8,128)(2,1)} %bitcast.76), channel_id=1, source_target_pairs={{0,1},{1,0},{2,3},{3,2},{4,5},{5,4},{6,7},{7,6},{8,9},{9,8},{10,11... | collective-permute-start | bytes 3145736 | tf_op jit(solution)/shard_map/ppermute | solution.py:21
  147.0 4.0 %copy-start.5 = (bf16[4,64,2048]{2,1,0:T(8,128)(2,1)S(1)}, bf16[4,64,2048]{2,1,0:T(8,128)(2,1)}, u32[]{:S(2)}) copy-start(bf16[4,64,2048]{2,1,0:T(8,128)(2,1)} %copy-done.4) | copy-start | bytes 3145732
  157.0 1.9 copy-start.1
  160.0 10.5 %collective-permute-start.3 = (bf16[256,2048]{1,0:T(8,128)(2,1)S(1)}, bf16[256,2048]{1,0:T(8,128)(2,1)S(1)}, u32[]{:S(2)}, u32[]{:S(2)}) collective-permute-start(bf16[256,2048]{1,0:T(8,128)(2,1)S(1)} %convolution_convert_fusion.1), channel_id=1, source_target_pairs={{0,1},{1,0},{2,3},{3,2},{4,5},{5,4},{6,7},{7,6},{8,9},{9,8},{10,11... | collective-permute-start | bytes 3145736 | tf_op jit(solution)/shard_map/ppermute | solution.py:21
  171.6 19.0 %copy-start.3 = (bf16[64,2048]{1,0:T(8,128)(2,1)S(1)}, bf16[64,2048]{1,0:T(8,128)(2,1)}, u32[]{:S(2)}) copy-start(bf16[64,2048]{1,0:T(8,128)(2,1)} %copy-done.2) | copy-start | bytes 786436
  206.6 6.8 %collective-permute-start.4 = (bf16[256,2048]{1,0:T(8,128)(2,1)S(1)}, bf16[256,2048]{1,0:T(8,128)(2,1)S(1)}, u32[]{:S(2)}, u32[]{:S(2)}) collective-permute-start(bf16[256,2048]{1,0:T(8,128)(2,1)S(1)} %bitcast.71), channel_id=1, source_target_pairs={{0,1},{1,0},{2,3},{3,2},{4,5},{5,4},{6,7},{7,6},{8,9},{9,8},{10,11... | collective-permute-start | bytes 3145736 | tf_op jit(solution)/shard_map/ppermute | solution.py:21
Sparse Core Ops, SparseCore 0:
  18.7 89.7 all-gather.1

commit v2 on v1

--- a/solution.py
+++ b/solution.py
@@ -27,6 +27,21 @@
 
 def copies(shard, axis, groups):
     return swapped(jnp.broadcast_to(shard[None], (len(groups[0]), *shard.shape)), axis, groups)
+
+
+def chip_away(shard, by):
+    pairs = [(2 * x + c, 2 * ((x + by) % NX) + c) for x in range(NX) for c in range(2)]
+    return lax.ppermute(shard, "tp", pairs)
+
+
+def all_chips_rows(shard, chip):
+    share = shard.shape[0]
+    rows = jnp.zeros((NX * share, shard.shape[1]), shard.dtype)
+    rows = lax.dynamic_update_slice_in_dim(rows, shard, chip * share, 0)
+    for by in (1, 3, 2):
+        sender = lax.rem(chip - by + NX, NX)
+        rows = lax.dynamic_update_slice_in_dim(rows, chip_away(shard, by), sender * share, 0)
+    return rows
 
 
 def rms_norm(stream, norm_gain):
@@ -80,11 +95,13 @@
     return attended.astype(jnp.bfloat16).reshape(local_rows, queries.shape[1])
 
 
-def sum_at_owner(theirs, mine):
+def pair_sum_of(theirs, mine):
     arrived = other_core(theirs)
-    pair_sum = (mine + arrived.astype(jnp.float32)).astype(jnp.bfloat16)
-    pieces = swapped(pair_sum.reshape(NX, -1, pair_sum.shape[1]), "tp", FAR_X)
-    return pieces.astype(jnp.float32).sum(axis=0)
+    return (mine + arrived.astype(jnp.float32)).astype(jnp.bfloat16)
+
+
+def to_owners(pair_sum):
+    return swapped(pair_sum.reshape(NX, -1, pair_sum.shape[1]), "tp", FAR_X)
 
 
 def on_device(
@@ -109,32 +126,39 @@
     near = copies(jnp.concatenate([w_gate, w_up], axis=1), "sp", FAR_Y)
     near = near.reshape(-1, 2 * ff)
     gate_up = lax.all_gather(near, "sp", axis=0, tiled=True, axis_index_groups=FAR_Z)
-    column = lax.all_gather(w_down.T, "sp", axis=0, tiled=True, axis_index_groups=FAR_Z)
-    down = copies(column, "sp", FAR_Y)
-    down = jnp.swapaxes(down.reshape(NY, NZ, -1, ff), 0, 1).reshape(width, ff)
-
     attended = attend(queries, key_rows, values, doc_ids, sink_logits)
     at_mine = lax.dynamic_slice_in_dim(attended, core * half, half, 0)
     at_theirs = lax.dynamic_slice_in_dim(attended, (1 - core) * half, half, 0)
-    mixed_sum = sum_at_owner(
+    pair_sum = pair_sum_of(
         jnp.dot(at_theirs, out_weight, preferred_element_type=jnp.float32).astype(jnp.bfloat16),
         jnp.dot(at_mine, out_weight, preferred_element_type=jnp.float32),
     )
+    pieces = to_owners(pair_sum)
+    padded = -(-ff // 256) * 256
+    turned, _ = lax.optimization_barrier((w_down.T, pair_sum))
+    turned = jnp.pad(turned, ((0, 0), (0, padded - ff)))
+    column = lax.all_gather(turned, "sp", axis=0, tiled=True, axis_index_groups=FAR_Z)
+    column, pieces = lax.optimization_barrier((column, pieces))
+    down = copies(column, "sp", FAR_Y)
+    down = jnp.swapaxes(down.reshape(NY, NZ, -1, padded), 0, 1).reshape(width, padded)
+    mixed_sum = pieces.astype(jnp.float32).sum(axis=0)
     base_rows = lax.dynamic_slice_in_dim(residual, core * half + chip * share, share, 0)
     stream = (base_rows.astype(jnp.float32) + mixed_sum).astype(jnp.bfloat16)
     normed = rms_norm(stream, norm_gain).astype(jnp.bfloat16)
-    normed = copies(normed, "tp", FAR_X).reshape(half, width)
+    normed = all_chips_rows(normed, chip)
     normed = jnp.concatenate([normed, other_core(normed)], axis=0)
 
     acts = jnp.dot(normed, gate_up, preferred_element_type=jnp.float32)
     hidden = (jax.nn.silu(acts[:, :ff]) * acts[:, ff:]).astype(jnp.bfloat16)
+    hidden = jnp.pad(hidden, ((0, 0), (0, padded - ff)))
 
     def through(part):
         return lax.dot_general(
             part, down, (((1,), (1,)), ((), ())), preferred_element_type=jnp.float32
         )
 
-    mlp_total = sum_at_owner(through(hidden[half:]).astype(jnp.bfloat16), through(hidden[:half]))
+    pair_sum = pair_sum_of(through(hidden[half:]).astype(jnp.bfloat16), through(hidden[:half]))
+    mlp_total = to_owners(pair_sum).astype(jnp.float32).sum(axis=0)
     finished = (stream.astype(jnp.float32) + mlp_total).astype(jnp.bfloat16)
     mine = copies(finished, "tp", FAR_X).reshape(half, width)
     theirs = other_core(mine)

time: 223 us -> 203 us (0.910)
  waiting for transfers between devices: 43.7 us -> 21.6 us
  starting transfers between devices: 42.2 us -> 48 us
  local copies, waits for them, and re-layouts: 15 us -> 10.2 us
    all_to_all x3 -> x2, waiting for transfers between devices: 36.7 us -> 6.93 us  [swapped(): lax.all_to_all(pieces, axis, 0, 0, tiled=True, axis_index_groups=groups)]
    ppermute x0 -> x3, starting transfers between devices: none -> 10.6 us  [chip_away(): return lax.ppermute(shard, 'tp', pairs)]
    ppermute x0 -> x3, waiting for transfers between devices: none -> 7.68 us  [chip_away(): return lax.ppermute(shard, 'tp', pairs)]
    all_to_all x1 -> x0, local copies, waits for them, and re-layouts: 2.79 us -> none  [swapped(): lax.all_to_all(pieces, axis, 0, 0, tiled=True, axis_index_groups=groups)]
    all_to_all x3 -> x2, starting transfers between devices: 10.8 us -> 8.2 us  [swapped(): lax.all_to_all(pieces, axis, 0, 0, tiled=True, axis_index_groups=groups)]
  transfers between devices with their start and end apart: 9 -> 11, of which waited for: 6 -> 7; matrix products, arithmetic and copies ran while one was open for 8% -> 7% of each run, Pallas kernels for 0% -> 0%
where the time goes in v2:
time: 203 us; the launch traced here: 202 us
  blocking collectives  90.8 us (45%)
  starting transfers between devices  48 us (24%)
  waiting for transfers between devices  21.6 us (11%)
  between operations  13.9 us (7%)
  matrix products  10.3 us (5%)
  local copies, waits for them, and re-layouts  10.2 us (5%)
  other arithmetic  6.82 us (3%)
    all_to_all x3, blocking collectives, swapped(): lax.all_to_all(pieces, axis, 0, 0, tiled=True, axis_index_groups=groups)  45.5 us
    all_gather x1, blocking collectives, on_device(): lax.all_gather(turned, 'sp', axis=0, tiled=True, axis_index_groups=FAR_Z)  45.4 us
    ppermute x4, starting transfers between devices, other_core(): return lax.ppermute(shard, 'tp', [(i, i ^ 1) for i in range(2 * NX)])  27 us
    ppermute x3, starting transfers between devices, chip_away(): return lax.ppermute(shard, 'tp', pairs)  10.6 us
    all_to_all x2, starting transfers between devices, swapped(): lax.all_to_all(pieces, axis, 0, 0, tiled=True, axis_index_groups=groups)  8.2 us
    ppermute x3, waiting for transfers between devices, chip_away(): return lax.ppermute(shard, 'tp', pairs)  7.68 us
    all_to_all x2, waiting for transfers between devices, swapped(): lax.all_to_all(pieces, axis, 0, 0, tiled=True, axis_index_groups=groups)  6.93 us
    ppermute x4, waiting for transfers between devices, other_core(): return lax.ppermute(shard, 'tp', [(i, i ^ 1) for i in range(2 * NX)])  6.77 us
  transfers between devices with their start and end apart: 11, of which 7 were waited for; matrix products, arithmetic and copies ran while one was open for 7% of the time, Pallas kernels for 0%

profile of v2, /device:TPU:1, one launch (start us, length us, event | category | flops | bytes accessed | tf_op | source)
XLA Modules:
  0.0 201.7 jit_solution(4640326983382402729)
XLA Ops:
  6.5 0.0 copy-start
  6.5 0.0 all-gather.2.cloned.1.call-start
  6.6 1.0 pad_maximum_fusion
  7.6 11.0 %all_to_all.25 = bf16[4,32,1408]{2,1,0:T(8,128)(2,1)} all-to-all(bf16[4,32,1408]{2,1,0:T(8,128)(2,1)S(1)} %broadcast_in_dim.26), channel_id=1, replica_groups={{0,8,16,24},{32,40,48,56},{64,72,80,88},{96,104,112,120},{128,136,144,1..., dimensions={0} | all-to-all | bytes 720896 | tf_op jit(solution)/shard_map/all_to_all | solution.py:25
  18.6 0.0 all-gather.2.cloned.1.call-update
  18.6 0.7 slice.68
  19.3 0.7 slice.69
  20.0 0.7 add_convert_fusion.3
  20.7 0.1 broadcast_in_dim.22
  20.8 2.2 %collective-permute-start = (bf16[136,128]{0,1:T(8,128)(2,1)S(1)}, bf16[136,128]{0,1:T(8,128)(2,1)S(1)}, u32[]{:S(2)}, u32[]{:S(2)}) collective-permute-start(bf16[136,128]{0,1:T(8,128)(2,1)S(1)} %pad_maximum_fusion.3), channel_id=1, source_target_pairs={{0,8},{8,16},{16,24},{24,32},{32,40},{40,48},{48,56},{56,64},{64,7... | collective-permute-start | bytes 104456 | tf_op jit(solution)/shard_map/ppermute | solution.py:17
  23.0 0.9 copy_bitcast_fusion.1
  23.9 0.0 copy-done.3
  24.0 0.1 reshape.148
  24.1 0.2 collective-permute-done
  24.4 0.1 add_reduce_fusion
  24.6 0.2 compare_and_fusion
  24.8 0.4 fusion.39
  25.1 0.0 copy-done.8
  25.2 0.1 broadcast_maximum_fusion
  25.2 0.2 fusion.8
  25.4 0.1 exponential_add_fusion
  25.5 0.3 fusion.7
  25.8 0.1 copy.29
  25.9 0.5 convolution_convert_fusion
  26.4 8.9 %collective-permute-start.1 = (bf16[256,2048]{1,0:T(8,128)(2,1)S(1)}, bf16[256,2048]{1,0:T(8,128)(2,1)S(1)}, u32[]{:S(2)}, u32[]{:S(2)}) collective-permute-start(bf16[256,2048]{1,0:T(8,128)(2,1)S(1)} %convolution_convert_fusion), channel_id=1, source_target_pairs={{0,1},{1,0},{2,3},{3,2},{4,5},{5,4},{6,7},{7,6},{8,9},{9,8},{10,11... | collective-permute-start | bytes 3145736 | tf_op jit(solution)/shard_map/ppermute | solution.py:21
  35.3 0.0 copy-start.5
  35.4 2.2 %collective-permute-done.1 = bf16[256,2048]{1,0:T(8,128)(2,1)S(1)} collective-permute-done((bf16[256,2048]{1,0:T(8,128)(2,1)S(1)}, bf16[256,2048]{1,0:T(8,128)(2,1)S(1)}, u32[]{:S(2)}, u32[]{:S(2)}) %collective-permute-start.1) | collective-permute-done | bytes 1048608 | tf_op jit(solution)/shard_map/ppermute | solution.py:21
  37.6 1.4 add_convert_fusion.1
  39.0 3.5 %all-to-all-start = ((bf16[4,64,2048]{2,1,0:T(8,128)(2,1)}), bf16[4,64,2048]{2,1,0:T(8,128)(2,1)S(1)}, u32[]{:S(2)}, u32[]{:S(2)}) async-start(bf16[4,64,2048]{2,1,0:T(8,128)(2,1)} %bitcast.12), calls=%async_computation | async-start | bytes 2097152 | tf_op jit(solution)/shard_map/all_to_all | solution.py:25
  42.6 0.0 copy-done.5
  42.6 45.4 %all_gather.6 = bf16[512,768]{1,0:T(8,128)(2,1)S(1)} all-gather(bf16[32,768]{1,0:T(8,128)(2,1)S(1)} %pad.8), channel_id=1, replica_groups={{0,32,64,96,128,160,192,224,256,288,320,352,384,416,448,480},{8,40,72,1..., dimensions={0}, use_global_device_ids=true | all-gather | bytes 835584 | tf_op jit(solution)/shard_map/all_gather | solution.py:140
  88.0 0.0 all-to-all-done
  88.0 1.9 broadcast_in_dim.27
  89.9 4.7 %all-to-all-start.2 = ((bf16[4,512,768]{2,1,0:T(8,128)(2,1)}), bf16[4,512,768]{2,1,0:T(8,128)(2,1)}, u32[]{:S(2)}, u32[]{:S(2)}) async-start(bf16[4,512,768]{2,1,0:T(8,128)(2,1)} %broadcast_in_dim.27), calls=%async_computation.2 | async-start | bytes 6291456 | tf_op jit(solution)/shard_map/all_to_all | solution.py:25
  94.6 0.0 copy-start.7
  94.6 0.2 convert_reduce_fusion.1
  94.8 1.1 fusion.9
  95.9 0.1 broadcast_in_dim.25
  96.1 0.1 constant_dynamic-update-slice_fusion.3
  96.2 3.8 %collective-permute-start.2 = (bf16[64,2048]{1,0:T(8,128)(2,1)S(1)}, bf16[64,2048]{1,0:T(8,128)(2,1)S(1)}, u32[]{:S(2)}, u32[]{:S(2)}) collective-permute-start(bf16[64,2048]{1,0:T(8,128)(2,1)S(1)} %get-tuple-element.12), channel_id=1, source_target_pairs={{0,2},{1,3},{2,4},{3,5},{4,6},{5,7},{6,0},{7,1},{8,10},{9,11},{10,... | collective-permute-start | bytes 786440 | tf_op jit(solution)/shard_map/ppermute | solution.py:34
  100.0 3.1 %collective-permute-start.3 = (bf16[64,2048]{1,0:T(8,128)(2,1)S(1)}, bf16[64,2048]{1,0:T(8,128)(2,1)S(1)}, u32[]{:S(2)}, u32[]{:S(2)}) collective-permute-start(bf16[64,2048]{1,0:T(8,128)(2,1)S(1)} %get-tuple-element.12), channel_id=1, source_target_pairs={{0,6},{1,7},{2,0},{3,1},{4,2},{5,3},{6,4},{7,5},{8,14},{9,15},{10,... | collective-permute-start | bytes 786440 | tf_op jit(solution)/shard_map/ppermute | solution.py:34
  103.2 3.6 %collective-permute-start.4 = (bf16[64,2048]{1,0:T(8,128)(2,1)S(1)}, bf16[64,2048]{1,0:T(8,128)(2,1)S(1)}, u32[]{:S(2)}, u32[]{:S(2)}) collective-permute-start(bf16[64,2048]{1,0:T(8,128)(2,1)S(1)} %get-tuple-element.12), channel_id=1, source_target_pairs={{0,4},{1,5},{2,6},{3,7},{4,0},{5,1},{6,2},{7,3},{8,12},{9,13},{10,... | collective-permute-start | bytes 786440 | tf_op jit(solution)/shard_map/ppermute | solution.py:34
  106.8 0.0 collective-permute-done.2
  106.9 0.6 collective-permute-done.3
  107.5 7.0 %collective-permute-done.4 = bf16[64,2048]{1,0:T(8,128)(2,1)S(1)} collective-permute-done((bf16[64,2048]{1,0:T(8,128)(2,1)S(1)}, bf16[64,2048]{1,0:T(8,128)(2,1)S(1)}, u32[]{:S(2)}, u32[]{:S(2)}) %collective-permute-start.4) | collective-permute-done | bytes 262176 | tf_op jit(solution)/shard_map/ppermute | solution.py:34
  114.6 5.8 %collective-permute-start.5 = (bf16[256,2048]{1,0:T(8,128)(2,1)S(1)}, bf16[256,2048]{1,0:T(8,128)(2,1)S(1)}, u32[]{:S(2)}, u32[]{:S(2)}) collective-permute-start(bf16[256,2048]{1,0:T(8,128)(2,1)S(1)} %constant_dynamic-update-slice_fusion), channel_id=1, source_target_pairs={{0,1},{1,0},{2,3},{3,2},{4,5},{5,4},{6,7},{7,6},{8,9},{9,8},{10,11... | collective-permute-start | bytes 3145736 | tf_op jit(solution)/shard_map/ppermute | solution.py:21
  120.4 6.9 %all-to-all-done.2 = bf16[4,512,768]{2,1,0:T(8,128)(2,1)} async-done(((bf16[4,512,768]{2,1,0:T(8,128)(2,1)}), bf16[4,512,768]{2,1,0:T(8,128)(2,1)}, u32[]{:S(2)}, u32[]{:S(2)}) %all-to-all-start.2) | async-done | bytes 3145760 | tf_op jit(solution)/shard_map/all_to_all | solution.py:25
  127.3 3.9 %copy.30 = bf16[16,4,32,768]{3,2,1,0:T(8,128)(2,1)} copy(bf16[16,4,32,768]{3,2,0,1:T(8,128)(2,1)} %bitcast.15) | data formatting | bytes 6291456 | tf_op jit(solution)/shard_map/transpose | solution.py:143
  131.2 0.0 collective-permute-done.5
  131.2 5.7 %fusion = f32[512,1408]{1,0:T(8,128)S(1)} fusion(bf16[2048,1408]{1,0:T(8,128)(2,1)} %all-gather.2.cloned.1.call-done, bf16[256,2048]{1,0:T(8,128)(2,1)S(1)} %collective-permute-done.5, bf16[256,2048]{1,0:T(8,128)(2,1)S(1)} %constant_dynamic-update-slice_fusion), kind=kOutput, calls=%fused_computation.2 | convolution fusion | flops 2956984320 | bytes 10747904 | tf_op jit(solution)/shard_map/dot_general | solution.py:151
  137.0 0.0 copy-start.1
  137.0 0.5 fusion.4
  137.5 1.4 copy-done.1
  138.9 1.0 convolution_convert_fusion.1
  139.9 7.7 %collective-permute-start.6 = (bf16[256,2048]{1,0:T(8,128)(2,1)S(1)}, bf16[256,2048]{1,0:T(8,128)(2,1)S(1)}, u32[]{:S(2)}, u32[]{:S(2)}) collective-permute-start(bf16[256,2048]{1,0:T(8,128)(2,1)S(1)} %convolution_convert_fusion.1), channel_id=1, source_target_pairs={{0,1},{1,0},{2,3},{3,2},{4,5},{5,4},{6,7},{7,6},{8,9},{9,8},{10,11... | collective-permute-start | bytes 3145736 | tf_op jit(solution)/shard_map/ppermute | solution.py:21
  147.6 2.3 %collective-permute-done.6 = bf16[256,2048]{1,0:T(8,128)(2,1)S(1)} collective-permute-done((bf16[256,2048]{1,0:T(8,128)(2,1)S(1)}, bf16[256,2048]{1,0:T(8,128)(2,1)S(1)}, u32[]{:S(2)}, u32[]{:S(2)}) %collective-permute-start.6) | collective-permute-done | bytes 1048608 | tf_op jit(solution)/shard_map/ppermute | solution.py:21
  149.9 1.0 add_convert_fusion
  150.9 18.7 %all_to_all.26 = bf16[4,64,2048]{2,1,0:T(8,128)(2,1)S(1)} all-to-all(bf16[4,64,2048]{2,1,0:T(8,128)(2,1)S(1)} %bitcast.73), channel_id=1, replica_groups={{0,2,4,6},{1,3,5,7},{8,10,12,14},{9,11,13,15},{16,18,20,22},{17,19,21,2..., dimensions={0} | all-to-all | bytes 2097152 | tf_op jit(solution)/shard_map/all_to_all | solution.py:25
  169.6 0.2 convert_reduce_fusion
  169.8 0.1 broadcast_in_dim.28
  169.9 15.8 %all_to_all.27 = bf16[4,64,2048]{2,1,0:T(8,128)(2,1)S(1)} all-to-all(bf16[4,64,2048]{2,1,0:T(8,128)(2,1)S(1)} %broadcast_in_dim.28), channel_id=1, replica_groups={{0,2,4,6},{1,3,5,7},{8,10,12,14},{9,11,13,15},{16,18,20,22},{17,19,21,2..., dimensions={0} | all-to-all | bytes 2097152 | tf_op jit(solution)/shard_map/all_to_all | solution.py:25
  185.7 4.6 %collective-permute-start.7 = (bf16[256,2048]{1,0:T(8,128)(2,1)S(1)}, bf16[256,2048]{1,0:T(8,128)(2,1)S(1)}, u32[]{:S(2)}, u32[]{:S(2)}) collective-permute-start(bf16[256,2048]{1,0:T(8,128)(2,1)S(1)} %bitcast.71), channel_id=1, source_target_pairs={{0,1},{1,0},{2,3},{3,2},{4,5},{5,4},{6,7},{7,6},{8,9},{9,8},{10,11... | collective-permute-start | bytes 3145736 | tf_op jit(solution)/shard_map/ppermute | solution.py:21
  190.3 2.3 %collective-permute-done.7 = bf16[256,2048]{1,0:T(8,128)(2,1)S(1)} collective-permute-done((bf16[256,2048]{1,0:T(8,128)(2,1)S(1)}, bf16[256,2048]{1,0:T(8,128)(2,1)S(1)}, u32[]{:S(2)}, u32[]{:S(2)}) %collective-permute-start.7) | collective-permute-done | bytes 1048608 | tf_op jit(solution)/shard_map/ppermute | solution.py:21
  192.6 2.3 %maximum_select_fusion = bf16[512,2048]{1,0:T(8,128)(2,1)} fusion(bf16[256,2048]{1,0:T(8,128)(2,1)S(1)} %collective-permute-done.7, bf16[256,2048]{1,0:T(8,128)(2,1)S(1)} %bitcast.72, pred[]{:T(512)S(6)} %eq.22), kind=kLoop, calls=%fused_computation.6 | loop fusion | flops 9437184 | bytes 4194305 | tf_op jit(solution)/shard_map/jit(_where)/select_n | solution.py:165
  (30 shorter events, 0.3 us)
Async XLA Ops:
  6.5 19.4 %copy-start = (bf16[128,2048]{1,0:T(8,128)(2,1)S(1)}, bf16[128,2048]{1,0:T(8,128)(2,1)}, u32[]{:S(2)}) copy-start(bf16[128,2048]{1,0:T(8,128)(2,1)} %param.17) | copy-start | bytes 1572868
  6.5 17.8 %copy-start.2 = (bf16[512,64]{0,1:T(8,128)(2,1)S(1)}, bf16[512,64]{0,1:T(8,128)(2,1)}, u32[]{:S(2)}) copy-start(bf16[512,64]{0,1:T(8,128)(2,1)} %param.12) | copy-start | bytes 196612
  6.5 17.4 %copy-start.3 = (bf16[512,64]{0,1:T(8,128)(2,1)S(1)}, bf16[512,64]{0,1:T(8,128)(2,1)}, u32[]{:S(2)}) copy-start(bf16[512,64]{0,1:T(8,128)(2,1)} %param.13) | copy-start | bytes 196612
  6.5 18.0 %copy-start.6 = (s32[512]{0:T(512)S(1)}, s32[512]{0:T(512)}, u32[]{:S(2)}) copy-start(s32[512]{0:T(512)} %param.14) | copy-start | bytes 6148
  6.5 17.4 %copy-start.4 = (bf16[512,128]{1,0:T(8,128)(2,1)S(1)}, bf16[512,128]{1,0:T(8,128)(2,1)}, u32[]{:S(2)}) copy-start(bf16[512,128]{1,0:T(8,128)(2,1)} %param.11) | copy-start | bytes 393220
  6.5 124.7 %all-gather.2.cloned.1.call-start = ((), (), s32[]{:S(2)}) async-start(), calls=%async_computation.5 | async-start | bytes 6127616 | tf_op jit(solution)/shard_map/all_gather | solution.py:128
  18.6 6.6 %copy-start.8 = (f32[2]{0:T(128)S(1)}, f32[2]{0:T(128)}, u32[]{:S(2)}) copy-start(f32[2]{0:T(128)} %param.15) | copy-start | bytes 28
  20.8 3.5 %collective-permute-start = (bf16[136,128]{0,1:T(8,128)(2,1)S(1)}, bf16[136,128]{0,1:T(8,128)(2,1)S(1)}, u32[]{:S(2)}, u32[]{:S(2)}) collective-permute-start(bf16[136,128]{0,1:T(8,128)(2,1)S(1)} %pad_maximum_fusion.3), channel_id=1, source_target_pairs={{0,8},{8,16},{16,24},{24,32},{32,40},{40,48},{48,56},{56,64},{64,7... | collective-permute-start | bytes 104456 | tf_op jit(solution)/shard_map/ppermute | solution.py:17
  26.4 11.2 %collective-permute-start.1 = (bf16[256,2048]{1,0:T(8,128)(2,1)S(1)}, bf16[256,2048]{1,0:T(8,128)(2,1)S(1)}, u32[]{:S(2)}, u32[]{:S(2)}) collective-permute-start(bf16[256,2048]{1,0:T(8,128)(2,1)S(1)} %convolution_convert_fusion), channel_id=1, source_target_pairs={{0,1},{1,0},{2,3},{3,2},{4,5},{5,4},{6,7},{7,6},{8,9},{9,8},{10,11... | collective-permute-start | bytes 3145736 | tf_op jit(solution)/shard_map/ppermute | solution.py:21
  35.3 7.2 %copy-start.5 = (bf16[704,32]{0,1:T(8,128)(2,1)S(1)}, bf16[704,32]{0,1:T(8,128)(2,1)}, u32[]{:S(2)}) copy-start(bf16[704,32]{0,1:T(8,128)(2,1)} %param.21) | copy-start | bytes 135172
  39.0 48.9 %all-to-all-start = ((bf16[4,64,2048]{2,1,0:T(8,128)(2,1)}), bf16[4,64,2048]{2,1,0:T(8,128)(2,1)S(1)}, u32[]{:S(2)}, u32[]{:S(2)}) async-start(bf16[4,64,2048]{2,1,0:T(8,128)(2,1)} %bitcast.12), calls=%async_computation | async-start | bytes 2097152 | tf_op jit(solution)/shard_map/all_to_all | solution.py:25
  89.9 37.4 %all-to-all-start.2 = ((bf16[4,512,768]{2,1,0:T(8,128)(2,1)}), bf16[4,512,768]{2,1,0:T(8,128)(2,1)}, u32[]{:S(2)}, u32[]{:S(2)}) async-start(bf16[4,512,768]{2,1,0:T(8,128)(2,1)} %broadcast_in_dim.27), calls=%async_computation.2 | async-start | bytes 6291456 | tf_op jit(solution)/shard_map/all_to_all | solution.py:25
  94.6 1.5 copy-start.7
  96.2 10.6 %collective-permute-start.2 = (bf16[64,2048]{1,0:T(8,128)(2,1)S(1)}, bf16[64,2048]{1,0:T(8,128)(2,1)S(1)}, u32[]{:S(2)}, u32[]{:S(2)}) collective-permute-start(bf16[64,2048]{1,0:T(8,128)(2,1)S(1)} %get-tuple-element.12), channel_id=1, source_target_pairs={{0,2},{1,3},{2,4},{3,5},{4,6},{5,7},{6,0},{7,1},{8,10},{9,11},{10,... | collective-permute-start | bytes 786440 | tf_op jit(solution)/shard_map/ppermute | solution.py:34
  100.0 7.5 %collective-permute-start.3 = (bf16[64,2048]{1,0:T(8,128)(2,1)S(1)}, bf16[64,2048]{1,0:T(8,128)(2,1)S(1)}, u32[]{:S(2)}, u32[]{:S(2)}) collective-permute-start(bf16[64,2048]{1,0:T(8,128)(2,1)S(1)} %get-tuple-element.12), channel_id=1, source_target_pairs={{0,6},{1,7},{2,0},{3,1},{4,2},{5,3},{6,4},{7,5},{8,14},{9,15},{10,... | collective-permute-start | bytes 786440 | tf_op jit(solution)/shard_map/ppermute | solution.py:34
  103.2 11.4 %collective-permute-start.4 = (bf16[64,2048]{1,0:T(8,128)(2,1)S(1)}, bf16[64,2048]{1,0:T(8,128)(2,1)S(1)}, u32[]{:S(2)}, u32[]{:S(2)}) collective-permute-start(bf16[64,2048]{1,0:T(8,128)(2,1)S(1)} %get-tuple-element.12), channel_id=1, source_target_pairs={{0,4},{1,5},{2,6},{3,7},{4,0},{5,1},{6,2},{7,3},{8,12},{9,13},{10,... | collective-permute-start | bytes 786440 | tf_op jit(solution)/shard_map/ppermute | solution.py:34
  114.6 16.6 %collective-permute-start.5 = (bf16[256,2048]{1,0:T(8,128)(2,1)S(1)}, bf16[256,2048]{1,0:T(8,128)(2,1)S(1)}, u32[]{:S(2)}, u32[]{:S(2)}) collective-permute-start(bf16[256,2048]{1,0:T(8,128)(2,1)S(1)} %constant_dynamic-update-slice_fusion), channel_id=1, source_target_pairs={{0,1},{1,0},{2,3},{3,2},{4,5},{5,4},{6,7},{7,6},{8,9},{9,8},{10,11... | collective-permute-start | bytes 3145736 | tf_op jit(solution)/shard_map/ppermute | solution.py:21
  137.0 1.9 copy-start.1
  139.9 10.0 %collective-permute-start.6 = (bf16[256,2048]{1,0:T(8,128)(2,1)S(1)}, bf16[256,2048]{1,0:T(8,128)(2,1)S(1)}, u32[]{:S(2)}, u32[]{:S(2)}) collective-permute-start(bf16[256,2048]{1,0:T(8,128)(2,1)S(1)} %convolution_convert_fusion.1), channel_id=1, source_target_pairs={{0,1},{1,0},{2,3},{3,2},{4,5},{5,4},{6,7},{7,6},{8,9},{9,8},{10,11... | collective-permute-start | bytes 3145736 | tf_op jit(solution)/shard_map/ppermute | solution.py:21
  185.7 6.8 %collective-permute-start.7 = (bf16[256,2048]{1,0:T(8,128)(2,1)S(1)}, bf16[256,2048]{1,0:T(8,128)(2,1)S(1)}, u32[]{:S(2)}, u32[]{:S(2)}) collective-permute-start(bf16[256,2048]{1,0:T(8,128)(2,1)S(1)} %bitcast.71), channel_id=1, source_target_pairs={{0,1},{1,0},{2,3},{3,2},{4,5},{5,4},{6,7},{7,6},{8,9},{9,8},{10,11... | collective-permute-start | bytes 3145736 | tf_op jit(solution)/shard_map/ppermute | solution.py:21
Sparse Core Ops, SparseCore 0:
  18.7 91.1 all-gather.1

commit v3 on v2

--- a/solution.py
+++ b/solution.py
@@ -3,9 +3,11 @@
 from jax import lax
 from jax.sharding import PartitionSpec as P
 
+
 HD = 64
 WINDOW = 128
 NZ, NY, NX = 16, 4, 4
+EARLY = 512
 FAR_Z = [[z * NY + y for z in range(NZ)] for y in range(NY)]
 FAR_Y = [[z * NY + y for y in range(NY)] for z in range(NZ)]
 FAR_X = [[2 * x + c for x in range(NX)] for c in range(2)]
@@ -123,9 +125,11 @@
     chip = lax.div(lax.axis_index("tp"), 2)
     ff = w_gate.shape[1]
 
-    near = copies(jnp.concatenate([w_gate, w_up], axis=1), "sp", FAR_Y)
-    near = near.reshape(-1, 2 * ff)
-    gate_up = lax.all_gather(near, "sp", axis=0, tiled=True, axis_index_groups=FAR_Z)
+    turned = w_down.T
+    near = copies(jnp.concatenate([w_gate, w_up, turned[:, EARLY:]], axis=1), "sp", FAR_Y)
+    near = near.reshape(-1, near.shape[2])
+    far = lax.all_gather(near, "sp", axis=0, tiled=True, axis_index_groups=FAR_Z)
+
     attended = attend(queries, key_rows, values, doc_ids, sink_logits)
     at_mine = lax.dynamic_slice_in_dim(attended, core * half, half, 0)
     at_theirs = lax.dynamic_slice_in_dim(attended, (1 - core) * half, half, 0)
@@ -134,13 +138,12 @@
         jnp.dot(at_mine, out_weight, preferred_element_type=jnp.float32),
     )
     pieces = to_owners(pair_sum)
-    padded = -(-ff // 256) * 256
-    turned, _ = lax.optimization_barrier((w_down.T, pair_sum))
-    turned = jnp.pad(turned, ((0, 0), (0, padded - ff)))
-    column = lax.all_gather(turned, "sp", axis=0, tiled=True, axis_index_groups=FAR_Z)
-    column, pieces = lax.optimization_barrier((column, pieces))
-    down = copies(column, "sp", FAR_Y)
-    down = jnp.swapaxes(down.reshape(NY, NZ, -1, padded), 0, 1).reshape(width, padded)
+    early, _ = lax.optimization_barrier((turned[:, :EARLY], pair_sum))
+    column = lax.all_gather(early, "sp", axis=0, tiled=True, axis_index_groups=FAR_Z)
+    spread = jnp.broadcast_to(column[None], (NY, *column.shape))
+    spread, pieces = lax.optimization_barrier((spread, pieces))
+    down = swapped(spread, "sp", FAR_Y)
+    down = jnp.swapaxes(down.reshape(NY, NZ, -1, EARLY), 0, 1).reshape(width, EARLY)
     mixed_sum = pieces.astype(jnp.float32).sum(axis=0)
     base_rows = lax.dynamic_slice_in_dim(residual, core * half + chip * share, share, 0)
     stream = (base_rows.astype(jnp.float32) + mixed_sum).astype(jnp.bfloat16)
@@ -148,25 +151,27 @@
     normed = all_chips_rows(normed, chip)
     normed = jnp.concatenate([normed, other_core(normed)], axis=0)
 
-    acts = jnp.dot(normed, gate_up, preferred_element_type=jnp.float32)
+    acts = jnp.dot(normed, far[:, : 2 * ff], preferred_element_type=jnp.float32)
     hidden = (jax.nn.silu(acts[:, :ff]) * acts[:, ff:]).astype(jnp.bfloat16)
-    hidden = jnp.pad(hidden, ((0, 0), (0, padded - ff)))
+
+    def turned_dot(left, right):
+        return lax.dot_general(
+            left, right, (((1,), (1,)), ((), ())), preferred_element_type=jnp.float32
+        )
+
+    late = far[:, 2 * ff :]
 
     def through(part):
-        return lax.dot_general(
-            part, down, (((1,), (1,)), ((), ())), preferred_element_type=jnp.float32
-        )
+        return turned_dot(part[:, EARLY:], late) + turned_dot(part[:, :EARLY], down)
 
     pair_sum = pair_sum_of(through(hidden[half:]).astype(jnp.bfloat16), through(hidden[:half]))
     mlp_total = to_owners(pair_sum).astype(jnp.float32).sum(axis=0)
     finished = (stream.astype(jnp.float32) + mlp_total).astype(jnp.bfloat16)
     mine = copies(finished, "tp", FAR_X).reshape(half, width)
     theirs = other_core(mine)
-    return jnp.where(
-        core == 0,
-        jnp.concatenate([mine, theirs], axis=0),
-        jnp.concatenate([theirs, mine], axis=0),
-    )
+    whole = jnp.zeros((rows, width), jnp.bfloat16)
+    whole = lax.dynamic_update_slice_in_dim(whole, mine, core * half, 0)
+    return lax.dynamic_update_slice_in_dim(whole, theirs, (1 - core) * half, 0)
 
 
 def solution(mesh):

time: 203 us -> 196 us (0.966)
  waiting for transfers between devices: 21.6 us -> 16.9 us
  blocking collectives: 90.8 us -> 86.2 us
  matrix products: 10.3 us -> 13.9 us
  other arithmetic: 6.82 us -> 3.66 us
  local copies, waits for them, and re-layouts: 10.2 us -> 12.5 us
    ppermute x3, waiting for transfers between devices: 7.68 us -> 2.96 us  [chip_away(): return lax.ppermute(shard, 'tp', pairs)]
    dot_general x3 -> x5, matrix products: 7.74 us -> 11.3 us  [the longest x1 6.39 us: on_device(): acts = jnp.dot(normed, far[:, :2 * ff], preferred_element_type=jnp.float32)]
    all_gather x1, blocking collectives: 45.4 us -> 41.9 us  [on_device(): lax.all_gather(early, 'sp', axis=0, tiled=True, axis_index_groups=FAR_Z)]
    dynamic_update_slice x3, local copies, waits for them, and re-layouts: 0.06 us -> 3.1 us  [all_chips_rows(): lax.dynamic_update_slice_in_dim(rows, chip_away(shard, by), sender * shar...]
    select_n x1 -> x0, other arithmetic: 2.32 us -> none  [on_device(): jnp.where(core == 0, jnp.concatenate([mine, theirs], axis=0), jnp.concate...]
    transpose x1, local copies, waits for them, and re-layouts: 3.89 us -> 1.73 us  [on_device(): jnp.swapaxes(down.reshape(NY, NZ, -1, EARLY), 0, 1).reshape(width, EARLY)]
    ppermute x4, waiting for transfers between devices: 6.77 us -> 4.68 us  [other_core(): return lax.ppermute(shard, 'tp', [(i, i ^ 1) for i in range(2 * NX)])]
  transfers between devices with their start and end apart: 11 -> 11, of which waited for: 7 -> 6; matrix products, arithmetic and copies ran while one was open for 7% -> 8% of each run, Pallas kernels for 0% -> 0%
where the time goes in v3:
time: 196 us; the launch traced here: 195 us
  blocking collectives  86.2 us (44%)
  starting transfers between devices  48.1 us (25%)
  waiting for transfers between devices  16.9 us (9%)
  between operations  14 us (7%)
  matrix products  13.9 us (7%)
  local copies, waits for them, and re-layouts  12.5 us (6%)
  other arithmetic  3.66 us (2%)
    all_to_all x3, blocking collectives, swapped(): lax.all_to_all(pieces, axis, 0, 0, tiled=True, axis_index_groups=groups)  44.3 us
    all_gather x1, blocking collectives, on_device(): lax.all_gather(early, 'sp', axis=0, tiled=True, axis_index_groups=FAR_Z)  41.9 us
    ppermute x4, starting transfers between devices, other_core(): return lax.ppermute(shard, 'tp', [(i, i ^ 1) for i in range(2 * NX)])  28.3 us
    ppermute x3, starting transfers between devices, chip_away(): return lax.ppermute(shard, 'tp', pairs)  10.4 us
    all_to_all x2, waiting for transfers between devices, swapped(): lax.all_to_all(pieces, axis, 0, 0, tiled=True, axis_index_groups=groups)  8.18 us
    all_to_all x2, starting transfers between devices, swapped(): lax.all_to_all(pieces, axis, 0, 0, tiled=True, axis_index_groups=groups)  7.14 us
    dot_general x1, matrix products, on_device(): acts = jnp.dot(normed, far[:, :2 * ff], preferred_element_type=jnp.float32)  6.39 us
    dot_general x4, matrix products, turned_dot(): lax.dot_general(left, right, (((1,), (1,)), ((), ())), preferred_element_...  4.93 us
  transfers between devices with their start and end apart: 11, of which 6 were waited for; matrix products, arithmetic and copies ran while one was open for 8% of the time, Pallas kernels for 0%

profile of v3, /device:TPU:1, one launch (start us, length us, event | category | flops | bytes accessed | tf_op | source)
XLA Modules:
  0.0 195.2 jit_solution(14286051599491315051)
XLA Ops:
  6.6 0.0 all-gather.2.cloned.1.call-start
  6.6 0.8 slice.120
  7.4 0.9 concatenate.39
  8.4 11.3 %all_to_all.25 = bf16[4,32,1600]{2,1,0:T(8,128)(2,1)} all-to-all(bf16[4,32,1600]{2,1,0:T(8,128)(2,1)S(1)} %broadcast_in_dim.30), channel_id=1, replica_groups={{0,8,16,24},{32,40,48,56},{64,72,80,88},{96,104,112,120},{128,136,144,1..., dimensions={0} | all-to-all | bytes 819200 | tf_op jit(solution)/shard_map/all_to_all | solution.py:27
  19.7 0.0 all-gather.2.cloned.1.call-update
  19.8 0.1 broadcast_in_dim.25
  19.9 2.2 %collective-permute-start = (bf16[136,128]{0,1:T(8,128)(2,1)S(1)}, bf16[136,128]{0,1:T(8,128)(2,1)S(1)}, u32[]{:S(2)}, u32[]{:S(2)}) collective-permute-start(bf16[136,128]{0,1:T(8,128)(2,1)S(1)} %pad_maximum_fusion.2), channel_id=1, source_target_pairs={{0,8},{8,16},{16,24},{24,32},{32,40},{40,48},{48,56},{56,64},{64,7... | collective-permute-start | bytes 104456 | tf_op jit(solution)/shard_map/ppermute | solution.py:19
  22.2 0.1 reshape.148
  22.4 1.0 collective-permute-done
  23.5 0.1 add_reduce_fusion
  23.6 0.2 compare_and_fusion
  23.8 0.4 fusion.48
  24.2 0.1 broadcast_maximum_fusion
  24.3 0.2 fusion.10
  24.4 0.1 exponential_add_fusion
  24.5 0.3 fusion.9
  24.8 0.1 copy.29
  25.0 0.5 convolution_convert_fusion
  25.5 8.9 %collective-permute-start.1 = (bf16[256,2048]{1,0:T(8,128)(2,1)S(1)}, bf16[256,2048]{1,0:T(8,128)(2,1)S(1)}, u32[]{:S(2)}, u32[]{:S(2)}) collective-permute-start(bf16[256,2048]{1,0:T(8,128)(2,1)S(1)} %convolution_convert_fusion), channel_id=1, source_target_pairs={{0,1},{1,0},{2,3},{3,2},{4,5},{5,4},{6,7},{7,6},{8,9},{9,8},{10,11... | collective-permute-start | bytes 3145736 | tf_op jit(solution)/shard_map/ppermute | solution.py:23
  34.4 0.0 copy-start.6
  34.4 2.2 %collective-permute-done.1 = bf16[256,2048]{1,0:T(8,128)(2,1)S(1)} collective-permute-done((bf16[256,2048]{1,0:T(8,128)(2,1)S(1)}, bf16[256,2048]{1,0:T(8,128)(2,1)S(1)}, u32[]{:S(2)}, u32[]{:S(2)}) %collective-permute-start.1) | collective-permute-done | bytes 1048608 | tf_op jit(solution)/shard_map/ppermute | solution.py:23
  36.7 1.4 add_convert_fusion.1
  38.1 3.5 %all-to-all-start = ((bf16[4,64,2048]{2,1,0:T(8,128)(2,1)}), bf16[4,64,2048]{2,1,0:T(8,128)(2,1)S(1)}, u32[]{:S(2)}, u32[]{:S(2)}) async-start(bf16[4,64,2048]{2,1,0:T(8,128)(2,1)} %bitcast.12), calls=%async_computation | async-start | bytes 2097152 | tf_op jit(solution)/shard_map/all_to_all | solution.py:27
  41.7 41.9 %all_gather.6 = bf16[512,512]{1,0:T(8,128)(2,1)S(1)} all-gather(bf16[32,512]{1,0:T(8,128)(2,1)S(1)} %slice.116), channel_id=1, replica_groups={{0,32,64,96,128,160,192,224,256,288,320,352,384,416,448,480},{8,40,72,1..., dimensions={0}, use_global_device_ids=true | all-gather | bytes 557056 | tf_op jit(solution)/shard_map/all_gather | solution.py:142
  83.6 0.0 all-to-all-done
  83.6 1.5 broadcast_in_dim.28
  85.1 0.2 convert_reduce_fusion.1
  85.3 1.1 fusion.15
  86.4 1.1 broadcast_in_dim.29
  87.5 0.9 constant_dynamic-update-slice_fusion.5
  88.5 3.7 %collective-permute-start.2 = (bf16[64,2048]{1,0:T(8,128)(2,1)}, bf16[64,2048]{1,0:T(8,128)(2,1)S(1)}, u32[]{:S(2)}, u32[]{:S(2)}) collective-permute-start(bf16[64,2048]{1,0:T(8,128)(2,1)} %get-tuple-element.12), channel_id=1, source_target_pairs={{0,2},{1,3},{2,4},{3,5},{4,6},{5,7},{6,0},{7,1},{8,10},{9,11},{10,... | collective-permute-start | bytes 786440 | tf_op jit(solution)/shard_map/ppermute | solution.py:36
  92.2 3.1 %collective-permute-start.3 = (bf16[64,2048]{1,0:T(8,128)(2,1)}, bf16[64,2048]{1,0:T(8,128)(2,1)S(1)}, u32[]{:S(2)}, u32[]{:S(2)}) collective-permute-start(bf16[64,2048]{1,0:T(8,128)(2,1)} %get-tuple-element.12), channel_id=1, source_target_pairs={{0,6},{1,7},{2,0},{3,1},{4,2},{5,3},{6,4},{7,5},{8,14},{9,15},{10,... | collective-permute-start | bytes 786440 | tf_op jit(solution)/shard_map/ppermute | solution.py:36
  95.3 3.6 %collective-permute-start.4 = (bf16[64,2048]{1,0:T(8,128)(2,1)}, bf16[64,2048]{1,0:T(8,128)(2,1)}, u32[]{:S(2)}, u32[]{:S(2)}) collective-permute-start(bf16[64,2048]{1,0:T(8,128)(2,1)} %get-tuple-element.12), channel_id=1, source_target_pairs={{0,4},{1,5},{2,6},{3,7},{4,0},{5,1},{6,2},{7,3},{8,12},{9,13},{10,... | collective-permute-start | bytes 786440 | tf_op jit(solution)/shard_map/ppermute | solution.py:36
  99.0 3.6 %all-to-all-start.2 = ((bf16[4,512,512]{2,1,0:T(8,128)(2,1)}), bf16[4,512,512]{2,1,0:T(8,128)(2,1)S(1)}, u32[]{:S(2)}, u32[]{:S(2)}) async-start(bf16[4,512,512]{2,1,0:T(8,128)(2,1)} %broadcast_in_dim.28), calls=%async_computation.2 | async-start | bytes 4194304 | tf_op jit(solution)/shard_map/all_to_all | solution.py:27
  102.6 0.0 collective-permute-done.2
  102.6 0.7 constant_dynamic-update-slice_fusion.4
  103.3 0.0 collective-permute-done.3
  103.3 0.7 constant_dynamic-update-slice_fusion.3
  104.0 3.0 %collective-permute-done.4 = bf16[64,2048]{1,0:T(8,128)(2,1)} collective-permute-done((bf16[64,2048]{1,0:T(8,128)(2,1)}, bf16[64,2048]{1,0:T(8,128)(2,1)}, u32[]{:S(2)}, u32[]{:S(2)}) %collective-permute-start.4) | collective-permute-done | bytes 262176 | tf_op jit(solution)/shard_map/ppermute | solution.py:36
  107.0 1.7 constant_dynamic-update-slice_fusion.2
  108.7 5.9 %collective-permute-start.5 = (bf16[256,2048]{1,0:T(8,128)(2,1)}, bf16[256,2048]{1,0:T(8,128)(2,1)}, u32[]{:S(2)}, u32[]{:S(2)}) collective-permute-start(bf16[256,2048]{1,0:T(8,128)(2,1)} %constant_dynamic-update-slice_fusion.2), channel_id=1, source_target_pairs={{0,1},{1,0},{2,3},{3,2},{4,5},{5,4},{6,7},{7,6},{8,9},{9,8},{10,11... | collective-permute-start | bytes 3145736 | tf_op jit(solution)/shard_map/ppermute | solution.py:23
  114.5 8.2 %all-to-all-done.2 = bf16[4,512,512]{2,1,0:T(8,128)(2,1)S(1)} async-done(((bf16[4,512,512]{2,1,0:T(8,128)(2,1)}), bf16[4,512,512]{2,1,0:T(8,128)(2,1)S(1)}, u32[]{:S(2)}, u32[]{:S(2)}) %all-to-all-start.2) | async-done | bytes 2097184 | tf_op jit(solution)/shard_map/all_to_all | solution.py:27
  122.7 1.3 copy-done.1
  124.0 1.7 copy.30
  125.8 0.0 collective-permute-done.5
  125.8 0.0 all-gather.2.cloned.1.call-done
  125.8 6.4 %fusion = f32[512,1408]{1,0:T(8,128)S(1)} fusion(bf16[2048,1600]{1,0:T(8,128)(2,1)} %all-gather.2.cloned.1.call-done, bf16[256,2048]{1,0:T(8,128)(2,1)} %collective-permute-done.5, bf16[256,2048]{1,0:T(8,128)(2,1)} %constant_dynamic-update-slice_fusion.2), kind=kOutput, calls=%fused_computation | convolution fusion | flops 2956984320 | bytes 10747904 | tf_op jit(solution)/shard_map/dot_general | solution.py:154
  132.2 0.5 fusion.6
  132.7 1.7 fusion.11
  134.4 0.8 fusion.2
  135.2 9.0 %collective-permute-start.6 = (bf16[256,2048]{1,0:T(8,128)(2,1)S(1)}, bf16[256,2048]{1,0:T(8,128)(2,1)S(1)}, u32[]{:S(2)}, u32[]{:S(2)}) collective-permute-start(bf16[256,2048]{1,0:T(8,128)(2,1)S(1)} %fusion.2), channel_id=1, source_target_pairs={{0,1},{1,0},{2,3},{3,2},{4,5},{5,4},{6,7},{7,6},{8,9},{9,8},{10,11... | collective-permute-start | bytes 3145736 | tf_op jit(solution)/shard_map/ppermute | solution.py:23
  144.2 1.7 fusion.13
  145.9 0.6 collective-permute-done.6
  146.5 0.8 add_convert_fusion
  147.3 17.1 %all_to_all.26 = bf16[4,64,2048]{2,1,0:T(8,128)(2,1)S(1)} all-to-all(bf16[4,64,2048]{2,1,0:T(8,128)(2,1)S(1)} %bitcast.71), channel_id=1, replica_groups={{0,2,4,6},{1,3,5,7},{8,10,12,14},{9,11,13,15},{16,18,20,22},{17,19,21,2..., dimensions={0} | all-to-all | bytes 2097152 | tf_op jit(solution)/shard_map/all_to_all | solution.py:27
  164.3 0.2 convert_reduce_fusion
  164.5 0.1 broadcast_in_dim.31
  164.6 15.9 %all_to_all.27 = bf16[4,64,2048]{2,1,0:T(8,128)(2,1)S(1)} all-to-all(bf16[4,64,2048]{2,1,0:T(8,128)(2,1)S(1)} %broadcast_in_dim.31), channel_id=1, replica_groups={{0,2,4,6},{1,3,5,7},{8,10,12,14},{9,11,13,15},{16,18,20,22},{17,19,21,2..., dimensions={0} | all-to-all | bytes 2097152 | tf_op jit(solution)/shard_map/all_to_all | solution.py:27
  180.6 4.5 %collective-permute-start.7 = (bf16[256,2048]{1,0:T(8,128)(2,1)S(1)}, bf16[256,2048]{1,0:T(8,128)(2,1)S(1)}, u32[]{:S(2)}, u32[]{:S(2)}) collective-permute-start(bf16[256,2048]{1,0:T(8,128)(2,1)S(1)} %bitcast.72), channel_id=1, source_target_pairs={{0,1},{1,0},{2,3},{3,2},{4,5},{5,4},{6,7},{7,6},{8,9},{9,8},{10,11... | collective-permute-start | bytes 3145736 | tf_op jit(solution)/shard_map/ppermute | solution.py:23
  185.0 0.2 broadcast_in_dim.24
  185.3 0.1 constant_dynamic-update-slice_fusion.1
  185.4 0.0 copy-start.2
  185.4 1.9 collective-permute-done.7
  187.3 1.0 constant_dynamic-update-slice_fusion
  (39 shorter events, 0.3 us)
Async XLA Ops:
  6.5 18.4 %copy-start = (bf16[128,2048]{1,0:T(8,128)(2,1)S(1)}, bf16[128,2048]{1,0:T(8,128)(2,1)}, u32[]{:S(2)}) copy-start(bf16[128,2048]{1,0:T(8,128)(2,1)} %param.17) | copy-start | bytes 1572868
  6.5 13.3 %slice-start = ((bf16[512,64]{0,1:T(8,128)(2,1)}), bf16[128,64]{0,1:T(8,128)(2,1)S(1)}, s32[]{:S(2)}) async-start(bf16[512,64]{0,1:T(8,128)(2,1)} %param.12), calls=%async_computation.6 | async-start | bytes 32768 | tf_op jit(solution)/shard_map/slice | solution.py:68
  6.5 15.6 %copy-start.3 = (bf16[512,64]{0,1:T(8,128)(2,1)S(1)}, bf16[512,64]{0,1:T(8,128)(2,1)}, u32[]{:S(2)}) copy-start(bf16[512,64]{0,1:T(8,128)(2,1)} %param.12) | copy-start | bytes 196612
  6.5 13.3 %slice-start.1 = ((bf16[512,64]{0,1:T(8,128)(2,1)}), bf16[128,64]{0,1:T(8,128)(2,1)S(1)}, s32[]{:S(2)}) async-start(bf16[512,64]{0,1:T(8,128)(2,1)} %param.13), calls=%async_computation.7 | async-start | bytes 32768 | tf_op jit(solution)/shard_map/slice | solution.py:68
  6.5 15.6 %copy-start.4 = (bf16[512,64]{0,1:T(8,128)(2,1)S(1)}, bf16[512,64]{0,1:T(8,128)(2,1)}, u32[]{:S(2)}) copy-start(bf16[512,64]{0,1:T(8,128)(2,1)} %param.13) | copy-start | bytes 196612
  6.5 13.2 %copy-start.7 = (s32[512]{0:T(512)S(1)}, s32[512]{0:T(512)}, u32[]{:S(2)}) copy-start(s32[512]{0:T(512)} %param.14) | copy-start | bytes 6148
  6.6 15.7 %copy-start.5 = (bf16[512,128]{1,0:T(8,128)(2,1)S(1)}, bf16[512,128]{1,0:T(8,128)(2,1)}, u32[]{:S(2)}) copy-start(bf16[512,128]{1,0:T(8,128)(2,1)} %param.11) | copy-start | bytes 393220
  6.6 119.2 %all-gather.2.cloned.1.call-start = ((), (), s32[]{:S(2)}) async-start(), calls=%async_computation.5 | async-start | bytes 7241728 | tf_op jit(solution)/shard_map/all_gather | solution.py:131
  19.7 4.5 %copy-start.9 = (f32[2]{0:T(128)S(1)}, f32[2]{0:T(128)}, u32[]{:S(2)}) copy-start(f32[2]{0:T(128)} %param.15) | copy-start | bytes 28
  19.9 3.5 %collective-permute-start = (bf16[136,128]{0,1:T(8,128)(2,1)S(1)}, bf16[136,128]{0,1:T(8,128)(2,1)S(1)}, u32[]{:S(2)}, u32[]{:S(2)}) collective-permute-start(bf16[136,128]{0,1:T(8,128)(2,1)S(1)} %pad_maximum_fusion.2), channel_id=1, source_target_pairs={{0,8},{8,16},{16,24},{24,32},{32,40},{40,48},{48,56},{56,64},{64,7... | collective-permute-start | bytes 104456 | tf_op jit(solution)/shard_map/ppermute | solution.py:19
  25.5 11.2 %collective-permute-start.1 = (bf16[256,2048]{1,0:T(8,128)(2,1)S(1)}, bf16[256,2048]{1,0:T(8,128)(2,1)S(1)}, u32[]{:S(2)}, u32[]{:S(2)}) collective-permute-start(bf16[256,2048]{1,0:T(8,128)(2,1)S(1)} %convolution_convert_fusion), channel_id=1, source_target_pairs={{0,1},{1,0},{2,3},{3,2},{4,5},{5,4},{6,7},{7,6},{8,9},{9,8},{10,11... | collective-permute-start | bytes 3145736 | tf_op jit(solution)/shard_map/ppermute | solution.py:23
  34.4 7.2 %copy-start.6 = (bf16[704,32]{0,1:T(8,128)(2,1)S(1)}, bf16[704,32]{0,1:T(8,128)(2,1)}, u32[]{:S(2)}) copy-start(bf16[704,32]{0,1:T(8,128)(2,1)} %param.21) | copy-start | bytes 135172
  38.1 45.5 %all-to-all-start = ((bf16[4,64,2048]{2,1,0:T(8,128)(2,1)}), bf16[4,64,2048]{2,1,0:T(8,128)(2,1)S(1)}, u32[]{:S(2)}, u32[]{:S(2)}) async-start(bf16[4,64,2048]{2,1,0:T(8,128)(2,1)} %bitcast.12), calls=%async_computation | async-start | bytes 2097152 | tf_op jit(solution)/shard_map/all_to_all | solution.py:27
  85.1 2.4 %copy-start.8 = (f32[2048]{0:T(1024)S(1)}, f32[2048]{0:T(1024)}, u32[]{:S(2)}) copy-start(f32[2048]{0:T(1024)} %param.18) | copy-start | bytes 24580
  88.5 14.1 %collective-permute-start.2 = (bf16[64,2048]{1,0:T(8,128)(2,1)}, bf16[64,2048]{1,0:T(8,128)(2,1)S(1)}, u32[]{:S(2)}, u32[]{:S(2)}) collective-permute-start(bf16[64,2048]{1,0:T(8,128)(2,1)} %get-tuple-element.12), channel_id=1, source_target_pairs={{0,2},{1,3},{2,4},{3,5},{4,6},{5,7},{6,0},{7,1},{8,10},{9,11},{10,... | collective-permute-start | bytes 786440 | tf_op jit(solution)/shard_map/ppermute | solution.py:36
  92.2 11.1 %collective-permute-start.3 = (bf16[64,2048]{1,0:T(8,128)(2,1)}, bf16[64,2048]{1,0:T(8,128)(2,1)S(1)}, u32[]{:S(2)}, u32[]{:S(2)}) collective-permute-start(bf16[64,2048]{1,0:T(8,128)(2,1)} %get-tuple-element.12), channel_id=1, source_target_pairs={{0,6},{1,7},{2,0},{3,1},{4,2},{5,3},{6,4},{7,5},{8,14},{9,15},{10,... | collective-permute-start | bytes 786440 | tf_op jit(solution)/shard_map/ppermute | solution.py:36
  95.3 11.7 %collective-permute-start.4 = (bf16[64,2048]{1,0:T(8,128)(2,1)}, bf16[64,2048]{1,0:T(8,128)(2,1)}, u32[]{:S(2)}, u32[]{:S(2)}) collective-permute-start(bf16[64,2048]{1,0:T(8,128)(2,1)} %get-tuple-element.12), channel_id=1, source_target_pairs={{0,4},{1,5},{2,6},{3,7},{4,0},{5,1},{6,2},{7,3},{8,12},{9,13},{10,... | collective-permute-start | bytes 786440 | tf_op jit(solution)/shard_map/ppermute | solution.py:36
  99.0 23.7 %all-to-all-start.2 = ((bf16[4,512,512]{2,1,0:T(8,128)(2,1)}), bf16[4,512,512]{2,1,0:T(8,128)(2,1)S(1)}, u32[]{:S(2)}, u32[]{:S(2)}) async-start(bf16[4,512,512]{2,1,0:T(8,128)(2,1)} %broadcast_in_dim.28), calls=%async_computation.2 | async-start | bytes 4194304 | tf_op jit(solution)/shard_map/all_to_all | solution.py:27
  108.7 17.1 %collective-permute-start.5 = (bf16[256,2048]{1,0:T(8,128)(2,1)}, bf16[256,2048]{1,0:T(8,128)(2,1)}, u32[]{:S(2)}, u32[]{:S(2)}) collective-permute-start(bf16[256,2048]{1,0:T(8,128)(2,1)} %constant_dynamic-update-slice_fusion.2), channel_id=1, source_target_pairs={{0,1},{1,0},{2,3},{3,2},{4,5},{5,4},{6,7},{7,6},{8,9},{9,8},{10,11... | collective-permute-start | bytes 3145736 | tf_op jit(solution)/shard_map/ppermute | solution.py:23
  122.7 1.3 copy-start.1
  135.2 11.3 %collective-permute-start.6 = (bf16[256,2048]{1,0:T(8,128)(2,1)S(1)}, bf16[256,2048]{1,0:T(8,128)(2,1)S(1)}, u32[]{:S(2)}, u32[]{:S(2)}) collective-permute-start(bf16[256,2048]{1,0:T(8,128)(2,1)S(1)} %fusion.2), channel_id=1, source_target_pairs={{0,1},{1,0},{2,3},{3,2},{4,5},{5,4},{6,7},{7,6},{8,9},{9,8},{10,11... | collective-permute-start | bytes 3145736 | tf_op jit(solution)/shard_map/ppermute | solution.py:23
  180.6 6.7 %collective-permute-start.7 = (bf16[256,2048]{1,0:T(8,128)(2,1)S(1)}, bf16[256,2048]{1,0:T(8,128)(2,1)S(1)}, u32[]{:S(2)}, u32[]{:S(2)}) collective-permute-start(bf16[256,2048]{1,0:T(8,128)(2,1)S(1)} %bitcast.72), channel_id=1, source_target_pairs={{0,1},{1,0},{2,3},{3,2},{4,5},{5,4},{6,7},{7,6},{8,9},{9,8},{10,11... | collective-permute-start | bytes 3145736 | tf_op jit(solution)/shard_map/ppermute | solution.py:23
  185.4 1.9 copy-start.2
Sparse Core Ops, SparseCore 0:
  19.9 100.1 all-gather.1

commit v4 on v3

--- a/solution.py
+++ b/solution.py
@@ -36,14 +36,17 @@
     return lax.ppermute(shard, "tp", pairs)
 
 
-def all_chips_rows(shard, chip):
-    share = shard.shape[0]
-    rows = jnp.zeros((NX * share, shard.shape[1]), shard.dtype)
-    rows = lax.dynamic_update_slice_in_dim(rows, shard, chip * share, 0)
+def from_chips(shard):
+    arrived = {by: chip_away(shard, by) for by in (2, 1, 3)}
+    return [shard] + [arrived[by] for by in (1, 2, 3)]
+
+
+def summed_at_owners(blocks):
+    arrived = {by: chip_away(blocks[-by], by) for by in (2, 1, 3)}
+    total = blocks[0].astype(jnp.float32)
     for by in (1, 3, 2):
-        sender = lax.rem(chip - by + NX, NX)
-        rows = lax.dynamic_update_slice_in_dim(rows, chip_away(shard, by), sender * share, 0)
-    return rows
+        total = total + arrived[by].astype(jnp.float32)
+    return total
 
 
 def rms_norm(stream, norm_gain):
@@ -148,7 +151,7 @@
     base_rows = lax.dynamic_slice_in_dim(residual, core * half + chip * share, share, 0)
     stream = (base_rows.astype(jnp.float32) + mixed_sum).astype(jnp.bfloat16)
     normed = rms_norm(stream, norm_gain).astype(jnp.bfloat16)
-    normed = all_chips_rows(normed, chip)
+    normed = jnp.concatenate(from_chips(normed), axis=0)
     normed = jnp.concatenate([normed, other_core(normed)], axis=0)
 
     acts = jnp.dot(normed, far[:, : 2 * ff], preferred_element_type=jnp.float32)
@@ -164,10 +167,17 @@
     def through(part):
         return turned_dot(part[:, EARLY:], late) + turned_dot(part[:, :EARLY], down)
 
-    pair_sum = pair_sum_of(through(hidden[half:]).astype(jnp.bfloat16), through(hidden[:half]))
-    mlp_total = to_owners(pair_sum).astype(jnp.float32).sum(axis=0)
+    arrived = other_core(through(hidden[half:]).astype(jnp.bfloat16))
+    total = through(hidden[:half])
+    blocks = [slice(r * share, (r + 1) * share) for r in range(NX)]
+    mlp_total = summed_at_owners(
+        [(total[b] + arrived[b].astype(jnp.float32)).astype(jnp.bfloat16) for b in blocks]
+    )
     finished = (stream.astype(jnp.float32) + mlp_total).astype(jnp.bfloat16)
-    mine = copies(finished, "tp", FAR_X).reshape(half, width)
+    mine = jnp.zeros((half, width), jnp.bfloat16)
+    for by, block in enumerate(from_chips(finished)):
+        at = lax.rem(chip - by + NX, NX) * share
+        mine = lax.dynamic_update_slice_in_dim(mine, block, at, 0)
     theirs = other_core(mine)
     whole = jnp.zeros((rows, width), jnp.bfloat16)
     whole = lax.dynamic_update_slice_in_dim(whole, mine, core * half, 0)

time: 196 us -> 201 us (1.026)
  blocking collectives: 86.2 us -> 53.3 us
  starting transfers between devices: 48.1 us -> 68.4 us
  waiting for transfers between devices: 16.9 us -> 29.9 us
  other arithmetic: 3.66 us -> 6.04 us
  local copies, waits for them, and re-layouts: 12.5 us -> 14.7 us
    all_to_all x3 -> x1, blocking collectives: 44.3 us -> 11.3 us  [swapped(): lax.all_to_all(pieces, axis, 0, 0, tiled=True, axis_index_groups=groups)]
    ppermute x3 -> x9, starting transfers between devices: 10.4 us -> 30.1 us  [chip_away(): return lax.ppermute(shard, 'tp', pairs)]
    ppermute x3 -> x9, waiting for transfers between devices: 2.96 us -> 19.4 us  [chip_away(): return lax.ppermute(shard, 'tp', pairs)]
    unnamed x21 -> x28, local copies, waits for them, and re-layouts: 1.38 us -> 6.67 us
    dynamic_update_slice x3, local copies, waits for them, and re-layouts: 3.1 us -> 0.06 us  [on_device(): mine = lax.dynamic_update_slice_in_dim(mine, block, at, 0)]
    all_to_all x2, waiting for transfers between devices: 8.18 us -> 5.36 us  [swapped(): lax.all_to_all(pieces, axis, 0, 0, tiled=True, axis_index_groups=groups)]
  transfers between devices with their start and end apart: 11 -> 17, of which waited for: 6 -> 11; matrix products, arithmetic and copies ran while one was open for 8% -> 9% of each run, Pallas kernels for 0% -> 0%
where the time goes in v4:
time: 201 us; the launch traced here: 200 us
  starting transfers between devices  68.4 us (34%)
  blocking collectives  53.3 us (27%)
  waiting for transfers between devices  29.9 us (15%)
  local copies, waits for them, and re-layouts  14.7 us (7%)
  between operations  14.1 us (7%)
  matrix products  13.9 us (7%)
  other arithmetic  6.04 us (3%)
    all_gather x1, blocking collectives, on_device(): lax.all_gather(early, 'sp', axis=0, tiled=True, axis_index_groups=FAR_Z)  41.9 us
    ppermute x9, starting transfers between devices, chip_away(): return lax.ppermute(shard, 'tp', pairs)  30.1 us
    ppermute x4, starting transfers between devices, other_core(): return lax.ppermute(shard, 'tp', [(i, i ^ 1) for i in range(2 * NX)])  28.9 us
    ppermute x9, waiting for transfers between devices, chip_away(): return lax.ppermute(shard, 'tp', pairs)  19.4 us
    all_to_all x1, blocking collectives, swapped(): lax.all_to_all(pieces, axis, 0, 0, tiled=True, axis_index_groups=groups)  11.3 us
    all_to_all x2, starting transfers between devices, swapped(): lax.all_to_all(pieces, axis, 0, 0, tiled=True, axis_index_groups=groups)  7.15 us
    unnamed x28, local copies, waits for them, and re-layouts  6.67 us
    dot_general x1, matrix products, on_device(): acts = jnp.dot(normed, far[:, :2 * ff], preferred_element_type=jnp.float32)  6.41 us
  transfers between devices with their start and end apart: 17, of which 11 were waited for; matrix products, arithmetic and copies ran while one was open for 9% of the time, Pallas kernels for 0%

profile of v4, /device:TPU:1, one launch (start us, length us, event | category | flops | bytes accessed | tf_op | source)
XLA Modules:
  0.0 200.3 jit_solution(18300157525468370100)
XLA Ops:
  6.6 0.8 slice.152
  7.4 0.9 concatenate.44
  8.4 11.3 %all_to_all.15 = bf16[4,32,1600]{2,1,0:T(8,128)(2,1)} all-to-all(bf16[4,32,1600]{2,1,0:T(8,128)(2,1)S(1)} %broadcast_in_dim.28), channel_id=1, replica_groups={{0,8,16,24},{32,40,48,56},{64,72,80,88},{96,104,112,120},{128,136,144,1..., dimensions={0} | all-to-all | bytes 819200 | tf_op jit(solution)/shard_map/all_to_all | solution.py:27
  19.9 2.2 %collective-permute-start = (bf16[136,128]{0,1:T(8,128)(2,1)S(1)}, bf16[136,128]{0,1:T(8,128)(2,1)S(1)}, u32[]{:S(2)}, u32[]{:S(2)}) collective-permute-start(bf16[136,128]{0,1:T(8,128)(2,1)S(1)} %pad_maximum_fusion.3), channel_id=1, source_target_pairs={{0,8},{8,16},{16,24},{24,32},{32,40},{40,48},{48,56},{56,64},{64,7... | collective-permute-start | bytes 104456 | tf_op jit(solution)/shard_map/ppermute | solution.py:19
  22.2 0.1 reshape.139
  22.4 1.0 collective-permute-done
  23.5 0.1 add_reduce_fusion
  23.6 0.2 compare_and_fusion
  23.8 0.4 fusion.47
  24.3 0.2 fusion.7
  24.5 0.3 fusion.6
  25.0 0.5 convolution_convert_fusion
  25.5 8.9 %collective-permute-start.1 = (bf16[256,2048]{1,0:T(8,128)(2,1)S(1)}, bf16[256,2048]{1,0:T(8,128)(2,1)S(1)}, u32[]{:S(2)}, u32[]{:S(2)}) collective-permute-start(bf16[256,2048]{1,0:T(8,128)(2,1)S(1)} %convolution_convert_fusion), channel_id=1, source_target_pairs={{0,1},{1,0},{2,3},{3,2},{4,5},{5,4},{6,7},{7,6},{8,9},{9,8},{10,11... | collective-permute-start | bytes 3145736 | tf_op jit(solution)/shard_map/ppermute | solution.py:23
  34.4 2.2 %collective-permute-done.1 = bf16[256,2048]{1,0:T(8,128)(2,1)S(1)} collective-permute-done((bf16[256,2048]{1,0:T(8,128)(2,1)S(1)}, bf16[256,2048]{1,0:T(8,128)(2,1)S(1)}, u32[]{:S(2)}, u32[]{:S(2)}) %collective-permute-start.1) | collective-permute-done | bytes 1048608 | tf_op jit(solution)/shard_map/ppermute | solution.py:23
  36.7 1.4 add_convert_fusion
  38.1 3.5 %all-to-all-start = ((bf16[4,64,2048]{2,1,0:T(8,128)(2,1)}), bf16[4,64,2048]{2,1,0:T(8,128)(2,1)S(1)}, u32[]{:S(2)}, u32[]{:S(2)}) async-start(bf16[4,64,2048]{2,1,0:T(8,128)(2,1)} %bitcast.12), calls=%async_computation | async-start | bytes 2097152 | tf_op jit(solution)/shard_map/all_to_all | solution.py:27
  41.7 41.9 %all_gather.6 = bf16[512,512]{1,0:T(8,128)(2,1)S(1)} all-gather(bf16[32,512]{1,0:T(8,128)(2,1)S(1)} %slice.148), channel_id=1, replica_groups={{0,32,64,96,128,160,192,224,256,288,320,352,384,416,448,480},{8,40,72,1..., dimensions={0}, use_global_device_ids=true | all-gather | bytes 557056 | tf_op jit(solution)/shard_map/all_gather | solution.py:145
  83.6 1.5 broadcast_in_dim.27
  85.2 0.2 convert_reduce_fusion
  85.3 1.1 fusion.12
  86.5 0.9 constant_dynamic-update-slice_fusion.4
  87.4 3.7 %collective-permute-start.2 = (bf16[64,2048]{1,0:T(8,128)(2,1)}, bf16[64,2048]{1,0:T(8,128)(2,1)S(1)}, u32[]{:S(2)}, u32[]{:S(2)}) collective-permute-start(bf16[64,2048]{1,0:T(8,128)(2,1)} %get-tuple-element.14), channel_id=1, source_target_pairs={{0,2},{1,3},{2,4},{3,5},{4,6},{5,7},{6,0},{7,1},{8,10},{9,11},{10,... | collective-permute-start | bytes 786440 | tf_op jit(solution)/shard_map/ppermute | solution.py:36
  91.1 4.3 %collective-permute-start.3 = (bf16[64,2048]{1,0:T(8,128)(2,1)}, bf16[64,2048]{1,0:T(8,128)(2,1)S(1)}, u32[]{:S(2)}, u32[]{:S(2)}) collective-permute-start(bf16[64,2048]{1,0:T(8,128)(2,1)} %get-tuple-element.14), channel_id=1, source_target_pairs={{0,4},{1,5},{2,6},{3,7},{4,0},{5,1},{6,2},{7,3},{8,12},{9,13},{10,... | collective-permute-start | bytes 786440 | tf_op jit(solution)/shard_map/ppermute | solution.py:36
  95.4 3.1 %collective-permute-start.4 = (bf16[64,2048]{1,0:T(8,128)(2,1)}, bf16[64,2048]{1,0:T(8,128)(2,1)}, u32[]{:S(2)}, u32[]{:S(2)}) collective-permute-start(bf16[64,2048]{1,0:T(8,128)(2,1)} %get-tuple-element.14), channel_id=1, source_target_pairs={{0,6},{1,7},{2,0},{3,1},{4,2},{5,3},{6,4},{7,5},{8,14},{9,15},{10,... | collective-permute-start | bytes 786440 | tf_op jit(solution)/shard_map/ppermute | solution.py:36
  98.5 3.6 %all-to-all-start.2 = ((bf16[4,512,512]{2,1,0:T(8,128)(2,1)}), bf16[4,512,512]{2,1,0:T(8,128)(2,1)S(1)}, u32[]{:S(2)}, u32[]{:S(2)}) async-start(bf16[4,512,512]{2,1,0:T(8,128)(2,1)} %broadcast_in_dim.27), calls=%async_computation.2 | async-start | bytes 4194304 | tf_op jit(solution)/shard_map/all_to_all | solution.py:27
  102.1 2.2 %collective-permute-done.4 = bf16[64,2048]{1,0:T(8,128)(2,1)} collective-permute-done((bf16[64,2048]{1,0:T(8,128)(2,1)}, bf16[64,2048]{1,0:T(8,128)(2,1)}, u32[]{:S(2)}, u32[]{:S(2)}) %collective-permute-start.4) | collective-permute-done | bytes 262176 | tf_op jit(solution)/shard_map/ppermute | solution.py:36
  104.3 1.1 pad_maximum_fusion
  105.4 7.3 %collective-permute-start.5 = (bf16[256,2048]{1,0:T(8,128)(2,1)S(1)}, bf16[256,2048]{1,0:T(8,128)(2,1)S(1)}, u32[]{:S(2)}, u32[]{:S(2)}) collective-permute-start(bf16[256,2048]{1,0:T(8,128)(2,1)S(1)} %pad_maximum_fusion), channel_id=1, source_target_pairs={{0,1},{1,0},{2,3},{3,2},{4,5},{5,4},{6,7},{7,6},{8,9},{9,8},{10,11... | collective-permute-start | bytes 3145736 | tf_op jit(solution)/shard_map/ppermute | solution.py:23
  112.7 0.7 constant_dynamic-update-slice_fusion.3
  113.4 0.7 constant_dynamic-update-slice_fusion.2
  114.2 1.7 constant_dynamic-update-slice_fusion.1
  115.8 1.0 constant_dynamic-update-slice_fusion
  116.9 5.4 %all-to-all-done.2 = bf16[4,512,512]{2,1,0:T(8,128)(2,1)S(1)} async-done(((bf16[4,512,512]{2,1,0:T(8,128)(2,1)}), bf16[4,512,512]{2,1,0:T(8,128)(2,1)S(1)}, u32[]{:S(2)}, u32[]{:S(2)}) %all-to-all-start.2) | async-done | bytes 2097184 | tf_op jit(solution)/shard_map/all_to_all | solution.py:27
  122.2 1.4 copy-done.2
  123.6 1.7 copy.30
  125.4 6.4 %fusion = f32[512,1408]{1,0:T(8,128)S(1)} fusion(bf16[512,2048]{1,0:T(8,128)(2,1)} %constant_dynamic-update-slice_fusion, bf16[2048,1600]{1,0:T(8,128)(2,1)} %all-gather.2.cloned.1.call-done), kind=kOutput, calls=%fused_computation | convolution fusion | flops 2952790016 | bytes 10747904 | tf_op jit(solution)/shard_map/dot_general | solution.py:157
  131.8 0.5 fusion.3
  132.3 1.7 fusion.8
  134.0 0.7 fusion.2
  134.7 9.0 %collective-permute-start.6 = (bf16[256,2048]{1,0:T(8,128)(2,1)S(1)}, bf16[256,2048]{1,0:T(8,128)(2,1)S(1)}, u32[]{:S(2)}, u32[]{:S(2)}) collective-permute-start(bf16[256,2048]{1,0:T(8,128)(2,1)S(1)} %fusion.2), channel_id=1, source_target_pairs={{0,1},{1,0},{2,3},{3,2},{4,5},{5,4},{6,7},{7,6},{8,9},{9,8},{10,11... | collective-permute-start | bytes 3145736 | tf_op jit(solution)/shard_map/ppermute | solution.py:23
  143.8 1.7 fusion.10
  145.5 0.7 convolution_add_fusion.1
  146.3 1.3 copy-done.1
  147.6 0.2 fusion.18
  147.7 0.8 copy-done.4
  148.6 2.2 %collective-permute-start.7 = (bf16[64,2048]{1,0:T(8,128)(2,1)S(1)}, bf16[64,2048]{1,0:T(8,128)(2,1)S(1)}, u32[]{:S(2)}, u32[]{:S(2)}) collective-permute-start(bf16[64,2048]{1,0:T(8,128)(2,1)S(1)} %get-tuple-element.17), channel_id=1, source_target_pairs={{0,2},{1,3},{2,4},{3,5},{4,6},{5,7},{6,0},{7,1},{8,10},{9,11},{10,... | collective-permute-start | bytes 786440 | tf_op jit(solution)/shard_map/ppermute | solution.py:36
  150.7 4.3 %collective-permute-start.8 = (bf16[64,2048]{1,0:T(8,128)(2,1)S(1)}, bf16[64,2048]{1,0:T(8,128)(2,1)S(1)}, u32[]{:S(2)}, u32[]{:S(2)}) collective-permute-start(bf16[64,2048]{1,0:T(8,128)(2,1)S(1)} %get-tuple-element.19), channel_id=1, source_target_pairs={{0,6},{1,7},{2,0},{3,1},{4,2},{5,3},{6,4},{7,5},{8,14},{9,15},{10,... | collective-permute-start | bytes 786440 | tf_op jit(solution)/shard_map/ppermute | solution.py:36
  155.1 1.9 collective-permute-start.9
  157.0 2.5 %collective-permute-done.7 = bf16[64,2048]{1,0:T(8,128)(2,1)S(1)} collective-permute-done((bf16[64,2048]{1,0:T(8,128)(2,1)S(1)}, bf16[64,2048]{1,0:T(8,128)(2,1)S(1)}, u32[]{:S(2)}, u32[]{:S(2)}) %collective-permute-start.7) | collective-permute-done | bytes 262176 | tf_op jit(solution)/shard_map/ppermute | solution.py:36
  159.5 1.5 collective-permute-done.8
  161.0 4.7 %collective-permute-done.9 = bf16[64,2048]{1,0:T(8,128)(2,1)S(1)} collective-permute-done((bf16[64,2048]{1,0:T(8,128)(2,1)S(1)}, bf16[64,2048]{1,0:T(8,128)(2,1)S(1)}, u32[]{:S(2)}, u32[]{:S(2)}) %collective-permute-start.9) | collective-permute-done | bytes 262176 | tf_op jit(solution)/shard_map/ppermute | solution.py:36
  165.7 0.1 broadcast_in_dim.23
  165.9 1.3 constant_dynamic-update-slice_fusion.10
  167.2 3.8 %collective-permute-start.10 = (bf16[64,2048]{1,0:T(8,128)(2,1)S(1)}, bf16[64,2048]{1,0:T(8,128)(2,1)S(1)}, u32[]{:S(2)}, u32[]{:S(2)}) collective-permute-start(bf16[64,2048]{1,0:T(8,128)(2,1)S(1)} %get-tuple-element.12), channel_id=1, source_target_pairs={{0,2},{1,3},{2,4},{3,5},{4,6},{5,7},{6,0},{7,1},{8,10},{9,11},{10,... | collective-permute-start | bytes 786440 | tf_op jit(solution)/shard_map/ppermute | solution.py:36
  171.0 4.9 %collective-permute-start.11 = (bf16[64,2048]{1,0:T(8,128)(2,1)S(1)}, bf16[64,2048]{1,0:T(8,128)(2,1)S(1)}, u32[]{:S(2)}, u32[]{:S(2)}) collective-permute-start(bf16[64,2048]{1,0:T(8,128)(2,1)S(1)} %get-tuple-element.12), channel_id=1, source_target_pairs={{0,4},{1,5},{2,6},{3,7},{4,0},{5,1},{6,2},{7,3},{8,12},{9,13},{10,... | collective-permute-start | bytes 786440 | tf_op jit(solution)/shard_map/ppermute | solution.py:36
  175.9 1.9 collective-permute-start.12
  177.9 0.4 collective-permute-done.10
  178.3 6.5 %collective-permute-done.11 = bf16[64,2048]{1,0:T(8,128)(2,1)S(1)} collective-permute-done((bf16[64,2048]{1,0:T(8,128)(2,1)S(1)}, bf16[64,2048]{1,0:T(8,128)(2,1)S(1)}, u32[]{:S(2)}, u32[]{:S(2)}) %collective-permute-start.11) | collective-permute-done | bytes 262176 | tf_op jit(solution)/shard_map/ppermute | solution.py:36
  184.9 1.5 collective-permute-done.12
  186.4 3.7 %collective-permute-start.13 = (bf16[256,2048]{1,0:T(8,128)(2,1)S(1)}, bf16[256,2048]{1,0:T(8,128)(2,1)S(1)}, u32[]{:S(2)}, u32[]{:S(2)}) collective-permute-start(bf16[256,2048]{1,0:T(8,128)(2,1)S(1)} %constant_dynamic-update-slice_fusion.7), channel_id=1, source_target_pairs={{0,1},{1,0},{2,3},{3,2},{4,5},{5,4},{6,7},{7,6},{8,9},{9,8},{10,11... | collective-permute-start | bytes 3145736 | tf_op jit(solution)/shard_map/ppermute | solution.py:23
  190.1 0.2 broadcast_in_dim.22
  190.4 0.1 constant_dynamic-update-slice_fusion.6
  190.5 1.9 collective-permute-done.13
  192.4 1.0 constant_dynamic-update-slice_fusion.5
  (57 shorter events, 0.8 us)
Async XLA Ops:
  6.5 18.4 %copy-start = (bf16[128,2048]{1,0:T(8,128)(2,1)S(1)}, bf16[128,2048]{1,0:T(8,128)(2,1)}, u32[]{:S(2)}) copy-start(bf16[128,2048]{1,0:T(8,128)(2,1)} %param.17) | copy-start | bytes 1572868
  6.5 13.3 %slice-start = ((bf16[512,64]{0,1:T(8,128)(2,1)}), bf16[128,64]{0,1:T(8,128)(2,1)S(1)}, s32[]{:S(2)}) async-start(bf16[512,64]{0,1:T(8,128)(2,1)} %param.12), calls=%async_computation.4 | async-start | bytes 32768 | tf_op jit(solution)/shard_map/slice | solution.py:71
  6.5 15.6 %copy-start.5 = (bf16[512,64]{0,1:T(8,128)(2,1)S(1)}, bf16[512,64]{0,1:T(8,128)(2,1)}, u32[]{:S(2)}) copy-start(bf16[512,64]{0,1:T(8,128)(2,1)} %param.12) | copy-start | bytes 196612
  6.5 13.3 %slice-start.1 = ((bf16[512,64]{0,1:T(8,128)(2,1)}), bf16[128,64]{0,1:T(8,128)(2,1)S(1)}, s32[]{:S(2)}) async-start(bf16[512,64]{0,1:T(8,128)(2,1)} %param.13), calls=%async_computation.5 | async-start | bytes 32768 | tf_op jit(solution)/shard_map/slice | solution.py:71
  6.5 15.6 %copy-start.6 = (bf16[512,64]{0,1:T(8,128)(2,1)S(1)}, bf16[512,64]{0,1:T(8,128)(2,1)}, u32[]{:S(2)}) copy-start(bf16[512,64]{0,1:T(8,128)(2,1)} %param.13) | copy-start | bytes 196612
  6.5 13.2 %copy-start.9 = (s32[512]{0:T(512)S(1)}, s32[512]{0:T(512)}, u32[]{:S(2)}) copy-start(s32[512]{0:T(512)} %param.14) | copy-start | bytes 6148
  6.6 15.7 %copy-start.7 = (bf16[512,128]{1,0:T(8,128)(2,1)S(1)}, bf16[512,128]{1,0:T(8,128)(2,1)}, u32[]{:S(2)}) copy-start(bf16[512,128]{1,0:T(8,128)(2,1)} %param.11) | copy-start | bytes 393220
  6.6 118.8 %all-gather.2.cloned.1.call-start = ((), (), s32[]{:S(2)}) async-start(), calls=%async_computation.3 | async-start | bytes 7241728 | tf_op jit(solution)/shard_map/all_gather | solution.py:134
  19.7 4.5 %copy-start.11 = (f32[2]{0:T(128)S(1)}, f32[2]{0:T(128)}, u32[]{:S(2)}) copy-start(f32[2]{0:T(128)} %param.15) | copy-start | bytes 28
  19.9 3.5 %collective-permute-start = (bf16[136,128]{0,1:T(8,128)(2,1)S(1)}, bf16[136,128]{0,1:T(8,128)(2,1)S(1)}, u32[]{:S(2)}, u32[]{:S(2)}) collective-permute-start(bf16[136,128]{0,1:T(8,128)(2,1)S(1)} %pad_maximum_fusion.3), channel_id=1, source_target_pairs={{0,8},{8,16},{16,24},{24,32},{32,40},{40,48},{48,56},{56,64},{64,7... | collective-permute-start | bytes 104456 | tf_op jit(solution)/shard_map/ppermute | solution.py:19
  25.5 11.2 %collective-permute-start.1 = (bf16[256,2048]{1,0:T(8,128)(2,1)S(1)}, bf16[256,2048]{1,0:T(8,128)(2,1)S(1)}, u32[]{:S(2)}, u32[]{:S(2)}) collective-permute-start(bf16[256,2048]{1,0:T(8,128)(2,1)S(1)} %convolution_convert_fusion), channel_id=1, source_target_pairs={{0,1},{1,0},{2,3},{3,2},{4,5},{5,4},{6,7},{7,6},{8,9},{9,8},{10,11... | collective-permute-start | bytes 3145736 | tf_op jit(solution)/shard_map/ppermute | solution.py:23
  34.4 7.2 %copy-start.8 = (bf16[704,32]{0,1:T(8,128)(2,1)S(1)}, bf16[704,32]{0,1:T(8,128)(2,1)}, u32[]{:S(2)}) copy-start(bf16[704,32]{0,1:T(8,128)(2,1)} %param.21) | copy-start | bytes 135172
  38.1 45.5 %all-to-all-start = ((bf16[4,64,2048]{2,1,0:T(8,128)(2,1)}), bf16[4,64,2048]{2,1,0:T(8,128)(2,1)S(1)}, u32[]{:S(2)}, u32[]{:S(2)}) async-start(bf16[4,64,2048]{2,1,0:T(8,128)(2,1)} %bitcast.12), calls=%async_computation | async-start | bytes 2097152 | tf_op jit(solution)/shard_map/all_to_all | solution.py:27
  83.6 2.9 %copy-start.10 = (f32[2048]{0:T(1024)S(1)}, f32[2048]{0:T(1024)}, u32[]{:S(2)}) copy-start(f32[2048]{0:T(1024)} %param.18) | copy-start | bytes 24580
  87.4 14.7 %collective-permute-start.2 = (bf16[64,2048]{1,0:T(8,128)(2,1)}, bf16[64,2048]{1,0:T(8,128)(2,1)S(1)}, u32[]{:S(2)}, u32[]{:S(2)}) collective-permute-start(bf16[64,2048]{1,0:T(8,128)(2,1)} %get-tuple-element.14), channel_id=1, source_target_pairs={{0,2},{1,3},{2,4},{3,5},{4,6},{5,7},{6,0},{7,1},{8,10},{9,11},{10,... | collective-permute-start | bytes 786440 | tf_op jit(solution)/shard_map/ppermute | solution.py:36
  91.1 11.0 %collective-permute-start.3 = (bf16[64,2048]{1,0:T(8,128)(2,1)}, bf16[64,2048]{1,0:T(8,128)(2,1)S(1)}, u32[]{:S(2)}, u32[]{:S(2)}) collective-permute-start(bf16[64,2048]{1,0:T(8,128)(2,1)} %get-tuple-element.14), channel_id=1, source_target_pairs={{0,4},{1,5},{2,6},{3,7},{4,0},{5,1},{6,2},{7,3},{8,12},{9,13},{10,... | collective-permute-start | bytes 786440 | tf_op jit(solution)/shard_map/ppermute | solution.py:36
  95.4 8.9 %collective-permute-start.4 = (bf16[64,2048]{1,0:T(8,128)(2,1)}, bf16[64,2048]{1,0:T(8,128)(2,1)}, u32[]{:S(2)}, u32[]{:S(2)}) collective-permute-start(bf16[64,2048]{1,0:T(8,128)(2,1)} %get-tuple-element.14), channel_id=1, source_target_pairs={{0,6},{1,7},{2,0},{3,1},{4,2},{5,3},{6,4},{7,5},{8,14},{9,15},{10,... | collective-permute-start | bytes 786440 | tf_op jit(solution)/shard_map/ppermute | solution.py:36
  98.5 23.8 %all-to-all-start.2 = ((bf16[4,512,512]{2,1,0:T(8,128)(2,1)}), bf16[4,512,512]{2,1,0:T(8,128)(2,1)S(1)}, u32[]{:S(2)}, u32[]{:S(2)}) async-start(bf16[4,512,512]{2,1,0:T(8,128)(2,1)} %broadcast_in_dim.27), calls=%async_computation.2 | async-start | bytes 4194304 | tf_op jit(solution)/shard_map/all_to_all | solution.py:27
  105.4 10.4 %collective-permute-start.5 = (bf16[256,2048]{1,0:T(8,128)(2,1)S(1)}, bf16[256,2048]{1,0:T(8,128)(2,1)S(1)}, u32[]{:S(2)}, u32[]{:S(2)}) collective-permute-start(bf16[256,2048]{1,0:T(8,128)(2,1)S(1)} %pad_maximum_fusion), channel_id=1, source_target_pairs={{0,1},{1,0},{2,3},{3,2},{4,5},{5,4},{6,7},{7,6},{8,9},{9,8},{10,11... | collective-permute-start | bytes 3145736 | tf_op jit(solution)/shard_map/ppermute | solution.py:23
  122.2 1.4 copy-start.2
  134.7 11.5 %collective-permute-start.6 = (bf16[256,2048]{1,0:T(8,128)(2,1)S(1)}, bf16[256,2048]{1,0:T(8,128)(2,1)S(1)}, u32[]{:S(2)}, u32[]{:S(2)}) collective-permute-start(bf16[256,2048]{1,0:T(8,128)(2,1)S(1)} %fusion.2), channel_id=1, source_target_pairs={{0,1},{1,0},{2,3},{3,2},{4,5},{5,4},{6,7},{7,6},{8,9},{9,8},{10,11... | collective-permute-start | bytes 3145736 | tf_op jit(solution)/shard_map/ppermute | solution.py:23
  146.2 1.3 copy-start.1
  147.6 1.0 copy-start.4
  148.6 10.9 %collective-permute-start.7 = (bf16[64,2048]{1,0:T(8,128)(2,1)S(1)}, bf16[64,2048]{1,0:T(8,128)(2,1)S(1)}, u32[]{:S(2)}, u32[]{:S(2)}) collective-permute-start(bf16[64,2048]{1,0:T(8,128)(2,1)S(1)} %get-tuple-element.17), channel_id=1, source_target_pairs={{0,2},{1,3},{2,4},{3,5},{4,6},{5,7},{6,0},{7,1},{8,10},{9,11},{10,... | collective-permute-start | bytes 786440 | tf_op jit(solution)/shard_map/ppermute | solution.py:36
  150.7 10.3 %collective-permute-start.8 = (bf16[64,2048]{1,0:T(8,128)(2,1)S(1)}, bf16[64,2048]{1,0:T(8,128)(2,1)S(1)}, u32[]{:S(2)}, u32[]{:S(2)}) collective-permute-start(bf16[64,2048]{1,0:T(8,128)(2,1)S(1)} %get-tuple-element.19), channel_id=1, source_target_pairs={{0,6},{1,7},{2,0},{3,1},{4,2},{5,3},{6,4},{7,5},{8,14},{9,15},{10,... | collective-permute-start | bytes 786440 | tf_op jit(solution)/shard_map/ppermute | solution.py:36
  155.1 10.7 %collective-permute-start.9 = (bf16[64,2048]{1,0:T(8,128)(2,1)S(1)}, bf16[64,2048]{1,0:T(8,128)(2,1)S(1)}, u32[]{:S(2)}, u32[]{:S(2)}) collective-permute-start(bf16[64,2048]{1,0:T(8,128)(2,1)S(1)} %get-tuple-element.18), channel_id=1, source_target_pairs={{0,4},{1,5},{2,6},{3,7},{4,0},{5,1},{6,2},{7,3},{8,12},{9,13},{10,... | collective-permute-start | bytes 786440 | tf_op jit(solution)/shard_map/ppermute | solution.py:36
  167.2 11.1 %collective-permute-start.10 = (bf16[64,2048]{1,0:T(8,128)(2,1)S(1)}, bf16[64,2048]{1,0:T(8,128)(2,1)S(1)}, u32[]{:S(2)}, u32[]{:S(2)}) collective-permute-start(bf16[64,2048]{1,0:T(8,128)(2,1)S(1)} %get-tuple-element.12), channel_id=1, source_target_pairs={{0,2},{1,3},{2,4},{3,5},{4,6},{5,7},{6,0},{7,1},{8,10},{9,11},{10,... | collective-permute-start | bytes 786440 | tf_op jit(solution)/shard_map/ppermute | solution.py:36
  171.0 13.8 %collective-permute-start.11 = (bf16[64,2048]{1,0:T(8,128)(2,1)S(1)}, bf16[64,2048]{1,0:T(8,128)(2,1)S(1)}, u32[]{:S(2)}, u32[]{:S(2)}) collective-permute-start(bf16[64,2048]{1,0:T(8,128)(2,1)S(1)} %get-tuple-element.12), channel_id=1, source_target_pairs={{0,4},{1,5},{2,6},{3,7},{4,0},{5,1},{6,2},{7,3},{8,12},{9,13},{10,... | collective-permute-start | bytes 786440 | tf_op jit(solution)/shard_map/ppermute | solution.py:36
  175.9 10.4 %collective-permute-start.12 = (bf16[64,2048]{1,0:T(8,128)(2,1)S(1)}, bf16[64,2048]{1,0:T(8,128)(2,1)S(1)}, u32[]{:S(2)}, u32[]{:S(2)}) collective-permute-start(bf16[64,2048]{1,0:T(8,128)(2,1)S(1)} %get-tuple-element.12), channel_id=1, source_target_pairs={{0,6},{1,7},{2,0},{3,1},{4,2},{5,3},{6,4},{7,5},{8,14},{9,15},{10,... | collective-permute-start | bytes 786440 | tf_op jit(solution)/shard_map/ppermute | solution.py:36
  186.4 6.0 %collective-permute-start.13 = (bf16[256,2048]{1,0:T(8,128)(2,1)S(1)}, bf16[256,2048]{1,0:T(8,128)(2,1)S(1)}, u32[]{:S(2)}, u32[]{:S(2)}) collective-permute-start(bf16[256,2048]{1,0:T(8,128)(2,1)S(1)} %constant_dynamic-update-slice_fusion.7), channel_id=1, source_target_pairs={{0,1},{1,0},{2,3},{3,2},{4,5},{5,4},{6,7},{7,6},{8,9},{9,8},{10,11... | collective-permute-start | bytes 3145736 | tf_op jit(solution)/shard_map/ppermute | solution.py:23
  190.5 1.9 copy-start.3
Sparse Core Ops, SparseCore 0:
  19.9 100.1 all-gather.1

commit v5 on v3

--- a/solution.py
+++ b/solution.py
@@ -1,13 +1,17 @@
 import jax
 import jax.numpy as jnp
 from jax import lax
+from jax.experimental import pallas as pl
+from jax.experimental.pallas import tpu as pltpu
 from jax.sharding import PartitionSpec as P
 
 
 HD = 64
 WINDOW = 128
 NZ, NY, NX = 16, 4, 4
-EARLY = 512
+EARLY = 640
+IN_VMEM = pl.BlockSpec(memory_space=pltpu.VMEM)
+IN_HBM = pl.BlockSpec(memory_space=pltpu.HBM)
 FAR_Z = [[z * NY + y for z in range(NZ)] for y in range(NY)]
 FAR_Y = [[z * NY + y for y in range(NY)] for z in range(NZ)]
 FAR_X = [[2 * x + c for x in range(NX)] for c in range(2)]
@@ -36,9 +40,8 @@
     return lax.ppermute(shard, "tp", pairs)
 
 
-def all_chips_rows(shard, chip):
+def all_chips_rows(shard, chip, rows):
     share = shard.shape[0]
-    rows = jnp.zeros((NX * share, shard.shape[1]), shard.dtype)
     rows = lax.dynamic_update_slice_in_dim(rows, shard, chip * share, 0)
     for by in (1, 3, 2):
         sender = lax.rem(chip - by + NX, NX)
@@ -104,6 +107,106 @@
 
 def to_owners(pair_sum):
     return swapped(pair_sum.reshape(NX, -1, pair_sum.shape[1]), "tp", FAR_X)
+
+
+def gated(mine, theirs, far, ff):
+    half, width = mine.shape
+    columns = far.shape[1]
+    steps = 4
+    depth = width // steps
+
+    def kernel(mine_ref, theirs_ref, far_ref, hidden_ref, late_ref, rows, held, acts_ref, arrived):
+        moves = []
+        for k in range(steps):
+            at = pl.ds(k * depth, depth)
+            pairs = (
+                (mine_ref.at[:, at], rows.at[k, pl.ds(0, half)]),
+                (theirs_ref.at[:, at], rows.at[k, pl.ds(half, half)]),
+                (far_ref.at[at], held.at[k]),
+            )
+            moves.append(
+                [pltpu.make_async_copy(*pair, arrived.at[k, i]) for i, pair in enumerate(pairs)]
+            )
+        for move in moves[0] + moves[1]:
+            move.start()
+        for k in range(steps):
+            for move in moves[k]:
+                move.wait()
+            if k + 2 < steps:
+                for move in moves[k + 2]:
+                    move.start()
+            late_ref[k * depth : (k + 1) * depth, :] = held[k, :, 2 * ff :]
+            part = jnp.dot(rows[k], held[k, :, : 2 * ff], preferred_element_type=jnp.float32)
+            if k == 0:
+                acts_ref[...] = part
+            elif k < steps - 1:
+                acts_ref[...] += part
+            else:
+                acts = acts_ref[...] + part
+                hidden_ref[...] = (jax.nn.silu(acts[:, :ff]) * acts[:, ff:]).astype(jnp.bfloat16)
+
+    return pl.pallas_call(
+        kernel,
+        out_shape=(
+            jax.ShapeDtypeStruct((2 * half, ff), jnp.bfloat16),
+            jax.ShapeDtypeStruct((width, columns - 2 * ff), jnp.bfloat16),
+        ),
+        in_specs=[IN_HBM] * 3,
+        out_specs=(IN_VMEM, IN_VMEM),
+        scratch_shapes=[
+            pltpu.VMEM((steps, 2 * half, depth), jnp.bfloat16),
+            pltpu.VMEM((steps, depth, columns), jnp.bfloat16),
+            pltpu.VMEM((2 * half, 2 * ff), jnp.float32),
+            pltpu.SemaphoreType.DMA((steps, 3)),
+        ],
+        name="gated",
+    )(mine, theirs, far)
+
+
+def lowered(hidden, down, late, first, half):
+    width = late.shape[0]
+    ny, nz, rows, _ = down.shape
+    pair = 2 * ny * rows
+
+    def kernel(hidden_ref, down_ref, late_ref, out_ref, left, first_units, last_units, arrived):
+        moves = [
+            pltpu.make_async_copy(hidden_ref.at[pl.ds(first, half)], left, arrived.at[0]),
+            pltpu.make_async_copy(late_ref, last_units, arrived.at[1]),
+        ]
+        groups = [pl.ds(0, nz // 4), pl.ds(nz // 4, nz - nz // 4)]
+        for i, group in enumerate(groups):
+            moves.append(
+                pltpu.make_async_copy(
+                    down_ref.at[:, group], first_units.at[:, group], arrived.at[2 + i]
+                )
+            )
+        for move in moves:
+            move.start()
+        for move in moves[:3]:
+            move.wait()
+        for z in range(0, nz, 2):
+            if z == nz // 4:
+                moves[3].wait()
+            blocks = [first_units[y, z + i] for i in range(2) for y in range(ny)]
+            at = slice(z * ny * rows, z * ny * rows + pair)
+            right = jnp.concatenate([jnp.concatenate(blocks, axis=0), last_units[at, :]], axis=1)
+            out_ref[:, at] = lax.dot_general(
+                left[...], right, (((1,), (1,)), ((), ())), preferred_element_type=jnp.float32
+            ).astype(out_ref.dtype)
+
+    return pl.pallas_call(
+        kernel,
+        out_shape=jax.ShapeDtypeStruct((half, width), jnp.bfloat16),
+        in_specs=[IN_HBM] * 3,
+        out_specs=IN_VMEM,
+        scratch_shapes=[
+            pltpu.VMEM((half, hidden.shape[1]), jnp.bfloat16),
+            pltpu.VMEM(down.shape, jnp.bfloat16),
+            pltpu.VMEM(late.shape, jnp.bfloat16),
+            pltpu.SemaphoreType.DMA((4,)),
+        ],
+        name="lowered",
+    )(hidden, down, late)
 
 
 def on_device(
@@ -143,28 +246,19 @@
     spread = jnp.broadcast_to(column[None], (NY, *column.shape))
     spread, pieces = lax.optimization_barrier((spread, pieces))
     down = swapped(spread, "sp", FAR_Y)
-    down = jnp.swapaxes(down.reshape(NY, NZ, -1, EARLY), 0, 1).reshape(width, EARLY)
+    down = down.reshape(NY, NZ, -1, EARLY)
     mixed_sum = pieces.astype(jnp.float32).sum(axis=0)
     base_rows = lax.dynamic_slice_in_dim(residual, core * half + chip * share, share, 0)
     stream = (base_rows.astype(jnp.float32) + mixed_sum).astype(jnp.bfloat16)
     normed = rms_norm(stream, norm_gain).astype(jnp.bfloat16)
-    normed = all_chips_rows(normed, chip)
-    normed = jnp.concatenate([normed, other_core(normed)], axis=0)
-
-    acts = jnp.dot(normed, far[:, : 2 * ff], preferred_element_type=jnp.float32)
-    hidden = (jax.nn.silu(acts[:, :ff]) * acts[:, ff:]).astype(jnp.bfloat16)
-
-    def turned_dot(left, right):
-        return lax.dot_general(
-            left, right, (((1,), (1,)), ((), ())), preferred_element_type=jnp.float32
-        )
-
-    late = far[:, 2 * ff :]
-
-    def through(part):
-        return turned_dot(part[:, EARLY:], late) + turned_dot(part[:, :EARLY], down)
-
-    pair_sum = pair_sum_of(through(hidden[half:]).astype(jnp.bfloat16), through(hidden[:half]))
+    normed = all_chips_rows(normed, chip, pair_sum)
+    theirs = other_core(normed)
+    hidden, late = gated(normed, theirs, far, ff)
+
+    pair_sum = pair_sum_of(
+        lowered(hidden, down, late, half, half),
+        lowered(hidden, down, late, 0, half).astype(jnp.float32),
+    )
     mlp_total = to_owners(pair_sum).astype(jnp.float32).sum(axis=0)
     finished = (stream.astype(jnp.float32) + mlp_total).astype(jnp.bfloat16)
     mine = copies(finished, "tp", FAR_X).reshape(half, width)

time: 196 us -> 194 us (0.990)
  Pallas kernels: 0 us -> 14.4 us
  matrix products: 13.9 us -> 2.57 us
  waiting for transfers between devices: 16.9 us -> 9.66 us
  blocking collectives: 86.2 us -> 90.2 us
  starting transfers between devices: 48.1 us -> 45 us
    pallas_call x0 -> x3, Pallas kernels: none -> 14.4 us  [the longest x2 7.71 us: lowered(): pl.pallas_call(kernel, out_shape=jax.ShapeDtypeStruct((half, width), jnp....]
    dot_general x5 -> x0, matrix products: 11.3 us -> none  [the longest x1 6.39 us: on_device(): acts = jnp.dot(normed, far[:, :2 * ff], preferred_element_type=jnp.float32)]
    all_to_all x2, waiting for transfers between devices: 8.18 us -> 0.01 us  [swapped(): lax.all_to_all(pieces, axis, 0, 0, tiled=True, axis_index_groups=groups)]
    ppermute x4, starting transfers between devices: 28.3 us -> 25.4 us  [other_core(): return lax.ppermute(shard, 'tp', [(i, i ^ 1) for i in range(2 * NX)])]
    all_gather x1, blocking collectives: 41.9 us -> 44.2 us  [on_device(): lax.all_gather(early, 'sp', axis=0, tiled=True, axis_index_groups=FAR_Z)]
    ppermute x4, waiting for transfers between devices: 4.68 us -> 6.72 us  [other_core(): return lax.ppermute(shard, 'tp', [(i, i ^ 1) for i in range(2 * NX)])]
  transfers between devices with their start and end apart: 11 -> 11, of which waited for: 6 -> 5; matrix products, arithmetic and copies ran while one was open for 8% -> 7% of each run, Pallas kernels for 0% -> 5%
where the time goes in v5:
time: 194 us
  blocking collectives  90.2 us (46%)
  starting transfers between devices  45 us (23%)
  Pallas kernels  14.4 us (7%)
  between operations  13.9 us (7%)
  local copies, waits for them, and re-layouts  12.4 us (6%)
  waiting for transfers between devices  9.66 us (5%)
  other arithmetic  5.44 us (3%)
  matrix products  2.57 us (1%)
    all_to_all x3, blocking collectives, swapped(): lax.all_to_all(pieces, axis, 0, 0, tiled=True, axis_index_groups=groups)  46 us
    all_gather x1, blocking collectives, on_device(): lax.all_gather(early, 'sp', axis=0, tiled=True, axis_index_groups=FAR_Z)  44.2 us
    ppermute x4, starting transfers between devices, other_core(): return lax.ppermute(shard, 'tp', [(i, i ^ 1) for i in range(2 * NX)])  25.4 us
    ppermute x3, starting transfers between devices, chip_away(): return lax.ppermute(shard, 'tp', pairs)  10.1 us
    pallas_call x2, Pallas kernels, lowered(): pl.pallas_call(kernel, out_shape=jax.ShapeDtypeStruct((half, width), jnp....  7.71 us
    all_to_all x2, starting transfers between devices, swapped(): lax.all_to_all(pieces, axis, 0, 0, tiled=True, axis_index_groups=groups)  7.19 us
    ppermute x4, waiting for transfers between devices, other_core(): return lax.ppermute(shard, 'tp', [(i, i ^ 1) for i in range(2 * NX)])  6.72 us
    pallas_call x1, Pallas kernels, gated(): pl.pallas_call(kernel, out_shape=(jax.ShapeDtypeStruct((2 * half, ff), jn...  6.7 us
  transfers between devices with their start and end apart: 11, of which 5 were waited for; matrix products, arithmetic and copies ran while one was open for 7% of the time, Pallas kernels for 5%

profile of v5, /device:TPU:1, one launch (start us, length us, event | category | flops | bytes accessed | tf_op | source)
XLA Modules:
  0.0 193.6 jit_solution(4873055166934686986)
XLA Ops:
  6.5 0.0 copy-start
  6.5 0.0 all-gather.2.cloned.1.call-start
  6.6 0.8 slice.82
  7.4 0.9 concatenate.35
  8.3 11.1 %all_to_all.25 = bf16[4,32,1472]{2,1,0:T(8,128)(2,1)} all-to-all(bf16[4,32,1472]{2,1,0:T(8,128)(2,1)S(1)} %broadcast_in_dim.27), channel_id=1, replica_groups={{0,8,16,24},{32,40,48,56},{64,72,80,88},{96,104,112,120},{128,136,144,1..., dimensions={0} | all-to-all | bytes 753664 | tf_op jit(solution)/shard_map/all_to_all | solution.py:31
  19.5 0.0 all-gather.2.cloned.1.call-update
  19.5 0.7 slice.63
  20.2 0.7 slice.64
  20.9 0.7 add_convert_fusion.3
  21.6 0.1 broadcast_in_dim.23
  21.7 2.2 %collective-permute-start = (bf16[136,128]{0,1:T(8,128)(2,1)S(1)}, bf16[136,128]{0,1:T(8,128)(2,1)S(1)}, u32[]{:S(2)}, u32[]{:S(2)}) collective-permute-start(bf16[136,128]{0,1:T(8,128)(2,1)S(1)} %pad_maximum_fusion.2), channel_id=1, source_target_pairs={{0,8},{8,16},{16,24},{24,32},{32,40},{40,48},{48,56},{56,64},{64,7... | collective-permute-start | bytes 104456 | tf_op jit(solution)/shard_map/ppermute | solution.py:23
  24.0 0.0 copy-done.4
  24.1 0.1 reshape.144
  24.2 1.0 collective-permute-done
  25.3 0.1 add_reduce_fusion
  25.5 0.2 compare_and_fusion
  25.7 0.4 fusion.30
  26.1 0.1 broadcast_maximum_fusion
  26.1 0.2 fusion.3
  26.3 0.1 exponential_add_fusion
  26.4 0.3 fusion.2
  26.7 0.1 copy.21
  26.8 0.5 convolution_convert_fusion
  27.3 8.9 %collective-permute-start.1 = (bf16[256,2048]{1,0:T(8,128)(2,1)S(1)}, bf16[256,2048]{1,0:T(8,128)(2,1)S(1)}, u32[]{:S(2)}, u32[]{:S(2)}) collective-permute-start(bf16[256,2048]{1,0:T(8,128)(2,1)S(1)} %convolution_convert_fusion), channel_id=1, source_target_pairs={{0,1},{1,0},{2,3},{3,2},{4,5},{5,4},{6,7},{7,6},{8,9},{9,8},{10,11... | collective-permute-start | bytes 3145736 | tf_op jit(solution)/shard_map/ppermute | solution.py:27
  36.3 0.0 copy-start.6
  36.3 2.2 %collective-permute-done.1 = bf16[256,2048]{1,0:T(8,128)(2,1)S(1)} collective-permute-done((bf16[256,2048]{1,0:T(8,128)(2,1)S(1)}, bf16[256,2048]{1,0:T(8,128)(2,1)S(1)}, u32[]{:S(2)}, u32[]{:S(2)}) %collective-permute-start.1) | collective-permute-done | bytes 1048608 | tf_op jit(solution)/shard_map/ppermute | solution.py:27
  38.5 1.4 add_convert_fusion.1
  39.9 3.5 %all-to-all-start = ((bf16[4,64,2048]{2,1,0:T(8,128)(2,1)}), bf16[4,64,2048]{2,1,0:T(8,128)(2,1)S(1)}, u32[]{:S(2)}, u32[]{:S(2)}) async-start(bf16[4,64,2048]{2,1,0:T(8,128)(2,1)} %bitcast.12), calls=%async_computation | async-start | bytes 2097152 | tf_op jit(solution)/shard_map/all_to_all | solution.py:31
  43.5 44.2 %all_gather.6 = bf16[512,640]{1,0:T(8,128)(2,1)S(1)} all-gather(bf16[32,640]{1,0:T(8,128)(2,1)S(1)} %slice.78), channel_id=1, replica_groups={{0,32,64,96,128,160,192,224,256,288,320,352,384,416,448,480},{8,40,72,1..., dimensions={0}, use_global_device_ids=true | all-gather | bytes 696320 | tf_op jit(solution)/shard_map/all_gather | solution.py:245
  87.7 0.0 all-to-all-done
  87.7 1.8 broadcast_in_dim.26
  89.4 0.2 convert_reduce_fusion.1
  89.6 1.1 fusion.4
  90.8 0.9 constant_dynamic-update-slice_fusion.5
  91.7 3.3 %collective-permute-start.2 = (bf16[64,2048]{1,0:T(8,128)(2,1)}, bf16[64,2048]{1,0:T(8,128)(2,1)}, u32[]{:S(2)}, u32[]{:S(2)}) collective-permute-start(bf16[64,2048]{1,0:T(8,128)(2,1)} %get-tuple-element.16), channel_id=1, source_target_pairs={{0,2},{1,3},{2,4},{3,5},{4,6},{5,7},{6,0},{7,1},{8,10},{9,11},{10,... | collective-permute-start | bytes 786440 | tf_op jit(solution)/shard_map/ppermute | solution.py:40
  95.0 3.7 %all-to-all-start.2 = ((bf16[4,512,640]{2,1,0:T(8,128)(2,1)}), bf16[4,512,640]{2,1,0:T(8,128)(2,1)S(1)}, u32[]{:S(2)}, u32[]{:S(2)}) async-start(bf16[4,512,640]{2,1,0:T(8,128)(2,1)} %broadcast_in_dim.26), calls=%async_computation.2 | async-start | bytes 5242880 | tf_op jit(solution)/shard_map/all_to_all | solution.py:31
  98.7 3.2 %collective-permute-start.3 = (bf16[64,2048]{1,0:T(8,128)(2,1)}, bf16[64,2048]{1,0:T(8,128)(2,1)}, u32[]{:S(2)}, u32[]{:S(2)}) collective-permute-start(bf16[64,2048]{1,0:T(8,128)(2,1)} %get-tuple-element.16), channel_id=1, source_target_pairs={{0,6},{1,7},{2,0},{3,1},{4,2},{5,3},{6,4},{7,5},{8,14},{9,15},{10,... | collective-permute-start | bytes 786440 | tf_op jit(solution)/shard_map/ppermute | solution.py:40
  101.9 3.6 %collective-permute-start.4 = (bf16[64,2048]{1,0:T(8,128)(2,1)}, bf16[64,2048]{1,0:T(8,128)(2,1)S(1)}, u32[]{:S(2)}, u32[]{:S(2)}) collective-permute-start(bf16[64,2048]{1,0:T(8,128)(2,1)} %get-tuple-element.16), channel_id=1, source_target_pairs={{0,4},{1,5},{2,6},{3,7},{4,0},{5,1},{6,2},{7,3},{8,12},{9,13},{10,... | collective-permute-start | bytes 786440 | tf_op jit(solution)/shard_map/ppermute | solution.py:40
  105.6 0.0 collective-permute-done.2
  105.6 1.7 constant_dynamic-update-slice_fusion.4
  107.2 0.0 collective-permute-done.3
  107.2 1.7 constant_dynamic-update-slice_fusion.3
  108.9 1.9 collective-permute-done.4
  110.8 0.7 constant_dynamic-update-slice_fusion.2.mine_ref
  111.5 8.4 %collective-permute-start.5 = (bf16[256,2048]{1,0:T(8,128)(2,1)}, bf16[256,2048]{1,0:T(8,128)(2,1)}, u32[]{:S(2)}, u32[]{:S(2)}) collective-permute-start(bf16[256,2048]{1,0:T(8,128)(2,1)} %constant_dynamic-update-slice_fusion.2.mine_ref), channel_id=1, source_target_pairs={{0,1},{1,0},{2,3},{3,2},{4,5},{5,4},{6,7},{7,6},{8,9},{9,8},{10,11... | collective-permute-start | bytes 3145736 | tf_op jit(solution)/shard_map/ppermute | solution.py:27
  119.9 2.6 %collective-permute-done.5.theirs_ref = bf16[256,2048]{1,0:T(8,128)(2,1)} collective-permute-done((bf16[256,2048]{1,0:T(8,128)(2,1)}, bf16[256,2048]{1,0:T(8,128)(2,1)}, u32[]{:S(2)}, u32[]{:S(2)}) %collective-permute-start.5) | collective-permute-done | bytes 1048608 | tf_op jit(solution)/shard_map/ppermute | solution.py:27
  122.5 6.7 %gated.1 = (bf16[512,704]{1,0:T(8,128)(2,1)}, bf16[2048,64]{1,0:T(8,128)(2,1)}) custom-call(bf16[256,2048]{1,0:T(8,128)(2,1)} %constant_dynamic-update-slice_fusion.2.mine_ref, bf16[256,2048]{1,0:T(8,128)(2,1)} %collective-permute-done.5.theirs_ref, bf16[2048,1472]{1,0:T(8,128)(2,1)} %all-gather.2.cloned.1.call-done.far_ref), custom_call_target="tpu_custom_call" | custom-call | tf_op jit(solution)/shard_map/gated/pallas_call | solution.py:148
  129.2 0.0 all-to-all-done.2
  129.3 1.5 copy-done.1
  130.8 3.8 %lowered.3 = bf16[256,2048]{1,0:T(8,128)(2,1)} custom-call(bf16[512,704]{1,0:T(8,128)(2,1)} %get-tuple-element.12.hidden_ref, bf16[4,16,32,640]{3,2,1,0:T(8,128)(2,1)} %bitcast.63, bf16[2048,64]{1,0:T(8,128)(2,1)} %get-tuple-element.14.late_ref), custom_call_target="tpu_custom_call" | custom-call | tf_op jit(solution)/shard_map/lowered/pallas_call | solution.py:197
  134.6 4.2 %collective-permute-start.6 = (bf16[256,2048]{1,0:T(8,128)(2,1)}, bf16[256,2048]{1,0:T(8,128)(2,1)S(1)}, u32[]{:S(2)}, u32[]{:S(2)}) collective-permute-start(bf16[256,2048]{1,0:T(8,128)(2,1)} %lowered.3), channel_id=1, source_target_pairs={{0,1},{1,0},{2,3},{3,2},{4,5},{5,4},{6,7},{7,6},{8,9},{9,8},{10,11... | collective-permute-start | bytes 3145736 | tf_op jit(solution)/shard_map/ppermute | solution.py:27
  138.8 3.9 %lowered.2 = bf16[256,2048]{1,0:T(8,128)(2,1)} custom-call(bf16[512,704]{1,0:T(8,128)(2,1)} %get-tuple-element.12.hidden_ref, bf16[4,16,32,640]{3,2,1,0:T(8,128)(2,1)} %bitcast.64, bf16[2048,64]{1,0:T(8,128)(2,1)} %get-tuple-element.14.late_ref), custom_call_target="tpu_custom_call" | custom-call | tf_op jit(solution)/shard_map/lowered/pallas_call | solution.py:197
  142.7 0.0 collective-permute-done.6
  142.7 1.6 add_convert_fusion
  144.3 18.4 %all_to_all.26 = bf16[4,64,2048]{2,1,0:T(8,128)(2,1)S(1)} all-to-all(bf16[4,64,2048]{2,1,0:T(8,128)(2,1)S(1)} %bitcast.65), channel_id=1, replica_groups={{0,2,4,6},{1,3,5,7},{8,10,12,14},{9,11,13,15},{16,18,20,22},{17,19,21,2..., dimensions={0} | all-to-all | bytes 2097152 | tf_op jit(solution)/shard_map/all_to_all | solution.py:31
  162.7 0.2 convert_reduce_fusion
  162.9 0.1 broadcast_in_dim.28
  163.1 16.5 %all_to_all.27 = bf16[4,64,2048]{2,1,0:T(8,128)(2,1)S(1)} all-to-all(bf16[4,64,2048]{2,1,0:T(8,128)(2,1)S(1)} %broadcast_in_dim.28), channel_id=1, replica_groups={{0,2,4,6},{1,3,5,7},{8,10,12,14},{9,11,13,15},{16,18,20,22},{17,19,21,2..., dimensions={0} | all-to-all | bytes 2097152 | tf_op jit(solution)/shard_map/all_to_all | solution.py:31
  179.5 3.9 %collective-permute-start.7 = (bf16[256,2048]{1,0:T(8,128)(2,1)S(1)}, bf16[256,2048]{1,0:T(8,128)(2,1)S(1)}, u32[]{:S(2)}, u32[]{:S(2)}) collective-permute-start(bf16[256,2048]{1,0:T(8,128)(2,1)S(1)} %bitcast.66), channel_id=1, source_target_pairs={{0,1},{1,0},{2,3},{3,2},{4,5},{5,4},{6,7},{7,6},{8,9},{9,8},{10,11... | collective-permute-start | bytes 3145736 | tf_op jit(solution)/shard_map/ppermute | solution.py:27
  183.4 0.2 broadcast_in_dim.22
  183.7 0.1 constant_dynamic-update-slice_fusion.1
  183.8 0.0 copy-start.2
  183.8 1.9 collective-permute-done.7
  185.7 1.0 constant_dynamic-update-slice_fusion
  (33 shorter events, 0.3 us)
Async XLA Ops:
  6.5 20.3 %copy-start = (bf16[128,2048]{1,0:T(8,128)(2,1)S(1)}, bf16[128,2048]{1,0:T(8,128)(2,1)}, u32[]{:S(2)}) copy-start(bf16[128,2048]{1,0:T(8,128)(2,1)} %param.17) | copy-start | bytes 1572868
  6.5 17.4 %copy-start.3 = (bf16[512,64]{0,1:T(8,128)(2,1)S(1)}, bf16[512,64]{0,1:T(8,128)(2,1)}, u32[]{:S(2)}) copy-start(bf16[512,64]{0,1:T(8,128)(2,1)} %param.12) | copy-start | bytes 196612
  6.5 17.4 %copy-start.4 = (bf16[512,64]{0,1:T(8,128)(2,1)S(1)}, bf16[512,64]{0,1:T(8,128)(2,1)}, u32[]{:S(2)}) copy-start(bf16[512,64]{0,1:T(8,128)(2,1)} %param.13) | copy-start | bytes 196612
  6.5 18.9 %copy-start.7 = (s32[512]{0:T(512)S(1)}, s32[512]{0:T(512)}, u32[]{:S(2)}) copy-start(s32[512]{0:T(512)} %param.14) | copy-start | bytes 6148
  6.5 17.5 %copy-start.5 = (bf16[512,128]{1,0:T(8,128)(2,1)S(1)}, bf16[512,128]{1,0:T(8,128)(2,1)}, u32[]{:S(2)}) copy-start(bf16[512,128]{1,0:T(8,128)(2,1)} %param.11) | copy-start | bytes 393220
  6.5 116.0 %all-gather.2.cloned.1.call-start = ((), (), s32[]{:S(2)}) async-start(), calls=%async_computation.5 | async-start | bytes 6684672 | tf_op jit(solution)/shard_map/all_gather | solution.py:234
  19.5 6.6 %copy-start.9 = (f32[2]{0:T(128)S(1)}, f32[2]{0:T(128)}, u32[]{:S(2)}) copy-start(f32[2]{0:T(128)} %param.15) | copy-start | bytes 28
  21.7 3.5 %collective-permute-start = (bf16[136,128]{0,1:T(8,128)(2,1)S(1)}, bf16[136,128]{0,1:T(8,128)(2,1)S(1)}, u32[]{:S(2)}, u32[]{:S(2)}) collective-permute-start(bf16[136,128]{0,1:T(8,128)(2,1)S(1)} %pad_maximum_fusion.2), channel_id=1, source_target_pairs={{0,8},{8,16},{16,24},{24,32},{32,40},{40,48},{48,56},{56,64},{64,7... | collective-permute-start | bytes 104456 | tf_op jit(solution)/shard_map/ppermute | solution.py:23
  27.3 11.2 %collective-permute-start.1 = (bf16[256,2048]{1,0:T(8,128)(2,1)S(1)}, bf16[256,2048]{1,0:T(8,128)(2,1)S(1)}, u32[]{:S(2)}, u32[]{:S(2)}) collective-permute-start(bf16[256,2048]{1,0:T(8,128)(2,1)S(1)} %convolution_convert_fusion), channel_id=1, source_target_pairs={{0,1},{1,0},{2,3},{3,2},{4,5},{5,4},{6,7},{7,6},{8,9},{9,8},{10,11... | collective-permute-start | bytes 3145736 | tf_op jit(solution)/shard_map/ppermute | solution.py:27
  36.3 7.2 %copy-start.6 = (bf16[704,32]{0,1:T(8,128)(2,1)S(1)}, bf16[704,32]{0,1:T(8,128)(2,1)}, u32[]{:S(2)}) copy-start(bf16[704,32]{0,1:T(8,128)(2,1)} %param.21) | copy-start | bytes 135172
  39.9 47.7 %all-to-all-start = ((bf16[4,64,2048]{2,1,0:T(8,128)(2,1)}), bf16[4,64,2048]{2,1,0:T(8,128)(2,1)S(1)}, u32[]{:S(2)}, u32[]{:S(2)}) async-start(bf16[4,64,2048]{2,1,0:T(8,128)(2,1)} %bitcast.12), calls=%async_computation | async-start | bytes 2097152 | tf_op jit(solution)/shard_map/all_to_all | solution.py:31
  89.4 1.3 copy-start.8
  91.7 13.9 %collective-permute-start.2 = (bf16[64,2048]{1,0:T(8,128)(2,1)}, bf16[64,2048]{1,0:T(8,128)(2,1)}, u32[]{:S(2)}, u32[]{:S(2)}) collective-permute-start(bf16[64,2048]{1,0:T(8,128)(2,1)} %get-tuple-element.16), channel_id=1, source_target_pairs={{0,2},{1,3},{2,4},{3,5},{4,6},{5,7},{6,0},{7,1},{8,10},{9,11},{10,... | collective-permute-start | bytes 786440 | tf_op jit(solution)/shard_map/ppermute | solution.py:40
  95.0 34.3 %all-to-all-start.2 = ((bf16[4,512,640]{2,1,0:T(8,128)(2,1)}), bf16[4,512,640]{2,1,0:T(8,128)(2,1)S(1)}, u32[]{:S(2)}, u32[]{:S(2)}) async-start(bf16[4,512,640]{2,1,0:T(8,128)(2,1)} %broadcast_in_dim.26), calls=%async_computation.2 | async-start | bytes 5242880 | tf_op jit(solution)/shard_map/all_to_all | solution.py:31
  98.7 8.6 %collective-permute-start.3 = (bf16[64,2048]{1,0:T(8,128)(2,1)}, bf16[64,2048]{1,0:T(8,128)(2,1)}, u32[]{:S(2)}, u32[]{:S(2)}) collective-permute-start(bf16[64,2048]{1,0:T(8,128)(2,1)} %get-tuple-element.16), channel_id=1, source_target_pairs={{0,6},{1,7},{2,0},{3,1},{4,2},{5,3},{6,4},{7,5},{8,14},{9,15},{10,... | collective-permute-start | bytes 786440 | tf_op jit(solution)/shard_map/ppermute | solution.py:40
  101.9 8.9 %collective-permute-start.4 = (bf16[64,2048]{1,0:T(8,128)(2,1)}, bf16[64,2048]{1,0:T(8,128)(2,1)S(1)}, u32[]{:S(2)}, u32[]{:S(2)}) collective-permute-start(bf16[64,2048]{1,0:T(8,128)(2,1)} %get-tuple-element.16), channel_id=1, source_target_pairs={{0,4},{1,5},{2,6},{3,7},{4,0},{5,1},{6,2},{7,3},{8,12},{9,13},{10,... | collective-permute-start | bytes 786440 | tf_op jit(solution)/shard_map/ppermute | solution.py:40
  111.5 11.0 %collective-permute-start.5 = (bf16[256,2048]{1,0:T(8,128)(2,1)}, bf16[256,2048]{1,0:T(8,128)(2,1)}, u32[]{:S(2)}, u32[]{:S(2)}) collective-permute-start(bf16[256,2048]{1,0:T(8,128)(2,1)} %constant_dynamic-update-slice_fusion.2.mine_ref), channel_id=1, source_target_pairs={{0,1},{1,0},{2,3},{3,2},{4,5},{5,4},{6,7},{7,6},{8,9},{9,8},{10,11... | collective-permute-start | bytes 3145736 | tf_op jit(solution)/shard_map/ppermute | solution.py:27
  129.2 1.5 copy-start.1
  134.6 8.1 %collective-permute-start.6 = (bf16[256,2048]{1,0:T(8,128)(2,1)}, bf16[256,2048]{1,0:T(8,128)(2,1)S(1)}, u32[]{:S(2)}, u32[]{:S(2)}) collective-permute-start(bf16[256,2048]{1,0:T(8,128)(2,1)} %lowered.3), channel_id=1, source_target_pairs={{0,1},{1,0},{2,3},{3,2},{4,5},{5,4},{6,7},{7,6},{8,9},{9,8},{10,11... | collective-permute-start | bytes 3145736 | tf_op jit(solution)/shard_map/ppermute | solution.py:27
  179.5 6.2 %collective-permute-start.7 = (bf16[256,2048]{1,0:T(8,128)(2,1)S(1)}, bf16[256,2048]{1,0:T(8,128)(2,1)S(1)}, u32[]{:S(2)}, u32[]{:S(2)}) collective-permute-start(bf16[256,2048]{1,0:T(8,128)(2,1)S(1)} %bitcast.66), channel_id=1, source_target_pairs={{0,1},{1,0},{2,3},{3,2},{4,5},{5,4},{6,7},{7,6},{8,9},{9,8},{10,11... | collective-permute-start | bytes 3145736 | tf_op jit(solution)/shard_map/ppermute | solution.py:27
  183.8 1.9 copy-start.2
Sparse Core Ops, SparseCore 0:
  19.6 94.6 all-gather.1

commit v6 on v3

--- a/solution.py
+++ b/solution.py
@@ -95,6 +95,17 @@
         "nhgqk,nkhd->nqhgd", weights, value_band, preferred_element_type=jnp.float32
     )
     return attended.astype(jnp.bfloat16).reshape(local_rows, queries.shape[1])
+
+
+def side_by_side(arrays):
+    whole = sum(a.shape[1] for a in arrays)
+    low = jnp.array(-jnp.inf, arrays[0].dtype)
+    at, joined = 0, None
+    for a in arrays:
+        padded = lax.pad(a, low, ((0, 0, 0), (at, whole - at - a.shape[1], 0)))
+        joined = padded if joined is None else jnp.maximum(joined, padded)
+        at += a.shape[1]
+    return joined
 
 
 def pair_sum_of(theirs, mine):
@@ -126,26 +137,21 @@
     ff = w_gate.shape[1]
 
     turned = w_down.T
-    near = copies(jnp.concatenate([w_gate, w_up, turned[:, EARLY:]], axis=1), "sp", FAR_Y)
+    near = copies(side_by_side([w_gate, w_up, turned[:, EARLY:]]), "sp", FAR_Y)
     near = near.reshape(-1, near.shape[2])
     far = lax.all_gather(near, "sp", axis=0, tiled=True, axis_index_groups=FAR_Z)
 
     attended = attend(queries, key_rows, values, doc_ids, sink_logits)
-    at_mine = lax.dynamic_slice_in_dim(attended, core * half, half, 0)
-    at_theirs = lax.dynamic_slice_in_dim(attended, (1 - core) * half, half, 0)
-    pair_sum = pair_sum_of(
-        jnp.dot(at_theirs, out_weight, preferred_element_type=jnp.float32).astype(jnp.bfloat16),
-        jnp.dot(at_mine, out_weight, preferred_element_type=jnp.float32),
-    )
-    pieces = to_owners(pair_sum)
-    early, _ = lax.optimization_barrier((turned[:, :EARLY], pair_sum))
+    mixed = jnp.dot(attended, out_weight, preferred_element_type=jnp.float32).astype(jnp.bfloat16)
+    pieces = lax.all_to_all(mixed.reshape(2 * NX, share, width), "tp", 0, 0, tiled=True)
+    early, _ = lax.optimization_barrier((turned[:, :EARLY], mixed))
     column = lax.all_gather(early, "sp", axis=0, tiled=True, axis_index_groups=FAR_Z)
     spread = jnp.broadcast_to(column[None], (NY, *column.shape))
     spread, pieces = lax.optimization_barrier((spread, pieces))
     down = swapped(spread, "sp", FAR_Y)
     down = jnp.swapaxes(down.reshape(NY, NZ, -1, EARLY), 0, 1).reshape(width, EARLY)
     mixed_sum = pieces.astype(jnp.float32).sum(axis=0)
-    base_rows = lax.dynamic_slice_in_dim(residual, core * half + chip * share, share, 0)
+    base_rows = lax.dynamic_slice_in_dim(residual, lax.axis_index("tp") * share, share, 0)
     stream = (base_rows.astype(jnp.float32) + mixed_sum).astype(jnp.bfloat16)
     normed = rms_norm(stream, norm_gain).astype(jnp.bfloat16)
     normed = all_chips_rows(normed, chip)
@@ -169,9 +175,10 @@
     finished = (stream.astype(jnp.float32) + mlp_total).astype(jnp.bfloat16)
     mine = copies(finished, "tp", FAR_X).reshape(half, width)
     theirs = other_core(mine)
-    whole = jnp.zeros((rows, width), jnp.bfloat16)
-    whole = lax.dynamic_update_slice_in_dim(whole, mine, core * half, 0)
-    return lax.dynamic_update_slice_in_dim(whole, theirs, (1 - core) * half, 0)
+    whole = jnp.zeros((NX, 2, share, width), jnp.bfloat16)
+    for part, at in ((mine, core), (theirs, 1 - core)):
+        whole = lax.dynamic_update_slice_in_dim(whole, part.reshape(NX, 1, share, width), at, 1)
+    return whole.reshape(rows, width)
 
 
 def solution(mesh):

time: 196 us -> 192 us (0.980)
  starting transfers between devices: 48.1 us -> 45 us
    all_to_all x0 -> x1, starting transfers between devices: none -> 10.7 us  [on_device(): lax.all_to_all(mixed.reshape(2 * NX, share, width), 'tp', 0, 0, tiled=True)]
    ppermute x4 -> x3, starting transfers between devices: 28.3 us -> 18.9 us  [other_core(): return lax.ppermute(shard, 'tp', [(i, i ^ 1) for i in range(2 * NX)])]
    all_to_all x2 -> x1, starting transfers between devices: 7.14 us -> 3.63 us  [swapped(): lax.all_to_all(pieces, axis, 0, 0, tiled=True, axis_index_groups=groups)]
    ppermute x4 -> x3, waiting for transfers between devices: 4.68 us -> 2.44 us  [other_core(): return lax.ppermute(shard, 'tp', [(i, i ^ 1) for i in range(2 * NX)])]
    all_to_all x2 -> x1, waiting for transfers between devices: 8.18 us -> 9.18 us  [swapped(): lax.all_to_all(pieces, axis, 0, 0, tiled=True, axis_index_groups=groups)]
  transfers between devices with their start and end apart: 11 -> 10, of which waited for: 6 -> 5; matrix products, arithmetic and copies ran while one was open for 8% -> 8% of each run, Pallas kernels for 0% -> 0%
where the time goes in v6:
time: 192 us
  blocking collectives  86.8 us (45%)
  starting transfers between devices  45 us (23%)
  waiting for transfers between devices  15.2 us (8%)
  matrix products  14.1 us (7%)
  between operations  13.9 us (7%)
  local copies, waits for them, and re-layouts  11.9 us (6%)
  other arithmetic  4.77 us (2%)
    all_to_all x3, blocking collectives, swapped(): lax.all_to_all(pieces, axis, 0, 0, tiled=True, axis_index_groups=groups)  44.2 us
    all_gather x1, blocking collectives, on_device(): lax.all_gather(early, 'sp', axis=0, tiled=True, axis_index_groups=FAR_Z)  42.6 us
    ppermute x3, starting transfers between devices, other_core(): return lax.ppermute(shard, 'tp', [(i, i ^ 1) for i in range(2 * NX)])  18.9 us
    all_to_all x1, starting transfers between devices, on_device(): lax.all_to_all(mixed.reshape(2 * NX, share, width), 'tp', 0, 0, tiled=True)  10.7 us
    ppermute x3, starting transfers between devices, chip_away(): return lax.ppermute(shard, 'tp', pairs)  9.59 us
    all_to_all x1, waiting for transfers between devices, swapped(): lax.all_to_all(pieces, axis, 0, 0, tiled=True, axis_index_groups=groups)  9.18 us
    dot_general x1, matrix products, on_device(): acts = jnp.dot(normed, far[:, :2 * ff], preferred_element_type=jnp.float32)  6.39 us
    dot_general x4, matrix products, turned_dot(): lax.dot_general(left, right, (((1,), (1,)), ((), ())), preferred_element_...  4.93 us
  transfers between devices with their start and end apart: 10, of which 5 were waited for; matrix products, arithmetic and copies ran while one was open for 8% of the time, Pallas kernels for 0%

profile of v6, /device:TPU:1, one launch (start us, length us, event | category | flops | bytes accessed | tf_op | source)
XLA Modules:
  0.0 191.7 jit_solution(14899751937402731801)
XLA Ops:
  6.6 0.0 all-gather.2.cloned.1.call-start
  6.6 0.8 slice.120
  7.4 0.9 pad_maximum_fusion
  8.4 11.3 %all_to_all.25 = bf16[4,32,1600]{2,1,0:T(8,128)(2,1)} all-to-all(bf16[4,32,1600]{2,1,0:T(8,128)(2,1)S(1)} %broadcast_in_dim.30), channel_id=1, replica_groups={{0,8,16,24},{32,40,48,56},{64,72,80,88},{96,104,112,120},{128,136,144,1..., dimensions={0} | all-to-all | bytes 819200 | tf_op jit(solution)/shard_map/all_to_all | solution.py:27
  19.7 0.0 all-gather.2.cloned.1.call-update
  19.7 0.1 broadcast_in_dim.25
  19.9 2.2 %collective-permute-start = (bf16[136,128]{0,1:T(8,128)(2,1)S(1)}, bf16[136,128]{0,1:T(8,128)(2,1)S(1)}, u32[]{:S(2)}, u32[]{:S(2)}) collective-permute-start(bf16[136,128]{0,1:T(8,128)(2,1)S(1)} %pad_maximum_fusion.3), channel_id=1, source_target_pairs={{0,8},{8,16},{16,24},{24,32},{32,40},{40,48},{48,56},{56,64},{64,7... | collective-permute-start | bytes 104456 | tf_op jit(solution)/shard_map/ppermute | solution.py:19
  22.2 0.0 copy-done.5
  22.2 0.1 reshape.156
  22.3 1.0 collective-permute-done
  23.5 0.1 add_reduce_fusion
  23.6 0.2 compare_and_fusion
  23.8 0.4 fusion.43
  24.2 0.1 broadcast_maximum_fusion
  24.3 0.2 fusion.10
  24.4 0.1 exponential_add_fusion
  24.5 0.3 fusion.9
  24.8 0.1 copy.29
  24.9 2.1 %convolution_convert_fusion = bf16[512,2048]{1,0:T(8,128)(2,1)} fusion(bf16[128,2048]{1,0:T(8,128)(2,1)S(1)} %copy-done, bf16[16,8,4,128]{3,2,1,0:T(4,128)(2,1)S(1)} %bitcast.79), kind=kOutput, calls=%fused_computation.3 | convolution fusion | flops 269484032 | bytes 2752512 | tf_op jit(solution)/shard_map/dot_general | solution.py:145
  27.0 10.7 %all-to-all-start = ((bf16[8,64,2048]{2,1,0:T(8,128)(2,1)}), bf16[8,64,2048]{2,1,0:T(8,128)(2,1)S(1)}, u32[]{:S(2)}, u32[]{:S(2)}) async-start(bf16[8,64,2048]{2,1,0:T(8,128)(2,1)} %bitcast.73), calls=%async_computation | async-start | bytes 4194304 | tf_op jit(solution)/shard_map/all_to_all | solution.py:146
  37.7 0.0 copy-done.6
  37.7 42.6 %all_gather.6 = bf16[512,512]{1,0:T(8,128)(2,1)S(1)} all-gather(bf16[32,512]{1,0:T(8,128)(2,1)S(1)} %slice.116), channel_id=1, replica_groups={{0,32,64,96,128,160,192,224,256,288,320,352,384,416,448,480},{8,40,72,1..., dimensions={0}, use_global_device_ids=true | all-gather | bytes 557056 | tf_op jit(solution)/shard_map/all_gather | solution.py:148
  80.3 0.0 all-to-all-done
  80.3 1.5 broadcast_in_dim.28
  81.8 0.3 convert_reduce_fusion
  82.1 1.1 fusion.15
  83.3 1.1 broadcast_in_dim.29
  84.4 0.0 copy-done.8
  84.4 0.9 constant_dynamic-update-slice_fusion.4
  85.3 2.8 %collective-permute-start.1 = (bf16[64,2048]{1,0:T(8,128)(2,1)}, bf16[64,2048]{1,0:T(8,128)(2,1)S(1)}, u32[]{:S(2)}, u32[]{:S(2)}) collective-permute-start(bf16[64,2048]{1,0:T(8,128)(2,1)} %get-tuple-element.12), channel_id=1, source_target_pairs={{0,2},{1,3},{2,4},{3,5},{4,6},{5,7},{6,0},{7,1},{8,10},{9,11},{10,... | collective-permute-start | bytes 786440 | tf_op jit(solution)/shard_map/ppermute | solution.py:36
  88.1 3.7 %collective-permute-start.2 = (bf16[64,2048]{1,0:T(8,128)(2,1)}, bf16[64,2048]{1,0:T(8,128)(2,1)S(1)}, u32[]{:S(2)}, u32[]{:S(2)}) collective-permute-start(bf16[64,2048]{1,0:T(8,128)(2,1)} %get-tuple-element.12), channel_id=1, source_target_pairs={{0,6},{1,7},{2,0},{3,1},{4,2},{5,3},{6,4},{7,5},{8,14},{9,15},{10,... | collective-permute-start | bytes 786440 | tf_op jit(solution)/shard_map/ppermute | solution.py:36
  91.9 3.1 %collective-permute-start.3 = (bf16[64,2048]{1,0:T(8,128)(2,1)}, bf16[64,2048]{1,0:T(8,128)(2,1)}, u32[]{:S(2)}, u32[]{:S(2)}) collective-permute-start(bf16[64,2048]{1,0:T(8,128)(2,1)} %get-tuple-element.12), channel_id=1, source_target_pairs={{0,4},{1,5},{2,6},{3,7},{4,0},{5,1},{6,2},{7,3},{8,12},{9,13},{10,... | collective-permute-start | bytes 786440 | tf_op jit(solution)/shard_map/ppermute | solution.py:36
  95.0 3.6 %all-to-all-start.2 = ((bf16[4,512,512]{2,1,0:T(8,128)(2,1)}), bf16[4,512,512]{2,1,0:T(8,128)(2,1)S(1)}, u32[]{:S(2)}, u32[]{:S(2)}) async-start(bf16[4,512,512]{2,1,0:T(8,128)(2,1)} %broadcast_in_dim.28), calls=%async_computation.2 | async-start | bytes 4194304 | tf_op jit(solution)/shard_map/all_to_all | solution.py:27
  98.6 0.0 collective-permute-done.1
  98.6 0.7 constant_dynamic-update-slice_fusion.3
  99.4 0.0 collective-permute-done.2
  99.4 0.7 constant_dynamic-update-slice_fusion.2
  100.1 2.5 %collective-permute-done.3 = bf16[64,2048]{1,0:T(8,128)(2,1)} collective-permute-done((bf16[64,2048]{1,0:T(8,128)(2,1)}, bf16[64,2048]{1,0:T(8,128)(2,1)}, u32[]{:S(2)}, u32[]{:S(2)}) %collective-permute-start.3) | collective-permute-done | bytes 262176 | tf_op jit(solution)/shard_map/ppermute | solution.py:36
  102.6 1.7 constant_dynamic-update-slice_fusion.1
  104.3 5.7 %collective-permute-start.4 = (bf16[256,2048]{1,0:T(8,128)(2,1)}, bf16[256,2048]{1,0:T(8,128)(2,1)}, u32[]{:S(2)}, u32[]{:S(2)}) collective-permute-start(bf16[256,2048]{1,0:T(8,128)(2,1)} %constant_dynamic-update-slice_fusion.1), channel_id=1, source_target_pairs={{0,1},{1,0},{2,3},{3,2},{4,5},{5,4},{6,7},{7,6},{8,9},{9,8},{10,11... | collective-permute-start | bytes 3145736 | tf_op jit(solution)/shard_map/ppermute | solution.py:23
  110.0 9.2 %all-to-all-done.2 = bf16[4,512,512]{2,1,0:T(8,128)(2,1)S(1)} async-done(((bf16[4,512,512]{2,1,0:T(8,128)(2,1)}), bf16[4,512,512]{2,1,0:T(8,128)(2,1)S(1)}, u32[]{:S(2)}, u32[]{:S(2)}) %all-to-all-start.2) | async-done | bytes 2097184 | tf_op jit(solution)/shard_map/all_to_all | solution.py:27
  119.2 1.3 copy-done.1
  120.5 1.7 copy.30
  122.3 0.0 collective-permute-done.4
  122.3 0.0 all-gather.2.cloned.1.call-done
  122.3 6.4 %fusion = f32[512,1408]{1,0:T(8,128)S(1)} fusion(bf16[2048,1600]{1,0:T(8,128)(2,1)} %all-gather.2.cloned.1.call-done, bf16[256,2048]{1,0:T(8,128)(2,1)} %collective-permute-done.4, bf16[256,2048]{1,0:T(8,128)(2,1)} %constant_dynamic-update-slice_fusion.1), kind=kOutput, calls=%fused_computation | convolution fusion | flops 2956984320 | bytes 10747904 | tf_op jit(solution)/shard_map/dot_general | solution.py:160
  128.7 0.5 fusion.6
  129.2 1.7 fusion.11
  130.9 0.8 fusion.2
  131.7 8.6 %collective-permute-start.5 = (bf16[256,2048]{1,0:T(8,128)(2,1)S(1)}, bf16[256,2048]{1,0:T(8,128)(2,1)S(1)}, u32[]{:S(2)}, u32[]{:S(2)}) collective-permute-start(bf16[256,2048]{1,0:T(8,128)(2,1)S(1)} %fusion.2), channel_id=1, source_target_pairs={{0,1},{1,0},{2,3},{3,2},{4,5},{5,4},{6,7},{7,6},{8,9},{9,8},{10,11... | collective-permute-start | bytes 3145736 | tf_op jit(solution)/shard_map/ppermute | solution.py:23
  140.3 1.7 fusion.13
  142.0 0.6 collective-permute-done.5
  142.5 0.8 add_convert_fusion
  143.3 17.1 %all_to_all.26 = bf16[4,64,2048]{2,1,0:T(8,128)(2,1)S(1)} all-to-all(bf16[4,64,2048]{2,1,0:T(8,128)(2,1)S(1)} %bitcast.75), channel_id=1, replica_groups={{0,2,4,6},{1,3,5,7},{8,10,12,14},{9,11,13,15},{16,18,20,22},{17,19,21,2..., dimensions={0} | all-to-all | bytes 2097152 | tf_op jit(solution)/shard_map/all_to_all | solution.py:27
  160.4 0.2 convert_reduce_fusion.1
  160.6 0.1 broadcast_in_dim.31
  160.7 15.8 %all_to_all.27 = bf16[4,64,2048]{2,1,0:T(8,128)(2,1)S(1)} all-to-all(bf16[4,64,2048]{2,1,0:T(8,128)(2,1)S(1)} %broadcast_in_dim.31), channel_id=1, replica_groups={{0,2,4,6},{1,3,5,7},{8,10,12,14},{9,11,13,15},{16,18,20,22},{17,19,21,2..., dimensions={0} | all-to-all | bytes 2097152 | tf_op jit(solution)/shard_map/all_to_all | solution.py:27
  176.5 4.6 %collective-permute-start.6 = (bf16[256,2048]{1,0:T(8,128)(2,1)S(1)}, bf16[256,2048]{1,0:T(8,128)(2,1)S(1)}, u32[]{:S(2)}, u32[]{:S(2)}) collective-permute-start(bf16[256,2048]{1,0:T(8,128)(2,1)S(1)} %bitcast.76), channel_id=1, source_target_pairs={{0,1},{1,0},{2,3},{3,2},{4,5},{5,4},{6,7},{7,6},{8,9},{9,8},{10,11... | collective-permute-start | bytes 3145736 | tf_op jit(solution)/shard_map/ppermute | solution.py:23
  181.1 0.2 broadcast_in_dim.24
  181.4 0.1 bitcast_dynamic-update-slice_fusion
  181.5 1.9 collective-permute-done.6
  183.4 0.1 constant_dynamic-update-slice_fusion
  183.5 0.0 copy-start.2
  183.5 1.3 copy-done.2
  (35 shorter events, 0.3 us)
Async XLA Ops:
  6.5 18.4 %copy-start = (bf16[128,2048]{1,0:T(8,128)(2,1)S(1)}, bf16[128,2048]{1,0:T(8,128)(2,1)}, u32[]{:S(2)}) copy-start(bf16[128,2048]{1,0:T(8,128)(2,1)} %param.17) | copy-start | bytes 1572868
  6.5 13.3 %slice-start = ((bf16[512,64]{0,1:T(8,128)(2,1)}), bf16[128,64]{0,1:T(8,128)(2,1)S(1)}, s32[]{:S(2)}) async-start(bf16[512,64]{0,1:T(8,128)(2,1)} %param.12), calls=%async_computation.6 | async-start | bytes 32768 | tf_op jit(solution)/shard_map/slice | solution.py:68
  6.5 15.5 %copy-start.3 = (bf16[512,64]{0,1:T(8,128)(2,1)S(1)}, bf16[512,64]{0,1:T(8,128)(2,1)}, u32[]{:S(2)}) copy-start(bf16[512,64]{0,1:T(8,128)(2,1)} %param.12) | copy-start | bytes 196612
  6.5 13.3 %slice-start.1 = ((bf16[512,64]{0,1:T(8,128)(2,1)}), bf16[128,64]{0,1:T(8,128)(2,1)S(1)}, s32[]{:S(2)}) async-start(bf16[512,64]{0,1:T(8,128)(2,1)} %param.13), calls=%async_computation.7 | async-start | bytes 32768 | tf_op jit(solution)/shard_map/slice | solution.py:68
  6.5 15.6 %copy-start.4 = (bf16[512,64]{0,1:T(8,128)(2,1)S(1)}, bf16[512,64]{0,1:T(8,128)(2,1)}, u32[]{:S(2)}) copy-start(bf16[512,64]{0,1:T(8,128)(2,1)} %param.13) | copy-start | bytes 196612
  6.5 13.2 %copy-start.7 = (s32[512]{0:T(512)S(1)}, s32[512]{0:T(512)}, u32[]{:S(2)}) copy-start(s32[512]{0:T(512)} %param.14) | copy-start | bytes 6148
  6.6 15.6 %copy-start.5 = (bf16[512,128]{1,0:T(8,128)(2,1)S(1)}, bf16[512,128]{1,0:T(8,128)(2,1)}, u32[]{:S(2)}) copy-start(bf16[512,128]{1,0:T(8,128)(2,1)} %param.11) | copy-start | bytes 393220
  6.6 115.7 %all-gather.2.cloned.1.call-start = ((), (), s32[]{:S(2)}) async-start(), calls=%async_computation.5 | async-start | bytes 7241728 | tf_op jit(solution)/shard_map/all_gather | solution.py:142
  19.7 4.5 %copy-start.9 = (f32[2]{0:T(128)S(1)}, f32[2]{0:T(128)}, u32[]{:S(2)}) copy-start(f32[2]{0:T(128)} %param.15) | copy-start | bytes 28
  19.9 3.5 %collective-permute-start = (bf16[136,128]{0,1:T(8,128)(2,1)S(1)}, bf16[136,128]{0,1:T(8,128)(2,1)S(1)}, u32[]{:S(2)}, u32[]{:S(2)}) collective-permute-start(bf16[136,128]{0,1:T(8,128)(2,1)S(1)} %pad_maximum_fusion.3), channel_id=1, source_target_pairs={{0,8},{8,16},{16,24},{24,32},{32,40},{40,48},{48,56},{56,64},{64,7... | collective-permute-start | bytes 104456 | tf_op jit(solution)/shard_map/ppermute | solution.py:19
  27.0 10.7 %copy-start.6 = (bf16[704,32]{0,1:T(8,128)(2,1)S(1)}, bf16[704,32]{0,1:T(8,128)(2,1)}, u32[]{:S(2)}) copy-start(bf16[704,32]{0,1:T(8,128)(2,1)} %param.21) | copy-start | bytes 135172
  27.0 53.3 %all-to-all-start = ((bf16[8,64,2048]{2,1,0:T(8,128)(2,1)}), bf16[8,64,2048]{2,1,0:T(8,128)(2,1)S(1)}, u32[]{:S(2)}, u32[]{:S(2)}) async-start(bf16[8,64,2048]{2,1,0:T(8,128)(2,1)} %bitcast.73), calls=%async_computation | async-start | bytes 4194304 | tf_op jit(solution)/shard_map/all_to_all | solution.py:146
  81.8 2.6 %copy-start.8 = (f32[2048]{0:T(1024)S(1)}, f32[2048]{0:T(1024)}, u32[]{:S(2)}) copy-start(f32[2048]{0:T(1024)} %param.18) | copy-start | bytes 24580
  85.3 13.3 %collective-permute-start.1 = (bf16[64,2048]{1,0:T(8,128)(2,1)}, bf16[64,2048]{1,0:T(8,128)(2,1)S(1)}, u32[]{:S(2)}, u32[]{:S(2)}) collective-permute-start(bf16[64,2048]{1,0:T(8,128)(2,1)} %get-tuple-element.12), channel_id=1, source_target_pairs={{0,2},{1,3},{2,4},{3,5},{4,6},{5,7},{6,0},{7,1},{8,10},{9,11},{10,... | collective-permute-start | bytes 786440 | tf_op jit(solution)/shard_map/ppermute | solution.py:36
  88.1 11.2 %collective-permute-start.2 = (bf16[64,2048]{1,0:T(8,128)(2,1)}, bf16[64,2048]{1,0:T(8,128)(2,1)S(1)}, u32[]{:S(2)}, u32[]{:S(2)}) collective-permute-start(bf16[64,2048]{1,0:T(8,128)(2,1)} %get-tuple-element.12), channel_id=1, source_target_pairs={{0,6},{1,7},{2,0},{3,1},{4,2},{5,3},{6,4},{7,5},{8,14},{9,15},{10,... | collective-permute-start | bytes 786440 | tf_op jit(solution)/shard_map/ppermute | solution.py:36
  91.9 10.7 %collective-permute-start.3 = (bf16[64,2048]{1,0:T(8,128)(2,1)}, bf16[64,2048]{1,0:T(8,128)(2,1)}, u32[]{:S(2)}, u32[]{:S(2)}) collective-permute-start(bf16[64,2048]{1,0:T(8,128)(2,1)} %get-tuple-element.12), channel_id=1, source_target_pairs={{0,4},{1,5},{2,6},{3,7},{4,0},{5,1},{6,2},{7,3},{8,12},{9,13},{10,... | collective-permute-start | bytes 786440 | tf_op jit(solution)/shard_map/ppermute | solution.py:36
  95.0 24.2 %all-to-all-start.2 = ((bf16[4,512,512]{2,1,0:T(8,128)(2,1)}), bf16[4,512,512]{2,1,0:T(8,128)(2,1)S(1)}, u32[]{:S(2)}, u32[]{:S(2)}) async-start(bf16[4,512,512]{2,1,0:T(8,128)(2,1)} %broadcast_in_dim.28), calls=%async_computation.2 | async-start | bytes 4194304 | tf_op jit(solution)/shard_map/all_to_all | solution.py:27
  104.3 18.0 %collective-permute-start.4 = (bf16[256,2048]{1,0:T(8,128)(2,1)}, bf16[256,2048]{1,0:T(8,128)(2,1)}, u32[]{:S(2)}, u32[]{:S(2)}) collective-permute-start(bf16[256,2048]{1,0:T(8,128)(2,1)} %constant_dynamic-update-slice_fusion.1), channel_id=1, source_target_pairs={{0,1},{1,0},{2,3},{3,2},{4,5},{5,4},{6,7},{7,6},{8,9},{9,8},{10,11... | collective-permute-start | bytes 3145736 | tf_op jit(solution)/shard_map/ppermute | solution.py:23
  119.2 1.3 copy-start.1
  131.7 10.9 %collective-permute-start.5 = (bf16[256,2048]{1,0:T(8,128)(2,1)S(1)}, bf16[256,2048]{1,0:T(8,128)(2,1)S(1)}, u32[]{:S(2)}, u32[]{:S(2)}) collective-permute-start(bf16[256,2048]{1,0:T(8,128)(2,1)S(1)} %fusion.2), channel_id=1, source_target_pairs={{0,1},{1,0},{2,3},{3,2},{4,5},{5,4},{6,7},{7,6},{8,9},{9,8},{10,11... | collective-permute-start | bytes 3145736 | tf_op jit(solution)/shard_map/ppermute | solution.py:23
  176.5 6.8 %collective-permute-start.6 = (bf16[256,2048]{1,0:T(8,128)(2,1)S(1)}, bf16[256,2048]{1,0:T(8,128)(2,1)S(1)}, u32[]{:S(2)}, u32[]{:S(2)}) collective-permute-start(bf16[256,2048]{1,0:T(8,128)(2,1)S(1)} %bitcast.76), channel_id=1, source_target_pairs={{0,1},{1,0},{2,3},{3,2},{4,5},{5,4},{6,7},{7,6},{8,9},{9,8},{10,11... | collective-permute-start | bytes 3145736 | tf_op jit(solution)/shard_map/ppermute | solution.py:23
  183.5 1.3 copy-start.2
Sparse Core Ops, SparseCore 0:
  19.8 100.0 all-gather.1

commit v7 on v3

--- a/solution.py
+++ b/solution.py
@@ -95,6 +95,21 @@
         "nhgqk,nkhd->nqhgd", weights, value_band, preferred_element_type=jnp.float32
     )
     return attended.astype(jnp.bfloat16).reshape(local_rows, queries.shape[1])
+
+
+def side_by_side(w_gate, w_up, turned):
+    ff = w_gate.shape[1]
+    whole = 3 * ff - EARLY
+    zero = jnp.zeros((), w_gate.dtype)
+    column = lax.broadcasted_iota(jnp.int32, (w_gate.shape[0], whole), 1)
+
+    def placed(array, at):
+        return lax.pad(array, zero, ((0, 0, 0), (at, whole - at - ff, 0)))
+
+    last = placed(turned, whole - ff)
+    return jnp.where(
+        column < ff, placed(w_gate, 0), jnp.where(column < 2 * ff, placed(w_up, ff), last)
+    )
 
 
 def pair_sum_of(theirs, mine):
@@ -126,19 +141,15 @@
     ff = w_gate.shape[1]
 
     turned = w_down.T
-    near = copies(jnp.concatenate([w_gate, w_up, turned[:, EARLY:]], axis=1), "sp", FAR_Y)
+    near = copies(side_by_side(w_gate, w_up, turned), "sp", FAR_Y)
     near = near.reshape(-1, near.shape[2])
     far = lax.all_gather(near, "sp", axis=0, tiled=True, axis_index_groups=FAR_Z)
 
     attended = attend(queries, key_rows, values, doc_ids, sink_logits)
-    at_mine = lax.dynamic_slice_in_dim(attended, core * half, half, 0)
-    at_theirs = lax.dynamic_slice_in_dim(attended, (1 - core) * half, half, 0)
-    pair_sum = pair_sum_of(
-        jnp.dot(at_theirs, out_weight, preferred_element_type=jnp.float32).astype(jnp.bfloat16),
-        jnp.dot(at_mine, out_weight, preferred_element_type=jnp.float32),
-    )
-    pieces = to_owners(pair_sum)
-    early, _ = lax.optimization_barrier((turned[:, :EARLY], pair_sum))
+    attended = jnp.swapaxes(attended.reshape(2, NX, share, -1), 0, 1).reshape(rows, -1)
+    mixed = jnp.dot(attended, out_weight, preferred_element_type=jnp.float32).astype(jnp.bfloat16)
+    pieces = lax.all_to_all(mixed.reshape(2 * NX, share, width), "tp", 0, 0, tiled=True)
+    early, _ = lax.optimization_barrier((turned[:, :EARLY], mixed))
     column = lax.all_gather(early, "sp", axis=0, tiled=True, axis_index_groups=FAR_Z)
     spread = jnp.broadcast_to(column[None], (NY, *column.shape))
     spread, pieces = lax.optimization_barrier((spread, pieces))
@@ -151,6 +162,7 @@
     normed = all_chips_rows(normed, chip)
     normed = jnp.concatenate([normed, other_core(normed)], axis=0)
 
+    late = far[:, 2 * ff :]
     acts = jnp.dot(normed, far[:, : 2 * ff], preferred_element_type=jnp.float32)
     hidden = (jax.nn.silu(acts[:, :ff]) * acts[:, ff:]).astype(jnp.bfloat16)
 
@@ -159,7 +171,6 @@
             left, right, (((1,), (1,)), ((), ())), preferred_element_type=jnp.float32
         )
 
-    late = far[:, 2 * ff :]
 
     def through(part):
         return turned_dot(part[:, EARLY:], late) + turned_dot(part[:, :EARLY], down)

time: 196 us -> 191 us (0.974)
  starting transfers between devices: 48.1 us -> 45.5 us
    all_to_all x0 -> x1, starting transfers between devices: none -> 10.7 us  [on_device(): lax.all_to_all(mixed.reshape(2 * NX, share, width), 'tp', 0, 0, tiled=True)]
    ppermute x4 -> x3, starting transfers between devices: 28.3 us -> 18.9 us  [other_core(): return lax.ppermute(shard, 'tp', [(i, i ^ 1) for i in range(2 * NX)])]
    all_to_all x2 -> x1, starting transfers between devices: 7.14 us -> 3.62 us  [swapped(): lax.all_to_all(pieces, axis, 0, 0, tiled=True, axis_index_groups=groups)]
    ppermute x4 -> x3, waiting for transfers between devices: 4.68 us -> 2.43 us  [other_core(): return lax.ppermute(shard, 'tp', [(i, i ^ 1) for i in range(2 * NX)])]
    all_to_all x2 -> x1, waiting for transfers between devices: 8.18 us -> 9.05 us  [swapped(): lax.all_to_all(pieces, axis, 0, 0, tiled=True, axis_index_groups=groups)]
  transfers between devices with their start and end apart: 11 -> 10, of which waited for: 6 -> 5; matrix products, arithmetic and copies ran while one was open for 8% -> 8% of each run, Pallas kernels for 0% -> 0%
where the time goes in v7:
time: 191 us
  blocking collectives  86.1 us (45%)
  starting transfers between devices  45.5 us (24%)
  waiting for transfers between devices  15.2 us (8%)
  matrix products  14 us (7%)
  between operations  13.9 us (7%)
  local copies, waits for them, and re-layouts  10.9 us (6%)
  other arithmetic  4.91 us (3%)
    all_to_all x3, blocking collectives, swapped(): lax.all_to_all(pieces, axis, 0, 0, tiled=True, axis_index_groups=groups)  43.9 us
    all_gather x1, blocking collectives, on_device(): lax.all_gather(early, 'sp', axis=0, tiled=True, axis_index_groups=FAR_Z)  42.2 us
    ppermute x3, starting transfers between devices, other_core(): return lax.ppermute(shard, 'tp', [(i, i ^ 1) for i in range(2 * NX)])  18.9 us
    all_to_all x1, starting transfers between devices, on_device(): lax.all_to_all(mixed.reshape(2 * NX, share, width), 'tp', 0, 0, tiled=True)  10.7 us
    ppermute x3, starting transfers between devices, chip_away(): return lax.ppermute(shard, 'tp', pairs)  10.1 us
    all_to_all x1, waiting for transfers between devices, swapped(): lax.all_to_all(pieces, axis, 0, 0, tiled=True, axis_index_groups=groups)  9.05 us
    dot_general x1, matrix products, on_device(): acts = jnp.dot(normed, far[:, :2 * ff], preferred_element_type=jnp.float32)  6.39 us
    dot_general x4, matrix products, turned_dot(): lax.dot_general(left, right, (((1,), (1,)), ((), ())), preferred_element_...  4.93 us
  transfers between devices with their start and end apart: 10, of which 5 were waited for; matrix products, arithmetic and copies ran while one was open for 8% of the time, Pallas kernels for 0%

profile of v7, /device:TPU:1, one launch (start us, length us, event | category | flops | bytes accessed | tf_op | source)
XLA Modules:
  0.0 190.5 jit_solution(15429474104596766412)
XLA Ops:
  6.6 0.0 all-gather.2.cloned.1.call-start
  6.6 1.0 select_select_fusion
  7.7 11.3 %all_to_all.25 = bf16[4,32,1600]{2,1,0:T(8,128)(2,1)} all-to-all(bf16[4,32,1600]{2,1,0:T(8,128)(2,1)S(1)} %broadcast_in_dim.30), channel_id=1, replica_groups={{0,8,16,24},{32,40,48,56},{64,72,80,88},{96,104,112,120},{128,136,144,1..., dimensions={0} | all-to-all | bytes 819200 | tf_op jit(solution)/shard_map/all_to_all | solution.py:27
  19.0 0.0 all-gather.2.cloned.1.call-update
  19.1 0.0 copy-done.7
  19.1 0.1 broadcast_in_dim.25
  19.2 2.2 %collective-permute-start = (bf16[136,128]{0,1:T(8,128)(2,1)S(1)}, bf16[136,128]{0,1:T(8,128)(2,1)S(1)}, u32[]{:S(2)}, u32[]{:S(2)}) collective-permute-start(bf16[136,128]{0,1:T(8,128)(2,1)S(1)} %pad_maximum_fusion.2), channel_id=1, source_target_pairs={{0,8},{8,16},{16,24},{24,32},{32,40},{40,48},{48,56},{56,64},{64,7... | collective-permute-start | bytes 104456 | tf_op jit(solution)/shard_map/ppermute | solution.py:19
  21.5 0.0 copy-done.4
  21.5 0.1 reshape.148
  21.7 1.0 collective-permute-done
  22.8 0.1 add_reduce_fusion
  22.9 0.2 compare_and_fusion
  23.2 0.4 fusion.41
  23.5 0.0 copy-done.9
  23.5 0.1 broadcast_maximum_fusion
  23.6 0.2 fusion.10
  23.8 0.1 exponential_add_fusion
  23.8 0.3 fusion.9
  24.2 0.2 copy.30
  24.3 0.1 reshape_reshape.3
  24.5 0.0 copy-done
  24.5 2.0 %convolution_convert_fusion = bf16[512,2048]{1,0:T(8,128)(2,1)} fusion(bf16[512,128]{1,0:T(8,128)(2,1)S(1)} %bitcast.74, bf16[128,2048]{1,0:T(8,128)(2,1)S(1)} %copy-done), kind=kOutput, calls=%fused_computation.3 | convolution fusion | flops 269484032 | bytes 2752512 | tf_op jit(solution)/shard_map/dot_general | solution.py:150
  26.5 10.7 %all-to-all-start = ((bf16[8,64,2048]{2,1,0:T(8,128)(2,1)}), bf16[8,64,2048]{2,1,0:T(8,128)(2,1)S(1)}, u32[]{:S(2)}, u32[]{:S(2)}) async-start(bf16[8,64,2048]{2,1,0:T(8,128)(2,1)} %bitcast.67), calls=%async_computation | async-start | bytes 4194304 | tf_op jit(solution)/shard_map/all_to_all | solution.py:151
  37.2 42.2 %all_gather.6 = bf16[512,512]{1,0:T(8,128)(2,1)S(1)} all-gather(bf16[32,512]{1,0:T(8,128)(2,1)S(1)} %slice.112), channel_id=1, replica_groups={{0,32,64,96,128,160,192,224,256,288,320,352,384,416,448,480},{8,40,72,1..., dimensions={0}, use_global_device_ids=true | all-gather | bytes 557056 | tf_op jit(solution)/shard_map/all_gather | solution.py:153
  79.4 0.0 all-to-all-done
  79.4 1.5 broadcast_in_dim.28
  80.9 0.3 convert_reduce_fusion
  81.3 1.1 fusion.15
  82.4 1.1 broadcast_in_dim.29
  83.5 0.9 constant_dynamic-update-slice_fusion.5
  84.5 3.3 %collective-permute-start.1 = (bf16[64,2048]{1,0:T(8,128)(2,1)}, bf16[64,2048]{1,0:T(8,128)(2,1)S(1)}, u32[]{:S(2)}, u32[]{:S(2)}) collective-permute-start(bf16[64,2048]{1,0:T(8,128)(2,1)} %get-tuple-element.12), channel_id=1, source_target_pairs={{0,2},{1,3},{2,4},{3,5},{4,6},{5,7},{6,0},{7,1},{8,10},{9,11},{10,... | collective-permute-start | bytes 786440 | tf_op jit(solution)/shard_map/ppermute | solution.py:36
  87.8 3.2 %collective-permute-start.2 = (bf16[64,2048]{1,0:T(8,128)(2,1)}, bf16[64,2048]{1,0:T(8,128)(2,1)S(1)}, u32[]{:S(2)}, u32[]{:S(2)}) collective-permute-start(bf16[64,2048]{1,0:T(8,128)(2,1)} %get-tuple-element.12), channel_id=1, source_target_pairs={{0,6},{1,7},{2,0},{3,1},{4,2},{5,3},{6,4},{7,5},{8,14},{9,15},{10,... | collective-permute-start | bytes 786440 | tf_op jit(solution)/shard_map/ppermute | solution.py:36
  91.0 3.6 %collective-permute-start.3 = (bf16[64,2048]{1,0:T(8,128)(2,1)}, bf16[64,2048]{1,0:T(8,128)(2,1)}, u32[]{:S(2)}, u32[]{:S(2)}) collective-permute-start(bf16[64,2048]{1,0:T(8,128)(2,1)} %get-tuple-element.12), channel_id=1, source_target_pairs={{0,4},{1,5},{2,6},{3,7},{4,0},{5,1},{6,2},{7,3},{8,12},{9,13},{10,... | collective-permute-start | bytes 786440 | tf_op jit(solution)/shard_map/ppermute | solution.py:36
  94.6 3.6 %all-to-all-start.2 = ((bf16[4,512,512]{2,1,0:T(8,128)(2,1)}), bf16[4,512,512]{2,1,0:T(8,128)(2,1)S(1)}, u32[]{:S(2)}, u32[]{:S(2)}) async-start(bf16[4,512,512]{2,1,0:T(8,128)(2,1)} %broadcast_in_dim.28), calls=%async_computation.2 | async-start | bytes 4194304 | tf_op jit(solution)/shard_map/all_to_all | solution.py:27
  98.3 0.0 collective-permute-done.1
  98.3 0.7 constant_dynamic-update-slice_fusion.4
  99.0 0.0 collective-permute-done.2
  99.0 0.7 constant_dynamic-update-slice_fusion.3
  99.7 2.6 %collective-permute-done.3 = bf16[64,2048]{1,0:T(8,128)(2,1)} collective-permute-done((bf16[64,2048]{1,0:T(8,128)(2,1)}, bf16[64,2048]{1,0:T(8,128)(2,1)}, u32[]{:S(2)}, u32[]{:S(2)}) %collective-permute-start.3) | collective-permute-done | bytes 262176 | tf_op jit(solution)/shard_map/ppermute | solution.py:36
  102.3 1.7 constant_dynamic-update-slice_fusion.2
  104.0 5.7 %collective-permute-start.4 = (bf16[256,2048]{1,0:T(8,128)(2,1)}, bf16[256,2048]{1,0:T(8,128)(2,1)}, u32[]{:S(2)}, u32[]{:S(2)}) collective-permute-start(bf16[256,2048]{1,0:T(8,128)(2,1)} %constant_dynamic-update-slice_fusion.2), channel_id=1, source_target_pairs={{0,1},{1,0},{2,3},{3,2},{4,5},{5,4},{6,7},{7,6},{8,9},{9,8},{10,11... | collective-permute-start | bytes 3145736 | tf_op jit(solution)/shard_map/ppermute | solution.py:23
  109.7 9.1 %all-to-all-done.2 = bf16[4,512,512]{2,1,0:T(8,128)(2,1)S(1)} async-done(((bf16[4,512,512]{2,1,0:T(8,128)(2,1)}), bf16[4,512,512]{2,1,0:T(8,128)(2,1)S(1)}, u32[]{:S(2)}, u32[]{:S(2)}) %all-to-all-start.2) | async-done | bytes 2097184 | tf_op jit(solution)/shard_map/all_to_all | solution.py:27
  118.8 1.3 copy-done.1
  120.1 1.7 copy.32
  121.8 0.0 collective-permute-done.4
  121.8 0.0 all-gather.2.cloned.1.call-done
  121.9 6.4 %fusion = f32[512,1408]{1,0:T(8,128)S(1)} fusion(bf16[2048,1600]{1,0:T(8,128)(2,1)} %all-gather.2.cloned.1.call-done, bf16[256,2048]{1,0:T(8,128)(2,1)} %collective-permute-done.4, bf16[256,2048]{1,0:T(8,128)(2,1)} %constant_dynamic-update-slice_fusion.2), kind=kOutput, calls=%fused_computation | convolution fusion | flops 2956984320 | bytes 10747904 | tf_op jit(solution)/shard_map/dot_general | solution.py:166
  128.3 0.5 fusion.6
  128.8 1.7 fusion.11
  130.5 0.8 fusion.2
  131.2 8.6 %collective-permute-start.5 = (bf16[256,2048]{1,0:T(8,128)(2,1)S(1)}, bf16[256,2048]{1,0:T(8,128)(2,1)S(1)}, u32[]{:S(2)}, u32[]{:S(2)}) collective-permute-start(bf16[256,2048]{1,0:T(8,128)(2,1)S(1)} %fusion.2), channel_id=1, source_target_pairs={{0,1},{1,0},{2,3},{3,2},{4,5},{5,4},{6,7},{7,6},{8,9},{9,8},{10,11... | collective-permute-start | bytes 3145736 | tf_op jit(solution)/shard_map/ppermute | solution.py:23
  139.9 1.7 fusion.13
  141.6 0.6 collective-permute-done.5
  142.2 0.8 add_convert_fusion
  142.9 16.7 %all_to_all.26 = bf16[4,64,2048]{2,1,0:T(8,128)(2,1)S(1)} all-to-all(bf16[4,64,2048]{2,1,0:T(8,128)(2,1)S(1)} %bitcast.69), channel_id=1, replica_groups={{0,2,4,6},{1,3,5,7},{8,10,12,14},{9,11,13,15},{16,18,20,22},{17,19,21,2..., dimensions={0} | all-to-all | bytes 2097152 | tf_op jit(solution)/shard_map/all_to_all | solution.py:27
  159.7 0.2 convert_reduce_fusion.1
  159.9 0.1 broadcast_in_dim.31
  160.0 15.9 %all_to_all.27 = bf16[4,64,2048]{2,1,0:T(8,128)(2,1)S(1)} all-to-all(bf16[4,64,2048]{2,1,0:T(8,128)(2,1)S(1)} %broadcast_in_dim.31), channel_id=1, replica_groups={{0,2,4,6},{1,3,5,7},{8,10,12,14},{9,11,13,15},{16,18,20,22},{17,19,21,2..., dimensions={0} | all-to-all | bytes 2097152 | tf_op jit(solution)/shard_map/all_to_all | solution.py:27
  175.9 4.5 %collective-permute-start.6 = (bf16[256,2048]{1,0:T(8,128)(2,1)S(1)}, bf16[256,2048]{1,0:T(8,128)(2,1)S(1)}, u32[]{:S(2)}, u32[]{:S(2)}) collective-permute-start(bf16[256,2048]{1,0:T(8,128)(2,1)S(1)} %bitcast.70), channel_id=1, source_target_pairs={{0,1},{1,0},{2,3},{3,2},{4,5},{5,4},{6,7},{7,6},{8,9},{9,8},{10,11... | collective-permute-start | bytes 3145736 | tf_op jit(solution)/shard_map/ppermute | solution.py:23
  180.4 0.2 broadcast_in_dim.24
  180.6 0.1 constant_dynamic-update-slice_fusion.1
  180.8 0.0 copy-start.2
  180.8 1.9 collective-permute-done.6
  182.6 1.0 constant_dynamic-update-slice_fusion
  (37 shorter events, 0.3 us)
Async XLA Ops:
  6.5 18.0 %copy-start = (bf16[128,2048]{1,0:T(8,128)(2,1)S(1)}, bf16[128,2048]{1,0:T(8,128)(2,1)}, u32[]{:S(2)}) copy-start(bf16[128,2048]{1,0:T(8,128)(2,1)} %param.17) | copy-start | bytes 1572868
  6.5 12.6 %slice-start = ((bf16[512,64]{0,1:T(8,128)(2,1)}), bf16[128,64]{0,1:T(8,128)(2,1)S(1)}, s32[]{:S(2)}) async-start(bf16[512,64]{0,1:T(8,128)(2,1)} %param.12), calls=%async_computation.6 | async-start | bytes 32768 | tf_op jit(solution)/shard_map/slice | solution.py:68
  6.5 14.9 %copy-start.3 = (bf16[512,64]{0,1:T(8,128)(2,1)S(1)}, bf16[512,64]{0,1:T(8,128)(2,1)}, u32[]{:S(2)}) copy-start(bf16[512,64]{0,1:T(8,128)(2,1)} %param.12) | copy-start | bytes 196612
  6.5 12.6 %slice-start.1 = ((bf16[512,64]{0,1:T(8,128)(2,1)}), bf16[128,64]{0,1:T(8,128)(2,1)S(1)}, s32[]{:S(2)}) async-start(bf16[512,64]{0,1:T(8,128)(2,1)} %param.13), calls=%async_computation.7 | async-start | bytes 32768 | tf_op jit(solution)/shard_map/slice | solution.py:68
  6.5 14.9 %copy-start.4 = (bf16[512,64]{0,1:T(8,128)(2,1)S(1)}, bf16[512,64]{0,1:T(8,128)(2,1)}, u32[]{:S(2)}) copy-start(bf16[512,64]{0,1:T(8,128)(2,1)} %param.13) | copy-start | bytes 196612
  6.5 12.5 %copy-start.7 = (s32[512]{0:T(512)S(1)}, s32[512]{0:T(512)}, u32[]{:S(2)}) copy-start(s32[512]{0:T(512)} %param.14) | copy-start | bytes 6148
  6.6 15.0 %copy-start.6 = (bf16[512,128]{1,0:T(8,128)(2,1)S(1)}, bf16[512,128]{1,0:T(8,128)(2,1)}, u32[]{:S(2)}) copy-start(bf16[512,128]{1,0:T(8,128)(2,1)} %param.11) | copy-start | bytes 393220
  6.6 115.3 %all-gather.2.cloned.1.call-start = ((), (), s32[]{:S(2)}) async-start(), calls=%async_computation.5 | async-start | bytes 7241728 | tf_op jit(solution)/shard_map/all_gather | solution.py:146
  19.0 4.5 %copy-start.9 = (f32[2]{0:T(128)S(1)}, f32[2]{0:T(128)}, u32[]{:S(2)}) copy-start(f32[2]{0:T(128)} %param.15) | copy-start | bytes 28
  19.2 3.5 %collective-permute-start = (bf16[136,128]{0,1:T(8,128)(2,1)S(1)}, bf16[136,128]{0,1:T(8,128)(2,1)S(1)}, u32[]{:S(2)}, u32[]{:S(2)}) collective-permute-start(bf16[136,128]{0,1:T(8,128)(2,1)S(1)} %pad_maximum_fusion.2), channel_id=1, source_target_pairs={{0,8},{8,16},{16,24},{24,32},{32,40},{40,48},{48,56},{56,64},{64,7... | collective-permute-start | bytes 104456 | tf_op jit(solution)/shard_map/ppermute | solution.py:19
  26.5 10.7 %copy-start.5 = (bf16[704,32]{0,1:T(8,128)(2,1)S(1)}, bf16[704,32]{0,1:T(8,128)(2,1)}, u32[]{:S(2)}) copy-start(bf16[704,32]{0,1:T(8,128)(2,1)} %param.21) | copy-start | bytes 135172
  26.5 52.9 %all-to-all-start = ((bf16[8,64,2048]{2,1,0:T(8,128)(2,1)}), bf16[8,64,2048]{2,1,0:T(8,128)(2,1)S(1)}, u32[]{:S(2)}, u32[]{:S(2)}) async-start(bf16[8,64,2048]{2,1,0:T(8,128)(2,1)} %bitcast.67), calls=%async_computation | async-start | bytes 4194304 | tf_op jit(solution)/shard_map/all_to_all | solution.py:151
  80.9 2.6 %copy-start.8 = (f32[2048]{0:T(1024)S(1)}, f32[2048]{0:T(1024)}, u32[]{:S(2)}) copy-start(f32[2048]{0:T(1024)} %param.18) | copy-start | bytes 24580
  84.5 13.8 %collective-permute-start.1 = (bf16[64,2048]{1,0:T(8,128)(2,1)}, bf16[64,2048]{1,0:T(8,128)(2,1)S(1)}, u32[]{:S(2)}, u32[]{:S(2)}) collective-permute-start(bf16[64,2048]{1,0:T(8,128)(2,1)} %get-tuple-element.12), channel_id=1, source_target_pairs={{0,2},{1,3},{2,4},{3,5},{4,6},{5,7},{6,0},{7,1},{8,10},{9,11},{10,... | collective-permute-start | bytes 786440 | tf_op jit(solution)/shard_map/ppermute | solution.py:36
  87.8 11.2 %collective-permute-start.2 = (bf16[64,2048]{1,0:T(8,128)(2,1)}, bf16[64,2048]{1,0:T(8,128)(2,1)S(1)}, u32[]{:S(2)}, u32[]{:S(2)}) collective-permute-start(bf16[64,2048]{1,0:T(8,128)(2,1)} %get-tuple-element.12), channel_id=1, source_target_pairs={{0,6},{1,7},{2,0},{3,1},{4,2},{5,3},{6,4},{7,5},{8,14},{9,15},{10,... | collective-permute-start | bytes 786440 | tf_op jit(solution)/shard_map/ppermute | solution.py:36
  91.0 11.3 %collective-permute-start.3 = (bf16[64,2048]{1,0:T(8,128)(2,1)}, bf16[64,2048]{1,0:T(8,128)(2,1)}, u32[]{:S(2)}, u32[]{:S(2)}) collective-permute-start(bf16[64,2048]{1,0:T(8,128)(2,1)} %get-tuple-element.12), channel_id=1, source_target_pairs={{0,4},{1,5},{2,6},{3,7},{4,0},{5,1},{6,2},{7,3},{8,12},{9,13},{10,... | collective-permute-start | bytes 786440 | tf_op jit(solution)/shard_map/ppermute | solution.py:36
  94.6 24.1 %all-to-all-start.2 = ((bf16[4,512,512]{2,1,0:T(8,128)(2,1)}), bf16[4,512,512]{2,1,0:T(8,128)(2,1)S(1)}, u32[]{:S(2)}, u32[]{:S(2)}) async-start(bf16[4,512,512]{2,1,0:T(8,128)(2,1)} %broadcast_in_dim.28), calls=%async_computation.2 | async-start | bytes 4194304 | tf_op jit(solution)/shard_map/all_to_all | solution.py:27
  104.0 17.9 %collective-permute-start.4 = (bf16[256,2048]{1,0:T(8,128)(2,1)}, bf16[256,2048]{1,0:T(8,128)(2,1)}, u32[]{:S(2)}, u32[]{:S(2)}) collective-permute-start(bf16[256,2048]{1,0:T(8,128)(2,1)} %constant_dynamic-update-slice_fusion.2), channel_id=1, source_target_pairs={{0,1},{1,0},{2,3},{3,2},{4,5},{5,4},{6,7},{7,6},{8,9},{9,8},{10,11... | collective-permute-start | bytes 3145736 | tf_op jit(solution)/shard_map/ppermute | solution.py:23
  118.8 1.3 copy-start.1
  131.2 10.9 %collective-permute-start.5 = (bf16[256,2048]{1,0:T(8,128)(2,1)S(1)}, bf16[256,2048]{1,0:T(8,128)(2,1)S(1)}, u32[]{:S(2)}, u32[]{:S(2)}) collective-permute-start(bf16[256,2048]{1,0:T(8,128)(2,1)S(1)} %fusion.2), channel_id=1, source_target_pairs={{0,1},{1,0},{2,3},{3,2},{4,5},{5,4},{6,7},{7,6},{8,9},{9,8},{10,11... | collective-permute-start | bytes 3145736 | tf_op jit(solution)/shard_map/ppermute | solution.py:23
  175.9 6.8 %collective-permute-start.6 = (bf16[256,2048]{1,0:T(8,128)(2,1)S(1)}, bf16[256,2048]{1,0:T(8,128)(2,1)S(1)}, u32[]{:S(2)}, u32[]{:S(2)}) collective-permute-start(bf16[256,2048]{1,0:T(8,128)(2,1)S(1)} %bitcast.70), channel_id=1, source_target_pairs={{0,1},{1,0},{2,3},{3,2},{4,5},{5,4},{6,7},{7,6},{8,9},{9,8},{10,11... | collective-permute-start | bytes 3145736 | tf_op jit(solution)/shard_map/ppermute | solution.py:23
  180.8 1.9 copy-start.2
Sparse Core Ops, SparseCore 0:
  19.2 100.0 all-gather.1

commit v8 on v7

--- a/solution.py
+++ b/solution.py
@@ -110,11 +110,6 @@
     return jnp.where(
         column < ff, placed(w_gate, 0), jnp.where(column < 2 * ff, placed(w_up, ff), last)
     )
-
-
-def pair_sum_of(theirs, mine):
-    arrived = other_core(theirs)
-    return (mine + arrived.astype(jnp.float32)).astype(jnp.bfloat16)
 
 
 def to_owners(pair_sum):
@@ -141,8 +136,9 @@
     ff = w_gate.shape[1]
 
     turned = w_down.T
-    near = copies(side_by_side(w_gate, w_up, turned), "sp", FAR_Y)
-    near = near.reshape(-1, near.shape[2])
+    near = lax.all_gather(
+        side_by_side(w_gate, w_up, turned), "sp", axis=0, tiled=True, axis_index_groups=FAR_Y
+    )
     far = lax.all_gather(near, "sp", axis=0, tiled=True, axis_index_groups=FAR_Z)
 
     attended = attend(queries, key_rows, values, doc_ids, sink_logits)
@@ -161,6 +157,7 @@
     normed = rms_norm(stream, norm_gain).astype(jnp.bfloat16)
     normed = all_chips_rows(normed, chip)
     normed = jnp.concatenate([normed, other_core(normed)], axis=0)
+    normed, far, down = lax.optimization_barrier((normed, far, down))
 
     late = far[:, 2 * ff :]
     acts = jnp.dot(normed, far[:, : 2 * ff], preferred_element_type=jnp.float32)
@@ -175,7 +172,9 @@
     def through(part):
         return turned_dot(part[:, EARLY:], late) + turned_dot(part[:, :EARLY], down)
 
-    pair_sum = pair_sum_of(through(hidden[half:]).astype(jnp.bfloat16), through(hidden[:half]))
+    swapped_part = other_core(through(hidden[half:]).astype(jnp.bfloat16))
+    own_part, swapped_part = lax.optimization_barrier((through(hidden[:half]), swapped_part))
+    pair_sum = (own_part + swapped_part.astype(jnp.float32)).astype(jnp.bfloat16)
     mlp_total = to_owners(pair_sum).astype(jnp.float32).sum(axis=0)
     finished = (stream.astype(jnp.float32) + mlp_total).astype(jnp.bfloat16)
     mine = copies(finished, "tp", FAR_X).reshape(half, width)

time: 191 us -> 195 us (1.021)
  waiting for transfers between devices: 15.2 us -> 10.8 us
  local copies, waits for them, and re-layouts: 10.9 us -> 15.1 us
  other arithmetic: 4.91 us -> 8.6 us
    all_gather x0 -> x1, blocking collectives: none -> 12.2 us  [on_device(): lax.all_gather(side_by_side(w_gate, w_up, turned), 'sp', axis=0, tiled=Tr...]
    all_to_all x3 -> x2, blocking collectives: 43.9 us -> 33.7 us  [swapped(): lax.all_to_all(pieces, axis, 0, 0, tiled=True, axis_index_groups=groups)]
    all_to_all x1, waiting for transfers between devices: 9.05 us -> 3.84 us  [swapped(): lax.all_to_all(pieces, axis, 0, 0, tiled=True, axis_index_groups=groups)]
    concatenate x0 -> x1, other arithmetic: none -> 2.8 us  [on_device(): normed = jnp.concatenate([normed, other_core(normed)], axis=0)]
  transfers between devices with their start and end apart: 10 -> 10, of which waited for: 5 -> 4; matrix products, arithmetic and copies ran while one was open for 8% -> 13% of each run, Pallas kernels for 0% -> 0%
where the time goes in v8:
time: 195 us; the launch traced here: 194 us
  blocking collectives  86.6 us (44%)
  starting transfers between devices  45.1 us (23%)
  local copies, waits for them, and re-layouts  15.1 us (8%)
  matrix products  14 us (7%)
  between operations  13.9 us (7%)
  waiting for transfers between devices  10.8 us (6%)
  other arithmetic  8.6 us (4%)
    all_gather x1, blocking collectives, on_device(): lax.all_gather(early, 'sp', axis=0, tiled=True, axis_index_groups=FAR_Z)  40.7 us
    all_to_all x2, blocking collectives, swapped(): lax.all_to_all(pieces, axis, 0, 0, tiled=True, axis_index_groups=groups)  33.7 us
    ppermute x3, starting transfers between devices, other_core(): return lax.ppermute(shard, 'tp', [(i, i ^ 1) for i in range(2 * NX)])  18.3 us
    all_gather x1, blocking collectives, on_device(): lax.all_gather(side_by_side(w_gate, w_up, turned), 'sp', axis=0, tiled=Tr...  12.2 us
    all_to_all x1, starting transfers between devices, on_device(): lax.all_to_all(mixed.reshape(2 * NX, share, width), 'tp', 0, 0, tiled=True)  10.5 us
    ppermute x3, starting transfers between devices, chip_away(): return lax.ppermute(shard, 'tp', pairs)  10.1 us
    dot_general x1, matrix products, on_device(): acts = jnp.dot(normed, far[:, :2 * ff], preferred_element_type=jnp.float32)  6.41 us
    dot_general x4, matrix products, turned_dot(): lax.dot_general(left, right, (((1,), (1,)), ((), ())), preferred_element_...  4.89 us
  transfers between devices with their start and end apart: 10, of which 4 were waited for; matrix products, arithmetic and copies ran while one was open for 13% of the time, Pallas kernels for 0%

profile of v8, /device:TPU:1, one launch (start us, length us, event | category | flops | bytes accessed | tf_op | source)
XLA Modules:
  0.0 194.0 jit_solution(4357653393381383102)
XLA Ops:
  6.5 0.0 all-gather.2.cloned.1.call-start
  6.6 1.0 select_select_fusion
  7.6 12.2 %all_gather.10 = bf16[128,1600]{1,0:T(8,128)(2,1)} all-gather(bf16[32,1600]{1,0:T(8,128)(2,1)S(1)} %select_select_fusion), channel_id=1, replica_groups={{0,8,16,24},{32,40,48,56},{64,72,80,88},{96,104,112,120},{128,136,144,1..., dimensions={0}, use_global_device_ids=true | all-gather | bytes 512000 | tf_op jit(solution)/shard_map/all_gather | solution.py:139
  19.8 0.0 all-gather.2.cloned.1.call-update
  19.8 0.7 slice.90
  20.5 0.7 slice.91
  21.2 0.7 add_convert_fusion.2
  21.9 0.1 broadcast_in_dim.23
  22.0 2.5 %collective-permute-start = (bf16[136,128]{0,1:T(8,128)(2,1)S(1)}, bf16[136,128]{0,1:T(8,128)(2,1)S(1)}, u32[]{:S(2)}, u32[]{:S(2)}) collective-permute-start(bf16[136,128]{0,1:T(8,128)(2,1)S(1)} %pad_maximum_fusion.3), channel_id=1, source_target_pairs={{0,8},{8,16},{16,24},{24,32},{32,40},{40,48},{48,56},{56,64},{64,7... | collective-permute-start | bytes 104456 | tf_op jit(solution)/shard_map/ppermute | solution.py:19
  24.6 0.9 copy_bitcast_fusion
  25.4 0.9 copy_bitcast_fusion.2
  26.3 1.0 reshape.143
  27.4 0.0 collective-permute-done
  27.5 0.1 add_reduce_fusion
  27.6 0.2 compare_and_fusion
  27.9 0.4 fusion.35
  28.2 0.1 broadcast_maximum_fusion
  28.3 0.2 fusion.7
  28.5 0.1 exponential_add_fusion
  28.5 0.3 fusion.6
  28.9 0.2 copy.30
  29.0 0.1 reshape_reshape.3
  29.2 2.0 %convolution_convert_fusion = bf16[512,2048]{1,0:T(8,128)(2,1)} fusion(bf16[512,128]{1,0:T(8,128)(2,1)S(1)} %bitcast.73, bf16[128,2048]{1,0:T(8,128)(2,1)S(1)} %copy-done), kind=kOutput, calls=%fused_computation.3 | convolution fusion | flops 269484032 | bytes 2752512 | tf_op jit(solution)/shard_map/dot_general | solution.py:146
  31.2 10.5 %all-to-all-start = ((bf16[8,64,2048]{2,1,0:T(8,128)(2,1)}), bf16[8,64,2048]{2,1,0:T(8,128)(2,1)S(1)}, u32[]{:S(2)}, u32[]{:S(2)}) async-start(bf16[8,64,2048]{2,1,0:T(8,128)(2,1)} %bitcast.67), calls=%async_computation | async-start | bytes 4194304 | tf_op jit(solution)/shard_map/all_to_all | solution.py:147
  41.8 40.7 %all_gather.9 = bf16[512,512]{1,0:T(8,128)(2,1)S(1)} all-gather(bf16[32,512]{1,0:T(8,128)(2,1)S(1)} %slice.112), channel_id=1, replica_groups={{0,32,64,96,128,160,192,224,256,288,320,352,384,416,448,480},{8,40,72,1..., dimensions={0}, use_global_device_ids=true | all-gather | bytes 557056 | tf_op jit(solution)/shard_map/all_gather | solution.py:149
  82.5 0.0 all-to-all-done
  82.5 1.6 broadcast_in_dim.26
  84.0 0.3 convert_reduce_fusion
  84.4 1.1 fusion.12
  85.5 1.1 broadcast_in_dim.27
  86.6 0.9 constant_dynamic-update-slice_fusion.5
  87.6 3.4 %collective-permute-start.1 = (bf16[64,2048]{1,0:T(8,128)(2,1)}, bf16[64,2048]{1,0:T(8,128)(2,1)S(1)}, u32[]{:S(2)}, u32[]{:S(2)}) collective-permute-start(bf16[64,2048]{1,0:T(8,128)(2,1)} %get-tuple-element.22), channel_id=1, source_target_pairs={{0,2},{1,3},{2,4},{3,5},{4,6},{5,7},{6,0},{7,1},{8,10},{9,11},{10,... | collective-permute-start | bytes 786440 | tf_op jit(solution)/shard_map/ppermute | solution.py:36
  90.9 3.1 %collective-permute-start.2 = (bf16[64,2048]{1,0:T(8,128)(2,1)}, bf16[64,2048]{1,0:T(8,128)(2,1)S(1)}, u32[]{:S(2)}, u32[]{:S(2)}) collective-permute-start(bf16[64,2048]{1,0:T(8,128)(2,1)} %get-tuple-element.22), channel_id=1, source_target_pairs={{0,6},{1,7},{2,0},{3,1},{4,2},{5,3},{6,4},{7,5},{8,14},{9,15},{10,... | collective-permute-start | bytes 786440 | tf_op jit(solution)/shard_map/ppermute | solution.py:36
  94.1 3.6 %collective-permute-start.3 = (bf16[64,2048]{1,0:T(8,128)(2,1)}, bf16[64,2048]{1,0:T(8,128)(2,1)}, u32[]{:S(2)}, u32[]{:S(2)}) collective-permute-start(bf16[64,2048]{1,0:T(8,128)(2,1)} %get-tuple-element.22), channel_id=1, source_target_pairs={{0,4},{1,5},{2,6},{3,7},{4,0},{5,1},{6,2},{7,3},{8,12},{9,13},{10,... | collective-permute-start | bytes 786440 | tf_op jit(solution)/shard_map/ppermute | solution.py:36
  97.8 3.6 %all-to-all-start.1 = ((bf16[4,512,512]{2,1,0:T(8,128)(2,1)}), bf16[4,512,512]{2,1,0:T(8,128)(2,1)S(1)}, u32[]{:S(2)}, u32[]{:S(2)}) async-start(bf16[4,512,512]{2,1,0:T(8,128)(2,1)} %broadcast_in_dim.26), calls=%async_computation.1 | async-start | bytes 4194304 | tf_op jit(solution)/shard_map/all_to_all | solution.py:27
  101.4 0.7 constant_dynamic-update-slice_fusion.4
  102.1 0.7 constant_dynamic-update-slice_fusion.3
  102.9 2.5 %collective-permute-done.3 = bf16[64,2048]{1,0:T(8,128)(2,1)} collective-permute-done((bf16[64,2048]{1,0:T(8,128)(2,1)}, bf16[64,2048]{1,0:T(8,128)(2,1)}, u32[]{:S(2)}, u32[]{:S(2)}) %collective-permute-start.3) | collective-permute-done | bytes 262176 | tf_op jit(solution)/shard_map/ppermute | solution.py:36
  105.4 1.7 constant_dynamic-update-slice_fusion.2
  107.1 5.7 %collective-permute-start.4 = (bf16[256,2048]{1,0:T(8,128)(2,1)}, bf16[256,2048]{1,0:T(8,128)(2,1)S(1)}, u32[]{:S(2)}, u32[]{:S(2)}) collective-permute-start(bf16[256,2048]{1,0:T(8,128)(2,1)} %constant_dynamic-update-slice_fusion.2), channel_id=1, source_target_pairs={{0,1},{1,0},{2,3},{3,2},{4,5},{5,4},{6,7},{7,6},{8,9},{9,8},{10,11... | collective-permute-start | bytes 3145736 | tf_op jit(solution)/shard_map/ppermute | solution.py:23
  112.8 2.5 %collective-permute-done.4 = bf16[256,2048]{1,0:T(8,128)(2,1)S(1)} collective-permute-done((bf16[256,2048]{1,0:T(8,128)(2,1)}, bf16[256,2048]{1,0:T(8,128)(2,1)S(1)}, u32[]{:S(2)}, u32[]{:S(2)}) %collective-permute-start.4) | collective-permute-done | bytes 1048608 | tf_op jit(solution)/shard_map/ppermute | solution.py:23
  115.3 2.8 %pad_maximum_fusion = bf16[512,2048]{1,0:T(8,128)(2,1)} fusion(bf16[256,2048]{1,0:T(8,128)(2,1)S(1)} %collective-permute-done.4, bf16[256,2048]{1,0:T(8,128)(2,1)} %constant_dynamic-update-slice_fusion.2), kind=kLoop, calls=%fused_computation.7 | loop fusion | flops 4194304 | bytes 4194304 | tf_op jit(solution)/shard_map/concatenate | solution.py:159
  118.1 3.8 %all-to-all-done.1 = bf16[4,512,512]{2,1,0:T(8,128)(2,1)S(1)} async-done(((bf16[4,512,512]{2,1,0:T(8,128)(2,1)}), bf16[4,512,512]{2,1,0:T(8,128)(2,1)S(1)}, u32[]{:S(2)}, u32[]{:S(2)}) %all-to-all-start.1) | async-done | bytes 2097184 | tf_op jit(solution)/shard_map/all_to_all | solution.py:27
  121.9 1.4 copy-done.1
  123.3 1.7 copy.32
  125.1 0.0 all-gather.2.cloned.1.call-done
  125.1 6.4 %fusion = f32[512,1408]{1,0:T(8,128)S(1)} fusion(bf16[512,2048]{1,0:T(8,128)(2,1)} %pad_maximum_fusion, bf16[2048,1600]{1,0:T(8,128)(2,1)} %all-gather.2.cloned.1.call-done), kind=kOutput, calls=%fused_computation | convolution fusion | flops 2952790016 | bytes 10747904 | tf_op jit(solution)/shard_map/dot_general | solution.py:163
  131.5 0.5 fusion.3
  132.0 1.7 fusion.8
  133.7 0.7 fusion.2
  134.4 8.7 %collective-permute-start.5 = (bf16[256,2048]{1,0:T(8,128)(2,1)S(1)}, bf16[256,2048]{1,0:T(8,128)(2,1)S(1)}, u32[]{:S(2)}, u32[]{:S(2)}) collective-permute-start(bf16[256,2048]{1,0:T(8,128)(2,1)S(1)} %fusion.2), channel_id=1, source_target_pairs={{0,1},{1,0},{2,3},{3,2},{4,5},{5,4},{6,7},{7,6},{8,9},{9,8},{10,11... | collective-permute-start | bytes 3145736 | tf_op jit(solution)/shard_map/ppermute | solution.py:23
  143.1 1.7 fusion.10
  144.8 0.7 convolution_add_fusion.1
  145.6 0.3 add_convert_fusion
  145.9 17.3 %all_to_all.20 = bf16[4,64,2048]{2,1,0:T(8,128)(2,1)S(1)} all-to-all(bf16[4,64,2048]{2,1,0:T(8,128)(2,1)S(1)} %bitcast.71), channel_id=1, replica_groups={{0,2,4,6},{1,3,5,7},{8,10,12,14},{9,11,13,15},{16,18,20,22},{17,19,21,2..., dimensions={0} | all-to-all | bytes 2097152 | tf_op jit(solution)/shard_map/all_to_all | solution.py:27
  163.2 0.2 convert_reduce_fusion.1
  163.4 0.1 broadcast_in_dim.28
  163.5 16.4 %all_to_all.21 = bf16[4,64,2048]{2,1,0:T(8,128)(2,1)S(1)} all-to-all(bf16[4,64,2048]{2,1,0:T(8,128)(2,1)S(1)} %broadcast_in_dim.28), channel_id=1, replica_groups={{0,2,4,6},{1,3,5,7},{8,10,12,14},{9,11,13,15},{16,18,20,22},{17,19,21,2..., dimensions={0} | all-to-all | bytes 2097152 | tf_op jit(solution)/shard_map/all_to_all | solution.py:27
  179.9 3.9 %collective-permute-start.6 = (bf16[256,2048]{1,0:T(8,128)(2,1)S(1)}, bf16[256,2048]{1,0:T(8,128)(2,1)S(1)}, u32[]{:S(2)}, u32[]{:S(2)}) collective-permute-start(bf16[256,2048]{1,0:T(8,128)(2,1)S(1)} %bitcast.69), channel_id=1, source_target_pairs={{0,1},{1,0},{2,3},{3,2},{4,5},{5,4},{6,7},{7,6},{8,9},{9,8},{10,11... | collective-permute-start | bytes 3145736 | tf_op jit(solution)/shard_map/ppermute | solution.py:23
  183.9 0.2 broadcast_in_dim.22
  184.1 0.1 constant_dynamic-update-slice_fusion.1
  184.3 0.0 copy-start.2
  184.3 1.9 collective-permute-done.6
  186.1 1.0 constant_dynamic-update-slice_fusion
  (34 shorter events, 0.2 us)
Async XLA Ops:
  6.5 22.7 %copy-start = (bf16[128,2048]{1,0:T(8,128)(2,1)S(1)}, bf16[128,2048]{1,0:T(8,128)(2,1)}, u32[]{:S(2)}) copy-start(bf16[128,2048]{1,0:T(8,128)(2,1)} %param.17) | copy-start | bytes 1572868
  6.5 20.9 %copy-start.3 = (bf16[512,64]{0,1:T(8,128)(2,1)S(1)}, bf16[512,64]{0,1:T(8,128)(2,1)}, u32[]{:S(2)}) copy-start(bf16[512,64]{0,1:T(8,128)(2,1)} %param.12) | copy-start | bytes 196612
  6.5 20.9 %copy-start.4 = (bf16[512,64]{0,1:T(8,128)(2,1)S(1)}, bf16[512,64]{0,1:T(8,128)(2,1)}, u32[]{:S(2)}) copy-start(bf16[512,64]{0,1:T(8,128)(2,1)} %param.13) | copy-start | bytes 196612
  6.5 21.1 %copy-start.6 = (s32[512]{0:T(512)S(1)}, s32[512]{0:T(512)}, u32[]{:S(2)}) copy-start(s32[512]{0:T(512)} %param.14) | copy-start | bytes 6148
  6.5 118.5 %all-gather.2.cloned.1.call-start = ((), (), s32[]{:S(2)}) async-start(), calls=%async_computation.4 | async-start | bytes 7241728 | tf_op jit(solution)/shard_map/all_gather | solution.py:142
  19.8 8.5 %copy-start.8 = (f32[2]{0:T(128)S(1)}, f32[2]{0:T(128)}, u32[]{:S(2)}) copy-start(f32[2]{0:T(128)} %param.15) | copy-start | bytes 28
  22.0 5.3 %collective-permute-start = (bf16[136,128]{0,1:T(8,128)(2,1)S(1)}, bf16[136,128]{0,1:T(8,128)(2,1)S(1)}, u32[]{:S(2)}, u32[]{:S(2)}) collective-permute-start(bf16[136,128]{0,1:T(8,128)(2,1)S(1)} %pad_maximum_fusion.3), channel_id=1, source_target_pairs={{0,8},{8,16},{16,24},{24,32},{32,40},{40,48},{48,56},{56,64},{64,7... | collective-permute-start | bytes 104456 | tf_op jit(solution)/shard_map/ppermute | solution.py:19
  31.2 10.5 %copy-start.5 = (bf16[704,32]{0,1:T(8,128)(2,1)S(1)}, bf16[704,32]{0,1:T(8,128)(2,1)}, u32[]{:S(2)}) copy-start(bf16[704,32]{0,1:T(8,128)(2,1)} %param.21) | copy-start | bytes 135172
  31.2 51.2 %all-to-all-start = ((bf16[8,64,2048]{2,1,0:T(8,128)(2,1)}), bf16[8,64,2048]{2,1,0:T(8,128)(2,1)S(1)}, u32[]{:S(2)}, u32[]{:S(2)}) async-start(bf16[8,64,2048]{2,1,0:T(8,128)(2,1)} %bitcast.67), calls=%async_computation | async-start | bytes 4194304 | tf_op jit(solution)/shard_map/all_to_all | solution.py:147
  84.0 2.6 %copy-start.7 = (f32[2048]{0:T(1024)S(1)}, f32[2048]{0:T(1024)}, u32[]{:S(2)}) copy-start(f32[2048]{0:T(1024)} %param.18) | copy-start | bytes 24580
  87.6 13.8 %collective-permute-start.1 = (bf16[64,2048]{1,0:T(8,128)(2,1)}, bf16[64,2048]{1,0:T(8,128)(2,1)S(1)}, u32[]{:S(2)}, u32[]{:S(2)}) collective-permute-start(bf16[64,2048]{1,0:T(8,128)(2,1)} %get-tuple-element.22), channel_id=1, source_target_pairs={{0,2},{1,3},{2,4},{3,5},{4,6},{5,7},{6,0},{7,1},{8,10},{9,11},{10,... | collective-permute-start | bytes 786440 | tf_op jit(solution)/shard_map/ppermute | solution.py:36
  90.9 11.2 %collective-permute-start.2 = (bf16[64,2048]{1,0:T(8,128)(2,1)}, bf16[64,2048]{1,0:T(8,128)(2,1)S(1)}, u32[]{:S(2)}, u32[]{:S(2)}) collective-permute-start(bf16[64,2048]{1,0:T(8,128)(2,1)} %get-tuple-element.22), channel_id=1, source_target_pairs={{0,6},{1,7},{2,0},{3,1},{4,2},{5,3},{6,4},{7,5},{8,14},{9,15},{10,... | collective-permute-start | bytes 786440 | tf_op jit(solution)/shard_map/ppermute | solution.py:36
  94.1 11.3 %collective-permute-start.3 = (bf16[64,2048]{1,0:T(8,128)(2,1)}, bf16[64,2048]{1,0:T(8,128)(2,1)}, u32[]{:S(2)}, u32[]{:S(2)}) collective-permute-start(bf16[64,2048]{1,0:T(8,128)(2,1)} %get-tuple-element.22), channel_id=1, source_target_pairs={{0,4},{1,5},{2,6},{3,7},{4,0},{5,1},{6,2},{7,3},{8,12},{9,13},{10,... | collective-permute-start | bytes 786440 | tf_op jit(solution)/shard_map/ppermute | solution.py:36
  97.8 24.1 %all-to-all-start.1 = ((bf16[4,512,512]{2,1,0:T(8,128)(2,1)}), bf16[4,512,512]{2,1,0:T(8,128)(2,1)S(1)}, u32[]{:S(2)}, u32[]{:S(2)}) async-start(bf16[4,512,512]{2,1,0:T(8,128)(2,1)} %broadcast_in_dim.26), calls=%async_computation.1 | async-start | bytes 4194304 | tf_op jit(solution)/shard_map/all_to_all | solution.py:27
  107.1 8.2 %collective-permute-start.4 = (bf16[256,2048]{1,0:T(8,128)(2,1)}, bf16[256,2048]{1,0:T(8,128)(2,1)S(1)}, u32[]{:S(2)}, u32[]{:S(2)}) collective-permute-start(bf16[256,2048]{1,0:T(8,128)(2,1)} %constant_dynamic-update-slice_fusion.2), channel_id=1, source_target_pairs={{0,1},{1,0},{2,3},{3,2},{4,5},{5,4},{6,7},{7,6},{8,9},{9,8},{10,11... | collective-permute-start | bytes 3145736 | tf_op jit(solution)/shard_map/ppermute | solution.py:23
  121.9 1.4 copy-start.1
  134.4 11.1 %collective-permute-start.5 = (bf16[256,2048]{1,0:T(8,128)(2,1)S(1)}, bf16[256,2048]{1,0:T(8,128)(2,1)S(1)}, u32[]{:S(2)}, u32[]{:S(2)}) collective-permute-start(bf16[256,2048]{1,0:T(8,128)(2,1)S(1)} %fusion.2), channel_id=1, source_target_pairs={{0,1},{1,0},{2,3},{3,2},{4,5},{5,4},{6,7},{7,6},{8,9},{9,8},{10,11... | collective-permute-start | bytes 3145736 | tf_op jit(solution)/shard_map/ppermute | solution.py:23
  179.9 6.2 %collective-permute-start.6 = (bf16[256,2048]{1,0:T(8,128)(2,1)S(1)}, bf16[256,2048]{1,0:T(8,128)(2,1)S(1)}, u32[]{:S(2)}, u32[]{:S(2)}) collective-permute-start(bf16[256,2048]{1,0:T(8,128)(2,1)S(1)} %bitcast.69), channel_id=1, source_target_pairs={{0,1},{1,0},{2,3},{3,2},{4,5},{5,4},{6,7},{7,6},{8,9},{9,8},{10,11... | collective-permute-start | bytes 3145736 | tf_op jit(solution)/shard_map/ppermute | solution.py:23
  184.3 1.9 copy-start.2
Sparse Core Ops, SparseCore 0:
  19.9 102.2 all-gather.1

commit v9 on v7

--- a/solution.py
+++ b/solution.py
@@ -110,11 +110,6 @@
     return jnp.where(
         column < ff, placed(w_gate, 0), jnp.where(column < 2 * ff, placed(w_up, ff), last)
     )
-
-
-def pair_sum_of(theirs, mine):
-    arrived = other_core(theirs)
-    return (mine + arrived.astype(jnp.float32)).astype(jnp.bfloat16)
 
 
 def to_owners(pair_sum):
@@ -161,21 +156,25 @@
     normed = rms_norm(stream, norm_gain).astype(jnp.bfloat16)
     normed = all_chips_rows(normed, chip)
     normed = jnp.concatenate([normed, other_core(normed)], axis=0)
+    normed, far, down = lax.optimization_barrier((normed, far, down))
 
     late = far[:, 2 * ff :]
-    acts = jnp.dot(normed, far[:, : 2 * ff], preferred_element_type=jnp.float32)
-    hidden = (jax.nn.silu(acts[:, :ff]) * acts[:, ff:]).astype(jnp.bfloat16)
+    acts = lax.dot_general(
+        far[:, : 2 * ff], normed, (((0,), (1,)), ((), ())), preferred_element_type=jnp.float32
+    )
+    hidden = (jax.nn.silu(acts[:ff]) * acts[ff:]).astype(jnp.bfloat16)
 
     def turned_dot(left, right):
         return lax.dot_general(
-            left, right, (((1,), (1,)), ((), ())), preferred_element_type=jnp.float32
+            left, right, (((0,), (1,)), ((), ())), preferred_element_type=jnp.float32
         )
 
-
     def through(part):
-        return turned_dot(part[:, EARLY:], late) + turned_dot(part[:, :EARLY], down)
-
-    pair_sum = pair_sum_of(through(hidden[half:]).astype(jnp.bfloat16), through(hidden[:half]))
+        return turned_dot(part[EARLY:], late) + turned_dot(part[:EARLY], down)
+
+    swapped_part = other_core(through(hidden[:, half:]).astype(jnp.bfloat16))
+    own_part, swapped_part = lax.optimization_barrier((through(hidden[:, :half]), swapped_part))
+    pair_sum = (own_part + swapped_part.astype(jnp.float32)).astype(jnp.bfloat16)
     mlp_total = to_owners(pair_sum).astype(jnp.float32).sum(axis=0)
     finished = (stream.astype(jnp.float32) + mlp_total).astype(jnp.bfloat16)
     mine = copies(finished, "tp", FAR_X).reshape(half, width)

time: 191 us -> 192 us (level)
  waiting for transfers between devices: 15.2 us -> 11.8 us
  other arithmetic: 4.91 us -> 7.98 us
    all_to_all x1, waiting for transfers between devices: 9.05 us -> 3.76 us  [swapped(): lax.all_to_all(pieces, axis, 0, 0, tiled=True, axis_index_groups=groups)]
    concatenate x0 -> x1, other arithmetic: none -> 2.81 us  [on_device(): normed = jnp.concatenate([normed, other_core(normed)], axis=0)]
  transfers between devices with their start and end apart: 10 -> 10, of which waited for: 5 -> 5; matrix products, arithmetic and copies ran while one was open for 8% -> 10% of each run, Pallas kernels for 0% -> 0%
where the time goes in v9:
time: 192 us; the launch traced here: 191 us
  blocking collectives  87.2 us (45%)
  starting transfers between devices  44.9 us (23%)
  matrix products  14.2 us (7%)
  between operations  13.9 us (7%)
  waiting for transfers between devices  11.8 us (6%)
  local copies, waits for them, and re-layouts  11.1 us (6%)
  other arithmetic  7.98 us (4%)
    all_to_all x3, blocking collectives, swapped(): lax.all_to_all(pieces, axis, 0, 0, tiled=True, axis_index_groups=groups)  45 us
    all_gather x1, blocking collectives, on_device(): lax.all_gather(early, 'sp', axis=0, tiled=True, axis_index_groups=FAR_Z)  42.2 us
    ppermute x3, starting transfers between devices, other_core(): return lax.ppermute(shard, 'tp', [(i, i ^ 1) for i in range(2 * NX)])  18.3 us
    all_to_all x1, starting transfers between devices, on_device(): lax.all_to_all(mixed.reshape(2 * NX, share, width), 'tp', 0, 0, tiled=True)  10.7 us
    ppermute x3, starting transfers between devices, chip_away(): return lax.ppermute(shard, 'tp', pairs)  10.1 us
    dot_general x1, matrix products, on_device(): lax.dot_general(far[:, :2 * ff], normed, (((0,), (1,)), ((), ())), prefer...  6.54 us
    dot_general x4, matrix products, turned_dot(): lax.dot_general(left, right, (((0,), (1,)), ((), ())), preferred_element_...  4.94 us
    ppermute x3, waiting for transfers between devices, other_core(): return lax.ppermute(shard, 'tp', [(i, i ^ 1) for i in range(2 * NX)])  4.35 us
  transfers between devices with their start and end apart: 10, of which 5 were waited for; matrix products, arithmetic and copies ran while one was open for 10% of the time, Pallas kernels for 0%

profile of v9, /device:TPU:1, one launch (start us, length us, event | category | flops | bytes accessed | tf_op | source)
XLA Modules:
  0.0 191.1 jit_solution(8539162494839874596)
XLA Ops:
  6.6 0.0 all-gather.2.cloned.1.call-start
  6.6 1.0 select_select_fusion
  7.7 11.3 %all_to_all.25 = bf16[4,32,1600]{2,1,0:T(8,128)(2,1)} all-to-all(bf16[4,32,1600]{2,1,0:T(8,128)(2,1)S(1)} %broadcast_in_dim.30), channel_id=1, replica_groups={{0,8,16,24},{32,40,48,56},{64,72,80,88},{96,104,112,120},{128,136,144,1..., dimensions={0} | all-to-all | bytes 819200 | tf_op jit(solution)/shard_map/all_to_all | solution.py:27
  19.0 0.0 all-gather.2.cloned.1.call-update
  19.1 0.0 copy-done.7
  19.1 0.1 broadcast_in_dim.25
  19.2 2.2 %collective-permute-start = (bf16[136,128]{0,1:T(8,128)(2,1)S(1)}, bf16[136,128]{0,1:T(8,128)(2,1)S(1)}, u32[]{:S(2)}, u32[]{:S(2)}) collective-permute-start(bf16[136,128]{0,1:T(8,128)(2,1)S(1)} %pad_maximum_fusion.3), channel_id=1, source_target_pairs={{0,8},{8,16},{16,24},{24,32},{32,40},{40,48},{48,56},{56,64},{64,7... | collective-permute-start | bytes 104456 | tf_op jit(solution)/shard_map/ppermute | solution.py:19
  21.5 0.0 copy-done.4
  21.5 0.1 reshape.148
  21.7 1.0 collective-permute-done
  22.8 0.1 add_reduce_fusion
  22.9 0.2 compare_and_fusion
  23.2 0.4 fusion.35
  23.5 0.1 broadcast_maximum_fusion
  23.6 0.2 fusion.7
  23.8 0.1 exponential_add_fusion
  23.8 0.3 fusion.6
  24.2 0.2 copy.30
  24.3 0.1 reshape_reshape.3
  24.5 2.0 %convolution_convert_fusion = bf16[512,2048]{1,0:T(8,128)(2,1)} fusion(bf16[512,128]{1,0:T(8,128)(2,1)S(1)} %bitcast.75, bf16[128,2048]{1,0:T(8,128)(2,1)S(1)} %copy-done), kind=kOutput, calls=%fused_computation.3 | convolution fusion | flops 269484032 | bytes 2752512 | tf_op jit(solution)/shard_map/dot_general | solution.py:145
  26.5 10.7 %all-to-all-start = ((bf16[8,64,2048]{2,1,0:T(8,128)(2,1)}), bf16[8,64,2048]{2,1,0:T(8,128)(2,1)S(1)}, u32[]{:S(2)}, u32[]{:S(2)}) async-start(bf16[8,64,2048]{2,1,0:T(8,128)(2,1)} %bitcast.68), calls=%async_computation | async-start | bytes 4194304 | tf_op jit(solution)/shard_map/all_to_all | solution.py:146
  37.2 42.2 %all_gather.6 = bf16[512,512]{1,0:T(8,128)(2,1)S(1)} all-gather(bf16[32,512]{1,0:T(8,128)(2,1)S(1)} %slice.112), channel_id=1, replica_groups={{0,32,64,96,128,160,192,224,256,288,320,352,384,416,448,480},{8,40,72,1..., dimensions={0}, use_global_device_ids=true | all-gather | bytes 557056 | tf_op jit(solution)/shard_map/all_gather | solution.py:148
  79.4 0.0 all-to-all-done
  79.4 1.6 broadcast_in_dim.28
  81.0 0.3 convert_reduce_fusion
  81.3 1.1 fusion.12
  82.5 1.1 broadcast_in_dim.29
  83.6 0.9 constant_dynamic-update-slice_fusion.5
  84.6 3.3 %collective-permute-start.1 = (bf16[64,2048]{1,0:T(8,128)(2,1)}, bf16[64,2048]{1,0:T(8,128)(2,1)S(1)}, u32[]{:S(2)}, u32[]{:S(2)}) collective-permute-start(bf16[64,2048]{1,0:T(8,128)(2,1)} %get-tuple-element.22), channel_id=1, source_target_pairs={{0,2},{1,3},{2,4},{3,5},{4,6},{5,7},{6,0},{7,1},{8,10},{9,11},{10,... | collective-permute-start | bytes 786440 | tf_op jit(solution)/shard_map/ppermute | solution.py:36
  87.9 3.2 %collective-permute-start.2 = (bf16[64,2048]{1,0:T(8,128)(2,1)}, bf16[64,2048]{1,0:T(8,128)(2,1)S(1)}, u32[]{:S(2)}, u32[]{:S(2)}) collective-permute-start(bf16[64,2048]{1,0:T(8,128)(2,1)} %get-tuple-element.22), channel_id=1, source_target_pairs={{0,6},{1,7},{2,0},{3,1},{4,2},{5,3},{6,4},{7,5},{8,14},{9,15},{10,... | collective-permute-start | bytes 786440 | tf_op jit(solution)/shard_map/ppermute | solution.py:36
  91.1 3.6 %collective-permute-start.3 = (bf16[64,2048]{1,0:T(8,128)(2,1)}, bf16[64,2048]{1,0:T(8,128)(2,1)}, u32[]{:S(2)}, u32[]{:S(2)}) collective-permute-start(bf16[64,2048]{1,0:T(8,128)(2,1)} %get-tuple-element.22), channel_id=1, source_target_pairs={{0,4},{1,5},{2,6},{3,7},{4,0},{5,1},{6,2},{7,3},{8,12},{9,13},{10,... | collective-permute-start | bytes 786440 | tf_op jit(solution)/shard_map/ppermute | solution.py:36
  94.7 3.6 %all-to-all-start.2 = ((bf16[4,512,512]{2,1,0:T(8,128)(2,1)}), bf16[4,512,512]{2,1,0:T(8,128)(2,1)S(1)}, u32[]{:S(2)}, u32[]{:S(2)}) async-start(bf16[4,512,512]{2,1,0:T(8,128)(2,1)} %broadcast_in_dim.28), calls=%async_computation.2 | async-start | bytes 4194304 | tf_op jit(solution)/shard_map/all_to_all | solution.py:27
  98.3 0.0 collective-permute-done.1
  98.4 0.7 constant_dynamic-update-slice_fusion.4
  99.1 0.0 collective-permute-done.2
  99.1 0.7 constant_dynamic-update-slice_fusion.3
  99.8 2.6 %collective-permute-done.3 = bf16[64,2048]{1,0:T(8,128)(2,1)} collective-permute-done((bf16[64,2048]{1,0:T(8,128)(2,1)}, bf16[64,2048]{1,0:T(8,128)(2,1)}, u32[]{:S(2)}, u32[]{:S(2)}) %collective-permute-start.3) | collective-permute-done | bytes 262176 | tf_op jit(solution)/shard_map/ppermute | solution.py:36
  102.4 1.7 constant_dynamic-update-slice_fusion.2
  104.1 5.7 %collective-permute-start.4 = (bf16[256,2048]{1,0:T(8,128)(2,1)}, bf16[256,2048]{1,0:T(8,128)(2,1)S(1)}, u32[]{:S(2)}, u32[]{:S(2)}) collective-permute-start(bf16[256,2048]{1,0:T(8,128)(2,1)} %constant_dynamic-update-slice_fusion.2), channel_id=1, source_target_pairs={{0,1},{1,0},{2,3},{3,2},{4,5},{5,4},{6,7},{7,6},{8,9},{9,8},{10,11... | collective-permute-start | bytes 3145736 | tf_op jit(solution)/shard_map/ppermute | solution.py:23
  109.8 2.5 %collective-permute-done.4 = bf16[256,2048]{1,0:T(8,128)(2,1)S(1)} collective-permute-done((bf16[256,2048]{1,0:T(8,128)(2,1)}, bf16[256,2048]{1,0:T(8,128)(2,1)S(1)}, u32[]{:S(2)}, u32[]{:S(2)}) %collective-permute-start.4) | collective-permute-done | bytes 1048608 | tf_op jit(solution)/shard_map/ppermute | solution.py:23
  112.3 2.8 %pad_maximum_fusion = bf16[512,2048]{1,0:T(8,128)(2,1)} fusion(bf16[256,2048]{1,0:T(8,128)(2,1)S(1)} %collective-permute-done.4, bf16[256,2048]{1,0:T(8,128)(2,1)} %constant_dynamic-update-slice_fusion.2), kind=kLoop, calls=%fused_computation.7 | loop fusion | flops 4194304 | bytes 4194304 | tf_op jit(solution)/shard_map/concatenate | solution.py:158
  115.1 3.8 %all-to-all-done.2 = bf16[4,512,512]{2,1,0:T(8,128)(2,1)S(1)} async-done(((bf16[4,512,512]{2,1,0:T(8,128)(2,1)}), bf16[4,512,512]{2,1,0:T(8,128)(2,1)S(1)}, u32[]{:S(2)}, u32[]{:S(2)}) %all-to-all-start.2) | async-done | bytes 2097184 | tf_op jit(solution)/shard_map/all_to_all | solution.py:27
  118.8 1.4 copy-done.1
  120.2 1.7 copy.32
  122.0 0.0 all-gather.2.cloned.1.call-done
  122.0 6.5 %fusion = f32[1408,512]{1,0:T(8,128)S(1)} fusion(bf16[512,2048]{1,0:T(8,128)(2,1)} %pad_maximum_fusion, bf16[2048,1600]{1,0:T(8,128)(2,1)} %all-gather.2.cloned.1.call-done), kind=kOutput, calls=%fused_computation | convolution fusion | flops 2952790016 | bytes 10747904 | tf_op jit(solution)/shard_map/dot_general | solution.py:162
  128.6 0.5 fusion.3
  129.0 1.7 fusion.8
  130.7 0.8 fusion.2
  131.5 8.7 %collective-permute-start.5 = (bf16[256,2048]{1,0:T(8,128)(2,1)S(1)}, bf16[256,2048]{1,0:T(8,128)(2,1)S(1)}, u32[]{:S(2)}, u32[]{:S(2)}) collective-permute-start(bf16[256,2048]{1,0:T(8,128)(2,1)S(1)} %fusion.2), channel_id=1, source_target_pairs={{0,1},{1,0},{2,3},{3,2},{4,5},{5,4},{6,7},{7,6},{8,9},{9,8},{10,11... | collective-permute-start | bytes 3145736 | tf_op jit(solution)/shard_map/ppermute | solution.py:23
  140.2 1.7 fusion.10
  141.9 0.8 convolution_add_fusion.1
  142.6 0.0 collective-permute-done.5
  142.6 0.3 add_convert_fusion
  142.9 17.3 %all_to_all.26 = bf16[4,64,2048]{2,1,0:T(8,128)(2,1)S(1)} all-to-all(bf16[4,64,2048]{2,1,0:T(8,128)(2,1)S(1)} %bitcast.72), channel_id=1, replica_groups={{0,2,4,6},{1,3,5,7},{8,10,12,14},{9,11,13,15},{16,18,20,22},{17,19,21,2..., dimensions={0} | all-to-all | bytes 2097152 | tf_op jit(solution)/shard_map/all_to_all | solution.py:27
  160.2 0.2 convert_reduce_fusion.1
  160.4 0.1 broadcast_in_dim.31
  160.5 16.4 %all_to_all.27 = bf16[4,64,2048]{2,1,0:T(8,128)(2,1)S(1)} all-to-all(bf16[4,64,2048]{2,1,0:T(8,128)(2,1)S(1)} %broadcast_in_dim.31), channel_id=1, replica_groups={{0,2,4,6},{1,3,5,7},{8,10,12,14},{9,11,13,15},{16,18,20,22},{17,19,21,2..., dimensions={0} | all-to-all | bytes 2097152 | tf_op jit(solution)/shard_map/all_to_all | solution.py:27
  177.0 4.0 %collective-permute-start.6 = (bf16[256,2048]{1,0:T(8,128)(2,1)S(1)}, bf16[256,2048]{1,0:T(8,128)(2,1)S(1)}, u32[]{:S(2)}, u32[]{:S(2)}) collective-permute-start(bf16[256,2048]{1,0:T(8,128)(2,1)S(1)} %bitcast.70), channel_id=1, source_target_pairs={{0,1},{1,0},{2,3},{3,2},{4,5},{5,4},{6,7},{7,6},{8,9},{9,8},{10,11... | collective-permute-start | bytes 3145736 | tf_op jit(solution)/shard_map/ppermute | solution.py:23
  180.9 0.2 broadcast_in_dim.24
  181.2 0.1 constant_dynamic-update-slice_fusion.1
  181.3 0.0 copy-start.2
  181.3 1.9 collective-permute-done.6
  183.2 1.0 constant_dynamic-update-slice_fusion
  (39 shorter events, 0.3 us)
Async XLA Ops:
  6.5 18.0 %copy-start = (bf16[128,2048]{1,0:T(8,128)(2,1)S(1)}, bf16[128,2048]{1,0:T(8,128)(2,1)}, u32[]{:S(2)}) copy-start(bf16[128,2048]{1,0:T(8,128)(2,1)} %param.17) | copy-start | bytes 1572868
  6.5 12.6 %slice-start = ((bf16[512,64]{0,1:T(8,128)(2,1)}), bf16[128,64]{0,1:T(8,128)(2,1)S(1)}, s32[]{:S(2)}) async-start(bf16[512,64]{0,1:T(8,128)(2,1)} %param.12), calls=%async_computation.6 | async-start | bytes 32768 | tf_op jit(solution)/shard_map/slice | solution.py:68
  6.5 14.9 %copy-start.3 = (bf16[512,64]{0,1:T(8,128)(2,1)S(1)}, bf16[512,64]{0,1:T(8,128)(2,1)}, u32[]{:S(2)}) copy-start(bf16[512,64]{0,1:T(8,128)(2,1)} %param.12) | copy-start | bytes 196612
  6.5 12.6 %slice-start.1 = ((bf16[512,64]{0,1:T(8,128)(2,1)}), bf16[128,64]{0,1:T(8,128)(2,1)S(1)}, s32[]{:S(2)}) async-start(bf16[512,64]{0,1:T(8,128)(2,1)} %param.13), calls=%async_computation.7 | async-start | bytes 32768 | tf_op jit(solution)/shard_map/slice | solution.py:68
  6.5 14.9 %copy-start.4 = (bf16[512,64]{0,1:T(8,128)(2,1)S(1)}, bf16[512,64]{0,1:T(8,128)(2,1)}, u32[]{:S(2)}) copy-start(bf16[512,64]{0,1:T(8,128)(2,1)} %param.13) | copy-start | bytes 196612
  6.5 12.5 %copy-start.7 = (s32[512]{0:T(512)S(1)}, s32[512]{0:T(512)}, u32[]{:S(2)}) copy-start(s32[512]{0:T(512)} %param.14) | copy-start | bytes 6148
  6.6 15.0 %copy-start.6 = (bf16[512,128]{1,0:T(8,128)(2,1)S(1)}, bf16[512,128]{1,0:T(8,128)(2,1)}, u32[]{:S(2)}) copy-start(bf16[512,128]{1,0:T(8,128)(2,1)} %param.11) | copy-start | bytes 393220
  6.6 115.4 %all-gather.2.cloned.1.call-start = ((), (), s32[]{:S(2)}) async-start(), calls=%async_computation.5 | async-start | bytes 7241728 | tf_op jit(solution)/shard_map/all_gather | solution.py:141
  19.0 4.5 %copy-start.9 = (f32[2]{0:T(128)S(1)}, f32[2]{0:T(128)}, u32[]{:S(2)}) copy-start(f32[2]{0:T(128)} %param.15) | copy-start | bytes 28
  19.2 3.5 %collective-permute-start = (bf16[136,128]{0,1:T(8,128)(2,1)S(1)}, bf16[136,128]{0,1:T(8,128)(2,1)S(1)}, u32[]{:S(2)}, u32[]{:S(2)}) collective-permute-start(bf16[136,128]{0,1:T(8,128)(2,1)S(1)} %pad_maximum_fusion.3), channel_id=1, source_target_pairs={{0,8},{8,16},{16,24},{24,32},{32,40},{40,48},{48,56},{56,64},{64,7... | collective-permute-start | bytes 104456 | tf_op jit(solution)/shard_map/ppermute | solution.py:19
  26.5 10.7 %copy-start.5 = (bf16[704,32]{0,1:T(8,128)(2,1)S(1)}, bf16[704,32]{0,1:T(8,128)(2,1)}, u32[]{:S(2)}) copy-start(bf16[704,32]{0,1:T(8,128)(2,1)} %param.21) | copy-start | bytes 135172
  26.5 52.9 %all-to-all-start = ((bf16[8,64,2048]{2,1,0:T(8,128)(2,1)}), bf16[8,64,2048]{2,1,0:T(8,128)(2,1)S(1)}, u32[]{:S(2)}, u32[]{:S(2)}) async-start(bf16[8,64,2048]{2,1,0:T(8,128)(2,1)} %bitcast.68), calls=%async_computation | async-start | bytes 4194304 | tf_op jit(solution)/shard_map/all_to_all | solution.py:146
  81.0 2.6 %copy-start.8 = (f32[2048]{0:T(1024)S(1)}, f32[2048]{0:T(1024)}, u32[]{:S(2)}) copy-start(f32[2048]{0:T(1024)} %param.18) | copy-start | bytes 24580
  84.6 13.8 %collective-permute-start.1 = (bf16[64,2048]{1,0:T(8,128)(2,1)}, bf16[64,2048]{1,0:T(8,128)(2,1)S(1)}, u32[]{:S(2)}, u32[]{:S(2)}) collective-permute-start(bf16[64,2048]{1,0:T(8,128)(2,1)} %get-tuple-element.22), channel_id=1, source_target_pairs={{0,2},{1,3},{2,4},{3,5},{4,6},{5,7},{6,0},{7,1},{8,10},{9,11},{10,... | collective-permute-start | bytes 786440 | tf_op jit(solution)/shard_map/ppermute | solution.py:36
  87.9 11.2 %collective-permute-start.2 = (bf16[64,2048]{1,0:T(8,128)(2,1)}, bf16[64,2048]{1,0:T(8,128)(2,1)S(1)}, u32[]{:S(2)}, u32[]{:S(2)}) collective-permute-start(bf16[64,2048]{1,0:T(8,128)(2,1)} %get-tuple-element.22), channel_id=1, source_target_pairs={{0,6},{1,7},{2,0},{3,1},{4,2},{5,3},{6,4},{7,5},{8,14},{9,15},{10,... | collective-permute-start | bytes 786440 | tf_op jit(solution)/shard_map/ppermute | solution.py:36
  91.1 11.3 %collective-permute-start.3 = (bf16[64,2048]{1,0:T(8,128)(2,1)}, bf16[64,2048]{1,0:T(8,128)(2,1)}, u32[]{:S(2)}, u32[]{:S(2)}) collective-permute-start(bf16[64,2048]{1,0:T(8,128)(2,1)} %get-tuple-element.22), channel_id=1, source_target_pairs={{0,4},{1,5},{2,6},{3,7},{4,0},{5,1},{6,2},{7,3},{8,12},{9,13},{10,... | collective-permute-start | bytes 786440 | tf_op jit(solution)/shard_map/ppermute | solution.py:36
  94.7 24.1 %all-to-all-start.2 = ((bf16[4,512,512]{2,1,0:T(8,128)(2,1)}), bf16[4,512,512]{2,1,0:T(8,128)(2,1)S(1)}, u32[]{:S(2)}, u32[]{:S(2)}) async-start(bf16[4,512,512]{2,1,0:T(8,128)(2,1)} %broadcast_in_dim.28), calls=%async_computation.2 | async-start | bytes 4194304 | tf_op jit(solution)/shard_map/all_to_all | solution.py:27
  104.1 8.2 %collective-permute-start.4 = (bf16[256,2048]{1,0:T(8,128)(2,1)}, bf16[256,2048]{1,0:T(8,128)(2,1)S(1)}, u32[]{:S(2)}, u32[]{:S(2)}) collective-permute-start(bf16[256,2048]{1,0:T(8,128)(2,1)} %constant_dynamic-update-slice_fusion.2), channel_id=1, source_target_pairs={{0,1},{1,0},{2,3},{3,2},{4,5},{5,4},{6,7},{7,6},{8,9},{9,8},{10,11... | collective-permute-start | bytes 3145736 | tf_op jit(solution)/shard_map/ppermute | solution.py:23
  118.8 1.4 copy-start.1
  131.5 11.1 %collective-permute-start.5 = (bf16[256,2048]{1,0:T(8,128)(2,1)S(1)}, bf16[256,2048]{1,0:T(8,128)(2,1)S(1)}, u32[]{:S(2)}, u32[]{:S(2)}) collective-permute-start(bf16[256,2048]{1,0:T(8,128)(2,1)S(1)} %fusion.2), channel_id=1, source_target_pairs={{0,1},{1,0},{2,3},{3,2},{4,5},{5,4},{6,7},{7,6},{8,9},{9,8},{10,11... | collective-permute-start | bytes 3145736 | tf_op jit(solution)/shard_map/ppermute | solution.py:23
  177.0 6.2 %collective-permute-start.6 = (bf16[256,2048]{1,0:T(8,128)(2,1)S(1)}, bf16[256,2048]{1,0:T(8,128)(2,1)S(1)}, u32[]{:S(2)}, u32[]{:S(2)}) collective-permute-start(bf16[256,2048]{1,0:T(8,128)(2,1)S(1)} %bitcast.70), channel_id=1, source_target_pairs={{0,1},{1,0},{2,3},{3,2},{4,5},{5,4},{6,7},{7,6},{8,9},{9,8},{10,11... | collective-permute-start | bytes 3145736 | tf_op jit(solution)/shard_map/ppermute | solution.py:23
  181.3 1.9 copy-start.2
Sparse Core Ops, SparseCore 0:
  19.2 100.0 all-gather.1

commit v10 on v8

--- a/solution.py
+++ b/solution.py
@@ -7,7 +7,7 @@
 HD = 64
 WINDOW = 128
 NZ, NY, NX = 16, 4, 4
-EARLY = 512
+EARLY = 640
 FAR_Z = [[z * NY + y for z in range(NZ)] for y in range(NY)]
 FAR_Y = [[z * NY + y for y in range(NY)] for z in range(NZ)]
 FAR_X = [[2 * x + c for x in range(NX)] for c in range(2)]
@@ -136,9 +136,8 @@
     ff = w_gate.shape[1]
 
     turned = w_down.T
-    near = lax.all_gather(
-        side_by_side(w_gate, w_up, turned), "sp", axis=0, tiled=True, axis_index_groups=FAR_Y
-    )
+    near = copies(side_by_side(w_gate, w_up, turned), "sp", FAR_Y)
+    near = near.reshape(-1, near.shape[2])
     far = lax.all_gather(near, "sp", axis=0, tiled=True, axis_index_groups=FAR_Z)
 
     attended = attend(queries, key_rows, values, doc_ids, sink_logits)
@@ -157,7 +156,7 @@
     normed = rms_norm(stream, norm_gain).astype(jnp.bfloat16)
     normed = all_chips_rows(normed, chip)
     normed = jnp.concatenate([normed, other_core(normed)], axis=0)
-    normed, far, down = lax.optimization_barrier((normed, far, down))
+    normed, far = lax.optimization_barrier((normed, far))
 
     late = far[:, 2 * ff :]
     acts = jnp.dot(normed, far[:, : 2 * ff], preferred_element_type=jnp.float32)

time: 195 us -> 202 us (1.036)
  waiting for transfers between devices: 10.8 us -> 14.7 us
  blocking collectives: 86.6 us -> 89.1 us
    all_gather x1 -> x0, blocking collectives: 12.2 us -> none  [on_device(): lax.all_gather(side_by_side(w_gate, w_up, turned), 'sp', axis=0, tiled=Tr...]
    all_to_all x2 -> x3, blocking collectives: 33.7 us -> 44.9 us  [swapped(): lax.all_to_all(pieces, axis, 0, 0, tiled=True, axis_index_groups=groups)]
    all_to_all x1, waiting for transfers between devices: 3.84 us -> 8.58 us  [swapped(): lax.all_to_all(pieces, axis, 0, 0, tiled=True, axis_index_groups=groups)]
    all_gather x1, blocking collectives: 40.7 us -> 44.2 us  [on_device(): lax.all_gather(early, 'sp', axis=0, tiled=True, axis_index_groups=FAR_Z)]
  transfers between devices with their start and end apart: 10 -> 10, of which waited for: 4 -> 5; matrix products, arithmetic and copies ran while one was open for 13% -> 12% of each run, Pallas kernels for 0% -> 0%
where the time goes in v10:
time: 202 us; the launch traced here: 201 us
  blocking collectives  89.1 us (44%)
  starting transfers between devices  45.6 us (23%)
  local copies, waits for them, and re-layouts  15.2 us (8%)
  waiting for transfers between devices  14.7 us (7%)
  matrix products  14.1 us (7%)
  between operations  13.9 us (7%)
  other arithmetic  8.62 us (4%)
    all_to_all x3, blocking collectives, swapped(): lax.all_to_all(pieces, axis, 0, 0, tiled=True, axis_index_groups=groups)  44.9 us
    all_gather x1, blocking collectives, on_device(): lax.all_gather(early, 'sp', axis=0, tiled=True, axis_index_groups=FAR_Z)  44.2 us
    ppermute x3, starting transfers between devices, other_core(): return lax.ppermute(shard, 'tp', [(i, i ^ 1) for i in range(2 * NX)])  19.2 us
    all_to_all x1, starting transfers between devices, on_device(): lax.all_to_all(mixed.reshape(2 * NX, share, width), 'tp', 0, 0, tiled=True)  10.6 us
    ppermute x3, starting transfers between devices, chip_away(): return lax.ppermute(shard, 'tp', pairs)  9.92 us
    all_to_all x1, waiting for transfers between devices, swapped(): lax.all_to_all(pieces, axis, 0, 0, tiled=True, axis_index_groups=groups)  8.58 us
    dot_general x1, matrix products, on_device(): acts = jnp.dot(normed, far[:, :2 * ff], preferred_element_type=jnp.float32)  6.4 us
    dynamic_update_slice x3, local copies, waits for them, and re-layouts, all_chips_rows(): lax.dynamic_update_slice_in_dim(rows, chip_away(shard, by), sender * shar...  5.06 us
  transfers between devices with their start and end apart: 10, of which 5 were waited for; matrix products, arithmetic and copies ran while one was open for 12% of the time, Pallas kernels for 0%

profile of v10, /device:TPU:1, one launch (start us, length us, event | category | flops | bytes accessed | tf_op | source)
XLA Modules:
  0.0 201.3 jit_solution(17847412549372809141)
XLA Ops:
  6.5 0.0 all-gather.2.cloned.1.call-start
  6.6 1.0 select_select_fusion
  7.6 11.1 %all_to_all.25 = bf16[4,32,1472]{2,1,0:T(8,128)(2,1)} all-to-all(bf16[4,32,1472]{2,1,0:T(8,128)(2,1)S(1)} %broadcast_in_dim.30), channel_id=1, replica_groups={{0,8,16,24},{32,40,48,56},{64,72,80,88},{96,104,112,120},{128,136,144,1..., dimensions={0} | all-to-all | bytes 753664 | tf_op jit(solution)/shard_map/all_to_all | solution.py:27
  18.8 0.0 all-gather.2.cloned.1.call-update
  18.8 0.7 slice.90
  19.5 0.7 slice.91
  20.3 0.7 add_convert_fusion.2
  20.9 0.1 broadcast_in_dim.25
  21.1 2.2 %collective-permute-start = (bf16[136,128]{0,1:T(8,128)(2,1)S(1)}, bf16[136,128]{0,1:T(8,128)(2,1)S(1)}, u32[]{:S(2)}, u32[]{:S(2)}) collective-permute-start(bf16[136,128]{0,1:T(8,128)(2,1)S(1)} %pad_maximum_fusion.3), channel_id=1, source_target_pairs={{0,8},{8,16},{16,24},{24,32},{32,40},{40,48},{48,56},{56,64},{64,7... | collective-permute-start | bytes 104456 | tf_op jit(solution)/shard_map/ppermute | solution.py:19
  23.4 0.1 reshape.148
  23.5 1.0 collective-permute-done
  24.6 0.1 add_reduce_fusion
  24.8 0.2 compare_and_fusion
  25.0 0.4 fusion.35
  25.4 0.1 broadcast_maximum_fusion
  25.5 0.2 fusion.7
  25.6 0.1 exponential_add_fusion
  25.7 0.3 fusion.6
  26.0 0.2 copy.30
  26.2 0.1 reshape_reshape.3
  26.4 2.0 %convolution_convert_fusion = bf16[512,2048]{1,0:T(8,128)(2,1)} fusion(bf16[512,128]{1,0:T(8,128)(2,1)S(1)} %bitcast.75, bf16[128,2048]{1,0:T(8,128)(2,1)S(1)} %copy-done), kind=kOutput, calls=%fused_computation.3 | convolution fusion | flops 269484032 | bytes 2752512 | tf_op jit(solution)/shard_map/dot_general | solution.py:145
  28.4 10.6 %all-to-all-start = ((bf16[8,64,2048]{2,1,0:T(8,128)(2,1)}), bf16[8,64,2048]{2,1,0:T(8,128)(2,1)S(1)}, u32[]{:S(2)}, u32[]{:S(2)}) async-start(bf16[8,64,2048]{2,1,0:T(8,128)(2,1)} %bitcast.69), calls=%async_computation | async-start | bytes 4194304 | tf_op jit(solution)/shard_map/all_to_all | solution.py:146
  39.1 44.2 %all_gather.6 = bf16[512,640]{1,0:T(8,128)(2,1)S(1)} all-gather(bf16[32,640]{1,0:T(8,128)(2,1)S(1)} %slice.112), channel_id=1, replica_groups={{0,32,64,96,128,160,192,224,256,288,320,352,384,416,448,480},{8,40,72,1..., dimensions={0}, use_global_device_ids=true | all-gather | bytes 696320 | tf_op jit(solution)/shard_map/all_gather | solution.py:148
  83.3 0.0 all-to-all-done
  83.3 1.8 broadcast_in_dim.28
  85.0 0.3 convert_reduce_fusion
  85.4 1.1 fusion.8
  86.6 1.1 broadcast_in_dim.29
  87.7 0.9 constant_dynamic-update-slice_fusion.5
  88.6 3.1 %collective-permute-start.1 = (bf16[64,2048]{1,0:T(8,128)(2,1)}, bf16[64,2048]{1,0:T(8,128)(2,1)}, u32[]{:S(2)}, u32[]{:S(2)}) collective-permute-start(bf16[64,2048]{1,0:T(8,128)(2,1)} %get-tuple-element.20), channel_id=1, source_target_pairs={{0,2},{1,3},{2,4},{3,5},{4,6},{5,7},{6,0},{7,1},{8,10},{9,11},{10,... | collective-permute-start | bytes 786440 | tf_op jit(solution)/shard_map/ppermute | solution.py:36
  91.7 3.3 %collective-permute-start.2 = (bf16[64,2048]{1,0:T(8,128)(2,1)}, bf16[64,2048]{1,0:T(8,128)(2,1)}, u32[]{:S(2)}, u32[]{:S(2)}) collective-permute-start(bf16[64,2048]{1,0:T(8,128)(2,1)} %get-tuple-element.20), channel_id=1, source_target_pairs={{0,6},{1,7},{2,0},{3,1},{4,2},{5,3},{6,4},{7,5},{8,14},{9,15},{10,... | collective-permute-start | bytes 786440 | tf_op jit(solution)/shard_map/ppermute | solution.py:36
  95.1 3.4 %collective-permute-start.3 = (bf16[64,2048]{1,0:T(8,128)(2,1)}, bf16[64,2048]{1,0:T(8,128)(2,1)}, u32[]{:S(2)}, u32[]{:S(2)}) collective-permute-start(bf16[64,2048]{1,0:T(8,128)(2,1)} %get-tuple-element.20), channel_id=1, source_target_pairs={{0,4},{1,5},{2,6},{3,7},{4,0},{5,1},{6,2},{7,3},{8,12},{9,13},{10,... | collective-permute-start | bytes 786440 | tf_op jit(solution)/shard_map/ppermute | solution.py:36
  98.6 3.7 %all-to-all-start.2 = ((bf16[4,512,640]{2,1,0:T(8,128)(2,1)}), bf16[4,512,640]{2,1,0:T(8,128)(2,1)S(1)}, u32[]{:S(2)}, u32[]{:S(2)}) async-start(bf16[4,512,640]{2,1,0:T(8,128)(2,1)} %broadcast_in_dim.28), calls=%async_computation.2 | async-start | bytes 5242880 | tf_op jit(solution)/shard_map/all_to_all | solution.py:27
  102.3 0.0 collective-permute-done.1
  102.3 1.7 constant_dynamic-update-slice_fusion.4
  104.0 1.7 constant_dynamic-update-slice_fusion.3
  105.7 0.7 collective-permute-done.3
  106.3 1.7 constant_dynamic-update-slice_fusion.2
  108.0 6.8 %collective-permute-start.4 = (bf16[256,2048]{1,0:T(8,128)(2,1)}, bf16[256,2048]{1,0:T(8,128)(2,1)S(1)}, u32[]{:S(2)}, u32[]{:S(2)}) collective-permute-start(bf16[256,2048]{1,0:T(8,128)(2,1)} %constant_dynamic-update-slice_fusion.2), channel_id=1, source_target_pairs={{0,1},{1,0},{2,3},{3,2},{4,5},{5,4},{6,7},{7,6},{8,9},{9,8},{10,11... | collective-permute-start | bytes 3145736 | tf_op jit(solution)/shard_map/ppermute | solution.py:23
  114.8 2.5 %collective-permute-done.4 = bf16[256,2048]{1,0:T(8,128)(2,1)S(1)} collective-permute-done((bf16[256,2048]{1,0:T(8,128)(2,1)}, bf16[256,2048]{1,0:T(8,128)(2,1)S(1)}, u32[]{:S(2)}, u32[]{:S(2)}) %collective-permute-start.4) | collective-permute-done | bytes 1048608 | tf_op jit(solution)/shard_map/ppermute | solution.py:23
  117.3 2.8 %pad_maximum_fusion = bf16[512,2048]{1,0:T(8,128)(2,1)} fusion(bf16[256,2048]{1,0:T(8,128)(2,1)S(1)} %collective-permute-done.4, bf16[256,2048]{1,0:T(8,128)(2,1)} %constant_dynamic-update-slice_fusion.2), kind=kLoop, calls=%fused_computation.7 | loop fusion | flops 4194304 | bytes 4194304 | tf_op jit(solution)/shard_map/concatenate | solution.py:158
  120.1 8.6 %all-to-all-done.2 = bf16[4,512,640]{2,1,0:T(8,128)(2,1)S(1)} async-done(((bf16[4,512,640]{2,1,0:T(8,128)(2,1)}), bf16[4,512,640]{2,1,0:T(8,128)(2,1)S(1)}, u32[]{:S(2)}, u32[]{:S(2)}) %all-to-all-start.2) | async-done | bytes 2621472 | tf_op jit(solution)/shard_map/all_to_all | solution.py:27
  128.7 1.6 copy-done.1
  130.3 2.1 %copy.32 = bf16[16,4,32,640]{3,2,1,0:T(8,128)(2,1)S(1)} copy(bf16[16,4,32,640]{3,2,0,1:T(8,128)(2,1)} %bitcast.68) | data formatting | bytes 5242880 | tf_op jit(solution)/shard_map/transpose | solution.py:152
  132.4 0.0 all-gather.2.cloned.1.call-done
  132.4 6.4 %fusion = f32[512,1408]{1,0:T(8,128)S(1)} fusion(bf16[512,2048]{1,0:T(8,128)(2,1)} %pad_maximum_fusion, bf16[2048,1472]{1,0:T(8,128)(2,1)} %all-gather.2.cloned.1.call-done), kind=kOutput, calls=%fused_computation | convolution fusion | flops 2952790016 | bytes 10747904 | tf_op jit(solution)/shard_map/dot_general | solution.py:162
  138.8 0.5 fusion.3
  139.3 1.5 fusion.13
  140.8 1.0 fusion.2
  141.8 8.4 %collective-permute-start.5 = (bf16[256,2048]{1,0:T(8,128)(2,1)S(1)}, bf16[256,2048]{1,0:T(8,128)(2,1)S(1)}, u32[]{:S(2)}, u32[]{:S(2)}) collective-permute-start(bf16[256,2048]{1,0:T(8,128)(2,1)S(1)} %fusion.2), channel_id=1, source_target_pairs={{0,1},{1,0},{2,3},{3,2},{4,5},{5,4},{6,7},{7,6},{8,9},{9,8},{10,11... | collective-permute-start | bytes 3145736 | tf_op jit(solution)/shard_map/ppermute | solution.py:23
  150.2 1.5 fusion.15
  151.7 1.0 convolution_add_fusion.1
  152.7 0.0 collective-permute-done.5
  152.7 0.3 add_convert_fusion
  153.1 17.3 %all_to_all.26 = bf16[4,64,2048]{2,1,0:T(8,128)(2,1)S(1)} all-to-all(bf16[4,64,2048]{2,1,0:T(8,128)(2,1)S(1)} %bitcast.72), channel_id=1, replica_groups={{0,2,4,6},{1,3,5,7},{8,10,12,14},{9,11,13,15},{16,18,20,22},{17,19,21,2..., dimensions={0} | all-to-all | bytes 2097152 | tf_op jit(solution)/shard_map/all_to_all | solution.py:27
  170.4 0.2 convert_reduce_fusion.1
  170.6 0.1 broadcast_in_dim.31
  170.7 16.4 %all_to_all.27 = bf16[4,64,2048]{2,1,0:T(8,128)(2,1)S(1)} all-to-all(bf16[4,64,2048]{2,1,0:T(8,128)(2,1)S(1)} %broadcast_in_dim.31), channel_id=1, replica_groups={{0,2,4,6},{1,3,5,7},{8,10,12,14},{9,11,13,15},{16,18,20,22},{17,19,21,2..., dimensions={0} | all-to-all | bytes 2097152 | tf_op jit(solution)/shard_map/all_to_all | solution.py:27
  187.1 4.0 %collective-permute-start.6 = (bf16[256,2048]{1,0:T(8,128)(2,1)S(1)}, bf16[256,2048]{1,0:T(8,128)(2,1)S(1)}, u32[]{:S(2)}, u32[]{:S(2)}) collective-permute-start(bf16[256,2048]{1,0:T(8,128)(2,1)S(1)} %bitcast.70), channel_id=1, source_target_pairs={{0,1},{1,0},{2,3},{3,2},{4,5},{5,4},{6,7},{7,6},{8,9},{9,8},{10,11... | collective-permute-start | bytes 3145736 | tf_op jit(solution)/shard_map/ppermute | solution.py:23
  191.1 0.2 broadcast_in_dim.24
  191.4 0.1 constant_dynamic-update-slice_fusion.1
  191.5 0.0 copy-start.2
  191.5 1.9 collective-permute-done.6
  193.4 1.0 constant_dynamic-update-slice_fusion
  (37 shorter events, 0.3 us)
Async XLA Ops:
  6.5 19.8 %copy-start = (bf16[128,2048]{1,0:T(8,128)(2,1)S(1)}, bf16[128,2048]{1,0:T(8,128)(2,1)}, u32[]{:S(2)}) copy-start(bf16[128,2048]{1,0:T(8,128)(2,1)} %param.17) | copy-start | bytes 1572868
  6.5 16.7 %copy-start.3 = (bf16[512,64]{0,1:T(8,128)(2,1)S(1)}, bf16[512,64]{0,1:T(8,128)(2,1)}, u32[]{:S(2)}) copy-start(bf16[512,64]{0,1:T(8,128)(2,1)} %param.12) | copy-start | bytes 196612
  6.5 16.8 %copy-start.4 = (bf16[512,64]{0,1:T(8,128)(2,1)S(1)}, bf16[512,64]{0,1:T(8,128)(2,1)}, u32[]{:S(2)}) copy-start(bf16[512,64]{0,1:T(8,128)(2,1)} %param.13) | copy-start | bytes 196612
  6.5 18.2 %copy-start.7 = (s32[512]{0:T(512)S(1)}, s32[512]{0:T(512)}, u32[]{:S(2)}) copy-start(s32[512]{0:T(512)} %param.14) | copy-start | bytes 6148
  6.5 16.8 %copy-start.6 = (bf16[512,128]{1,0:T(8,128)(2,1)S(1)}, bf16[512,128]{1,0:T(8,128)(2,1)}, u32[]{:S(2)}) copy-start(bf16[512,128]{1,0:T(8,128)(2,1)} %param.11) | copy-start | bytes 393220
  6.5 125.8 %all-gather.2.cloned.1.call-start = ((), (), s32[]{:S(2)}) async-start(), calls=%async_computation.5 | async-start | bytes 6684672 | tf_op jit(solution)/shard_map/all_gather | solution.py:141
  18.8 6.6 %copy-start.9 = (f32[2]{0:T(128)S(1)}, f32[2]{0:T(128)}, u32[]{:S(2)}) copy-start(f32[2]{0:T(128)} %param.15) | copy-start | bytes 28
  21.1 3.5 %collective-permute-start = (bf16[136,128]{0,1:T(8,128)(2,1)S(1)}, bf16[136,128]{0,1:T(8,128)(2,1)S(1)}, u32[]{:S(2)}, u32[]{:S(2)}) collective-permute-start(bf16[136,128]{0,1:T(8,128)(2,1)S(1)} %pad_maximum_fusion.3), channel_id=1, source_target_pairs={{0,8},{8,16},{16,24},{24,32},{32,40},{40,48},{48,56},{56,64},{64,7... | collective-permute-start | bytes 104456 | tf_op jit(solution)/shard_map/ppermute | solution.py:19
  28.4 10.7 %copy-start.5 = (bf16[704,32]{0,1:T(8,128)(2,1)S(1)}, bf16[704,32]{0,1:T(8,128)(2,1)}, u32[]{:S(2)}) copy-start(bf16[704,32]{0,1:T(8,128)(2,1)} %param.21) | copy-start | bytes 135172
  28.4 54.9 %all-to-all-start = ((bf16[8,64,2048]{2,1,0:T(8,128)(2,1)}), bf16[8,64,2048]{2,1,0:T(8,128)(2,1)S(1)}, u32[]{:S(2)}, u32[]{:S(2)}) async-start(bf16[8,64,2048]{2,1,0:T(8,128)(2,1)} %bitcast.69), calls=%async_computation | async-start | bytes 4194304 | tf_op jit(solution)/shard_map/all_to_all | solution.py:146
  85.0 2.6 %copy-start.8 = (f32[2048]{0:T(1024)S(1)}, f32[2048]{0:T(1024)}, u32[]{:S(2)}) copy-start(f32[2048]{0:T(1024)} %param.18) | copy-start | bytes 24580
  88.6 13.7 %collective-permute-start.1 = (bf16[64,2048]{1,0:T(8,128)(2,1)}, bf16[64,2048]{1,0:T(8,128)(2,1)}, u32[]{:S(2)}, u32[]{:S(2)}) collective-permute-start(bf16[64,2048]{1,0:T(8,128)(2,1)} %get-tuple-element.20), channel_id=1, source_target_pairs={{0,2},{1,3},{2,4},{3,5},{4,6},{5,7},{6,0},{7,1},{8,10},{9,11},{10,... | collective-permute-start | bytes 786440 | tf_op jit(solution)/shard_map/ppermute | solution.py:36
  91.7 12.2 %collective-permute-start.2 = (bf16[64,2048]{1,0:T(8,128)(2,1)}, bf16[64,2048]{1,0:T(8,128)(2,1)}, u32[]{:S(2)}, u32[]{:S(2)}) collective-permute-start(bf16[64,2048]{1,0:T(8,128)(2,1)} %get-tuple-element.20), channel_id=1, source_target_pairs={{0,6},{1,7},{2,0},{3,1},{4,2},{5,3},{6,4},{7,5},{8,14},{9,15},{10,... | collective-permute-start | bytes 786440 | tf_op jit(solution)/shard_map/ppermute | solution.py:36
  95.1 11.2 %collective-permute-start.3 = (bf16[64,2048]{1,0:T(8,128)(2,1)}, bf16[64,2048]{1,0:T(8,128)(2,1)}, u32[]{:S(2)}, u32[]{:S(2)}) collective-permute-start(bf16[64,2048]{1,0:T(8,128)(2,1)} %get-tuple-element.20), channel_id=1, source_target_pairs={{0,4},{1,5},{2,6},{3,7},{4,0},{5,1},{6,2},{7,3},{8,12},{9,13},{10,... | collective-permute-start | bytes 786440 | tf_op jit(solution)/shard_map/ppermute | solution.py:36
  98.6 30.1 %all-to-all-start.2 = ((bf16[4,512,640]{2,1,0:T(8,128)(2,1)}), bf16[4,512,640]{2,1,0:T(8,128)(2,1)S(1)}, u32[]{:S(2)}, u32[]{:S(2)}) async-start(bf16[4,512,640]{2,1,0:T(8,128)(2,1)} %broadcast_in_dim.28), calls=%async_computation.2 | async-start | bytes 5242880 | tf_op jit(solution)/shard_map/all_to_all | solution.py:27
  108.0 9.3 %collective-permute-start.4 = (bf16[256,2048]{1,0:T(8,128)(2,1)}, bf16[256,2048]{1,0:T(8,128)(2,1)S(1)}, u32[]{:S(2)}, u32[]{:S(2)}) collective-permute-start(bf16[256,2048]{1,0:T(8,128)(2,1)} %constant_dynamic-update-slice_fusion.2), channel_id=1, source_target_pairs={{0,1},{1,0},{2,3},{3,2},{4,5},{5,4},{6,7},{7,6},{8,9},{9,8},{10,11... | collective-permute-start | bytes 3145736 | tf_op jit(solution)/shard_map/ppermute | solution.py:23
  128.7 1.6 copy-start.1
  141.8 10.9 %collective-permute-start.5 = (bf16[256,2048]{1,0:T(8,128)(2,1)S(1)}, bf16[256,2048]{1,0:T(8,128)(2,1)S(1)}, u32[]{:S(2)}, u32[]{:S(2)}) collective-permute-start(bf16[256,2048]{1,0:T(8,128)(2,1)S(1)} %fusion.2), channel_id=1, source_target_pairs={{0,1},{1,0},{2,3},{3,2},{4,5},{5,4},{6,7},{7,6},{8,9},{9,8},{10,11... | collective-permute-start | bytes 3145736 | tf_op jit(solution)/shard_map/ppermute | solution.py:23
  187.1 6.3 %collective-permute-start.6 = (bf16[256,2048]{1,0:T(8,128)(2,1)S(1)}, bf16[256,2048]{1,0:T(8,128)(2,1)S(1)}, u32[]{:S(2)}, u32[]{:S(2)}) collective-permute-start(bf16[256,2048]{1,0:T(8,128)(2,1)S(1)} %bitcast.70), channel_id=1, source_target_pairs={{0,1},{1,0},{2,3},{3,2},{4,5},{5,4},{6,7},{7,6},{8,9},{9,8},{10,11... | collective-permute-start | bytes 3145736 | tf_op jit(solution)/shard_map/ppermute | solution.py:23
  191.5 1.9 copy-start.2
Sparse Core Ops, SparseCore 0:
  18.9 94.6 all-gather.1
